TPU v7x, 512 devices: a whole 4x4x16 slice. The times are simulated.
512 devices in a mesh: sp: 64 (over z, y), tp: 8 (over x, core).
Axes of the slice: x: 4, y: 4, z: 16, core: 2. Of those that a mesh axis runs over, the one named last changes fastest.
Arguments:
- resid: bfloat16 [16384, 2048], P('sp', 'tp'), may hold values from -6 to 6
- queries: bfloat16 [16384, 1024], P('sp', 'tp'), may hold values from -6 to 6
- keys_values: bfloat16 [8, 16384, 128], P('tp', 'sp'), may hold values from -6 to 6
- cum_gate: float32 [16, 16384], P('tp', 'sp'), as said below
- out_weight: bfloat16 [1024, 2048], P(None, 'tp'), may hold values from -1.5 to 1.5
- norm_gain: float32 [2048], replicated, may hold values from 0.1 to 1.9
- gate_weight: bfloat16 [2048, 5632], P('sp', 'tp'), may hold values from -0.125 to 0.125
- up_weight: bfloat16 [2048, 5632], P('sp', 'tp'), may hold values from -0.125 to 0.125
- conv_kernel: float32 [3, 2, 5632], P(None, None, 'tp'), may hold values from -3.5 to 3.5
- down_weight: bfloat16 [5632, 2048], P('tp', 'sp'), may hold values from -0.078125 to 0.078125
Outputs:
- layer_out: bfloat16 [16384, 2048], P('sp', 'tp')
Inputs may be any that keep to these rules, and one draw needn't show every extreme that they name: `cum_gate`: along positions each head's entries never increase.
All inputs are finite; a program needn't handle non-finite values.
Results may differ from a plain program's by a relative error of at most 0.015.
Values may be sent and summed in bfloat16 or wider, within the bound.
No kernel may reach another device: no remote copies, remote signals or barrier semaphores. Data moves between devices by JAX's collectives and lax.ppermute only.
A program may use at most 64 MiB of HBM per device.

v0:
```python
import functools

import jax
import jax.numpy as jnp
from jax import lax
from jax.experimental import pallas as pl
from jax.experimental.pallas import tpu as pltpu
from jax.sharding import Mesh
from jax.sharding import PartitionSpec as P


Z = ("zh", "zl")
Y = ("yh", "yl")
SP = Z + Y
TP = ("x", "c")
NORM_EPS = 1e-06
HALO = 16
MASKED = -1e30
F32 = jnp.float32
BF16 = jnp.bfloat16


def shifted(value, axis, by):
    size = lax.axis_size(axis)
    return lax.ppermute(value, axis, [(i, (i + by) % size) for i in range(size)])


def exchanged(value, axis):
    return lax.all_to_all(value, axis, 0, 0, tiled=True)


def spread(value, axis):
    size = lax.axis_size(axis)
    return exchanged(jnp.broadcast_to(value[None], (size, *value.shape)), axis)


def split3(value):
    high = value.astype(BF16)
    rest = value - high.astype(F32)
    middle = rest.astype(BF16)
    low = (rest - middle.astype(F32)).astype(BF16)
    return high, middle, low


def attend_kernel(at_ref, gate_ref, q_ref, own_ref, next_ref, far_a_ref, far_b_ref, last_ref,
                  out_ref, qa, ka, va, norm_out, lse_rows, lse_dense, *, rows, block):
    zh, zl, y = at_ref[0], at_ref[1], at_ref[2]
    z = 4 * zh + zl
    lane = lax.broadcasted_iota(jnp.int32, (1, 128), 1)
    group = rows - HALO

    def put_queries(start, piece):
        x = piece.astype(F32) * 0.125
        for head in range(2):
            part = x if head == 0 else pltpu.roll(x, 64, 1)
            first = 64 + 3 * head
            ones = jnp.where((lane >= first) & (lane < first + 3), 1.0, 0.0)
            both = jnp.where(lane < 64, part, ones)
            qa[pl.ds(head * rows + start, piece.shape[0]), :] = both.astype(BF16)

    put_queries(0, q_ref[0, 0:HALO, :])
    for i in range(4):
        put_queries(HALO + 256 * i, q_ref[i, HALO:HALO + 256, :])

    part_row = lax.broadcasted_iota(jnp.int32, (16, 256), 0)

    def put_keys(chunk, d, piece):
        cols = pl.ds(256 * d, 256)
        ka[chunk, 0:64, cols] = piece[0:64, :]
        g = piece[64:80, :].astype(F32)
        bias = []
        for head in range(2):
            total = g[3 * head:3 * head + 1, :] + g[3 * head + 1:3 * head + 2, :]
            bias.append(gate_ref[head] - (total + g[3 * head + 2:3 * head + 3, :]))
        b = jnp.where(part_row < 3, bias[0], bias[1])
        which = jnp.where(part_row < 3, part_row, part_row - 3)
        high, middle, low = split3(b)
        pick = jnp.where(which == 0, high.astype(F32), jnp.where(which == 1, middle.astype(F32), low.astype(F32)))
        ka[chunk, 64:80, cols] = jnp.where(part_row < 6, pick, 0.0).astype(BF16)
        ka[chunk, 80:128, cols] = jnp.zeros((48, 256), BF16)
        va[chunk, 0:64, cols] = piece[80:144, :]
        va[chunk, 64:128, cols] = jnp.ones((64, 256), BF16)

    for chunk in range(4):
        far = far_a_ref[chunk] if chunk < 2 else far_b_ref[chunk - 2]
        pieces = (own_ref[chunk], next_ref[chunk], far, last_ref[chunk])
        for d in range(4):
            put_keys(chunk, d, pieces[d])

    key_lane = lax.broadcasted_iota(jnp.int32, (1, 1024), 1)
    key_d = key_lane // 256
    first_masked = jnp.maximum(zh - jnp.where(zl == 0, 1, 0), 0)

    def row_block(r, _):
        start = pl.multiple_of(r * block, block)
        q = qa[pl.ds(start, block), :]
        row = start + lax.broadcasted_iota(jnp.int32, (block, 1), 0)
        query_pos = z * group - HALO + jnp.where(row >= rows, row - rows, row)

        def step(masked, chunk, state):
            top, acc = state
            s = lax.dot_general(q, ka[chunk], (((1,), (0,)), ((), ())), preferred_element_type=F32)
            if masked:
                turn = zl + key_d
                key_z = 4 * chunk + jnp.where(turn >= 4, turn - 4, turn)
                key_pos = key_z * group + y * 256 + (key_lane - 256 * key_d)
                s = jnp.where(query_pos >= key_pos, s, MASKED)
            new_top = jnp.maximum(top, jnp.max(s, axis=1, keepdims=True))
            p = jnp.exp(s - new_top).astype(BF16)
            more = lax.dot_general(p, va[chunk], (((1,), (1,)), ((), ())), preferred_element_type=F32)
            return new_top, acc * jnp.exp(top - new_top) + more

        state = (jnp.full((block, 1), MASKED, F32), jnp.zeros((block, 128), F32))
        state = lax.fori_loop(0, first_masked, functools.partial(step, False), state)
        top, acc = lax.fori_loop(first_masked, zh + 1, functools.partial(step, True), state)
        total = acc[:, 64:65]
        gate = jnp.where(row >= rows, gate_ref[1], gate_ref[0])
        norm_out[pl.ds(start, block), :] = acc / total
        lse_rows[pl.ds(start, block), :] = jnp.broadcast_to(top + jnp.log(total) - gate, (block, 128))
        return 0

    lax.fori_loop(0, 2 * rows // block, row_block, 0)
    tail = lse_rows.shape[0] - 2 * rows
    lse_rows[pl.ds(2 * rows, tail), :] = jnp.zeros((tail, 128), F32)
    lse_dense[...] = jnp.zeros(lse_dense.shape, F32)
    diagonal = lax.broadcasted_iota(jnp.int32, (128, 128), 0) == lax.broadcasted_iota(jnp.int32, (128, 128), 1)
    pair_rows = HALO + 512
    for pair in range(2):
        a = norm_out[pl.ds(512 * pair, pair_rows), :]
        b = norm_out[pl.ds(rows + 512 * pair, pair_rows), :]
        joined = jnp.where(lane < 64, a, pltpu.roll(b, 64, 1)).astype(BF16)
        for head in range(2):
            for t in range(5):
                tile = lse_rows[pl.ds(head * rows + 512 * pair + 128 * t, 128), :]
                lse_dense[pl.ds(5 * head + t, 1), :] = jnp.sum(jnp.where(diagonal, tile, 0.0), axis=0, keepdims=True)
        parts = split3(lse_dense[...])
        for i in range(2):
            out_ref[2 * pair + i, 0:pair_rows, :] = joined
            for k in range(3):
                out_ref[2 * pair + i, pair_rows + 16 * k:pair_rows + 16 * (k + 1), :] = parts[k]


def attend(at, gate, queries, own, nxt, far_a, far_b, last):
    rows = HALO + 1024
    pair_rows = HALO + 512
    smem = pl.BlockSpec(memory_space=pltpu.SMEM)
    vmem = pl.BlockSpec(memory_space=pltpu.VMEM)
    return pl.pallas_call(
        functools.partial(attend_kernel, rows=rows, block=416),
        out_shape=jax.ShapeDtypeStruct((4, pair_rows + 48, 128), BF16),
        in_specs=[smem, smem] + [vmem] * 6,
        out_specs=vmem,
        scratch_shapes=[
            pltpu.VMEM((2 * rows, 128), BF16),
            pltpu.VMEM((4, 128, 1024), BF16),
            pltpu.VMEM((4, 128, 1024), BF16),
            pltpu.VMEM((2 * rows, 128), F32),
            pltpu.VMEM((2 * rows + 112, 128), F32),
            pltpu.VMEM((16, 128), F32),
        ],
        compiler_params=pltpu.CompilerParams(vmem_limit_bytes=24 * 2**20),
        cost_estimate=pl.CostEstimate(flops=8 * 10**9, bytes_accessed=4 * 2**20, transcendentals=8 * 10**6),
        name="attend",
    )(at, gate, queries, own, nxt, far_a, far_b, last)


def merge_kernel(in_ref, out_ref):
    pair_rows = HALO + 512
    logs = []
    for i in range(4):
        parts = [in_ref[i, pair_rows + 16 * k:pair_rows + 16 * (k + 1), :].astype(F32) for k in range(3)]
        logs.append(parts[0] + parts[1] + parts[2])
    top = jnp.maximum(jnp.maximum(logs[0], logs[1]), jnp.maximum(logs[2], logs[3]))
    weights = [jnp.exp(v - top) for v in logs]
    total = weights[0] + weights[1] + weights[2] + weights[3]
    shares = [w / total for w in weights]
    lane = lax.broadcasted_iota(jnp.int32, (1, 128), 1)
    for t in range(5):
        size = 128 if t < 4 else pair_rows - 512
        diagonal = lax.broadcasted_iota(jnp.int32, (size, 128), 0) == lax.broadcasted_iota(jnp.int32, (size, 128), 1)
        acc = jnp.zeros((size, 128), F32)
        for i in range(4):
            cols = [
                jnp.sum(jnp.where(diagonal, shares[i][5 * head + t:5 * head + t + 1, :], 0.0), axis=1, keepdims=True)
                for head in range(2)
            ]
            share = jnp.where(lane < 64, cols[0], cols[1])
            acc = acc + share * in_ref[i, 128 * t:128 * t + size, :].astype(F32)
        out_ref[128 * t:128 * t + size, :] = acc.astype(BF16)


def merge(pieces):
    vmem = pl.BlockSpec(memory_space=pltpu.VMEM)
    return pl.pallas_call(
        merge_kernel,
        out_shape=jax.ShapeDtypeStruct((HALO + 512, 128), BF16),
        in_specs=[vmem],
        out_specs=vmem,
        compiler_params=pltpu.CompilerParams(vmem_limit_bytes=8 * 2**20),
        cost_estimate=pl.CostEstimate(flops=10**8, bytes_accessed=2**20, transcendentals=10**4),
        name="merge",
    )(pieces)


def feed_kernel(at_ref, attn_own, attn_other, out_own, out_other, resid_own, resid_other, gain_ref, conv_ref, w_ref,
                keep_ref, send_ref, mid_out_ref, af, mid, normed, wg, wu, wd, sems):
    copies = []
    for k, dst in enumerate((wg, wu, wd)):
        copy = pltpu.make_async_copy(w_ref.at[:, :, k], dst, sems.at[k])
        copy.start()
        copies.append(copy)
    is_first, half, core = at_ref[3], at_ref[4], at_ref[6]
    block = at_ref[5]
    rows = HALO + 512
    at_x = block // 2
    sides = ((core, attn_own, out_own, resid_own, keep_ref), (1 - core, attn_other, out_other, resid_other, send_ref))
    for c, attn, _, _, _ in sides:
        for x in range(4):
            af[:, pl.ds(pl.multiple_of(128 * (2 * x + c), 128), 128)] = attn[x]
    a = af[...]
    square = jnp.zeros((rows, 1), F32)
    for c, _, out, resid, _ in sides:
        for i, back in enumerate((0, 1, 3, 2)):
            x = jnp.where(at_x >= back, at_x - back, at_x - back + 4)
            branch = jnp.dot(a, out[i], preferred_element_type=F32)
            m = (branch + resid[x].astype(F32)).astype(BF16)
            mid[:, pl.ds(pl.multiple_of(256 * (2 * x + c), 256), 256)] = m
            m = m.astype(F32)
            square = square + jnp.sum(m * m, axis=1, keepdims=True)
    inverse = lax.rsqrt(square * (1.0 / 2048) + NORM_EPS)
    for j in range(8):
        cols = slice(256 * j, 256 * (j + 1))
        normed[:, cols] = (mid[:, cols].astype(F32) * inverse * gain_ref[:, cols]).astype(BF16)
    mid_out_ref[...] = mid[pl.ds(pl.multiple_of(HALO + 256 * half, 16), 256), pl.ds(pl.multiple_of(256 * block, 256), 256)]
    n = normed[...]
    copies[0].wait()
    copies[1].wait()
    row = lax.broadcasted_iota(jnp.int32, (rows, 1), 0)
    keep = jnp.logical_not((row < HALO) & (is_first == 1))

    def mixed(weight, index):
        pre = jnp.dot(n, weight[...].reshape(2048, 352), preferred_element_type=F32).astype(BF16).astype(F32)
        pre = jnp.where(keep, pre, 0.0)
        total = jnp.zeros((512, 352), F32)
        for k in range(3):
            total = total + conv_ref[2 * k + index:2 * k + index + 1, :] * pre[HALO - 2 + k:HALO - 2 + k + 512]
        return total

    gate = mixed(wg, 0)
    up = mixed(wu, 1)
    hidden = (gate / (1.0 + jnp.exp(-gate)) * up).astype(BF16)
    copies[2].wait()
    for c, _, _, _, part_ref in sides:
        for x in range(4):
            down = wd[pl.ds(2 * (2 * x + c), 2)].reshape(256, 352)
            part = lax.dot_general(hidden, down, (((1,), (1,)), ((), ())), preferred_element_type=F32).astype(BF16)
            for p in range(2):
                part_ref[p, x] = part[256 * p:256 * (p + 1)]


def feed(at, attn, other_attn, out, other_out, resid, other_resid, gain, conv, weights):
    smem = pl.BlockSpec(memory_space=pltpu.SMEM)
    vmem = pl.BlockSpec(memory_space=pltpu.VMEM)
    rows = HALO + 512
    half = jax.ShapeDtypeStruct((2, 4, 256, 256), BF16)
    return pl.pallas_call(
        feed_kernel,
        out_shape=(half, half, jax.ShapeDtypeStruct((256, 256), BF16)),
        in_specs=[smem] + [vmem] * 8 + [pl.BlockSpec(memory_space=pltpu.HBM)],
        out_specs=(vmem, vmem, vmem),
        scratch_shapes=[
            pltpu.VMEM((rows, 1024), BF16),
            pltpu.VMEM((rows, 2048), BF16),
            pltpu.VMEM((rows, 2048), BF16),
            pltpu.VMEM((16, 4, 32, 352), BF16),
            pltpu.VMEM((16, 4, 32, 352), BF16),
            pltpu.VMEM((16, 4, 32, 352), BF16),
            pltpu.SemaphoreType.DMA((3,)),
        ],
        compiler_params=pltpu.CompilerParams(vmem_limit_bytes=40 * 2**20),
        cost_estimate=pl.CostEstimate(flops=5 * 10**9, bytes_accessed=2**24, transcendentals=2 * 10**5),
        name="feed",
    )(at, attn, other_attn, out, other_out, resid, other_resid, gain, conv, weights)


def keys_kernel(kv_ref, gate_ref, out_ref):
    turned = kv_ref[0].astype(F32).T.astype(BF16)
    row = lax.broadcasted_iota(jnp.int32, (16, 256), 0)
    value = jnp.where(row < 3, gate_ref[0:1, :], gate_ref[1:2, :])
    which = jnp.where(row < 3, row, row - 3)
    high, middle, low = split3(value)
    pick = jnp.where(which == 0, high.astype(F32), jnp.where(which == 1, middle.astype(F32), low.astype(F32)))
    gates = jnp.where(row < 6, pick, 0.0).astype(BF16)
    for i in range(4):
        out_ref[i, 0:64, :] = turned[0:64]
        out_ref[i, 64:80, :] = gates
        out_ref[i, 80:144, :] = turned[64:128]


def halves_kernel(gate_ref, up_ref, down_ref, out_ref):
    for k, ref in enumerate((gate_ref, up_ref, down_ref)):
        value = ref[...].astype(F32)
        for p in range(2):
            piece = value[:, 352 * p:352 * (p + 1)].astype(BF16)
            for i in range(2):
                out_ref[2 * i + p, k] = piece


def small_call(kernel, shape, *operands):
    vmem = pl.BlockSpec(memory_space=pltpu.VMEM)
    return pl.pallas_call(
        kernel,
        out_shape=jax.ShapeDtypeStruct(shape, BF16),
        in_specs=[vmem] * len(operands),
        out_specs=vmem,
        compiler_params=pltpu.CompilerParams(vmem_limit_bytes=8 * 2**20),
        cost_estimate=pl.CostEstimate(flops=10**7, bytes_accessed=2**20, transcendentals=0),
    )(*operands)


def layer(resid, queries, keys_values, cum_gate, out_weight, norm_gain, gate_weight, up_weight, conv_kernel, down_weight):
    zh, zl = lax.axis_index("zh"), lax.axis_index("zl")
    y, half = lax.axis_index(Y), lax.axis_index("yl")
    is_first = (lax.axis_index(SP) < 2).astype(jnp.int32)
    at = jnp.stack([zh, zl, y, is_first, half, lax.axis_index(TP), lax.axis_index("c")]).astype(jnp.int32)

    own = exchanged(small_call(keys_kernel, (4, 144, 256), keys_values, cum_gate), "zh")
    rows_y = exchanged(small_call(halves_kernel, (4, 3, 32, 352), gate_weight, up_weight, down_weight.T), Y)
    weights = lax.all_gather(rows_y, Z, axis=0, tiled=False)
    tail = jnp.concatenate([queries[-HALO:], resid[-HALO:]], axis=1)
    before = shifted(tail, SP, 1)
    out = jnp.stack([out_weight] + [shifted(out_weight, "x", by) for by in (1, 3, 2)])
    other_out = shifted(out, "c", 1)
    group_q = spread(jnp.concatenate([before[:, :128], queries], axis=0), Y)
    last = shifted(own, Z, 1)
    nxt = shifted(own, Z, -1)
    far_a = shifted(own[:2], Z, -2)
    far_b = shifted(own[2:], Z, 2)
    mine = jnp.concatenate([before[:, 128:], resid], axis=0)
    theirs = shifted(mine, "yl", 1)
    pair = jnp.where(
        half == 0,
        jnp.concatenate([mine, theirs[HALO:]], axis=0),
        jnp.concatenate([theirs, mine[HALO:]], axis=0),
    )
    pair = spread(pair, "x")
    other_pair = shifted(pair, "c", 1)

    partial = attend(at, cum_gate[:, 0], group_q, own, nxt, far_a, far_b, last)
    partial = exchanged(partial, Y)
    attn = merge(partial)
    attn = lax.all_gather(attn, "x", axis=0, tiled=False)
    other_attn = shifted(attn, "c", 1)
    conv = lax.dynamic_slice_in_dim(conv_kernel.reshape(6, 704), half * 352, 352, 1)
    keep, send, middle = feed(
        at, attn, other_attn, out, other_out, pair, other_pair, norm_gain.reshape(1, 2048), conv, weights
    )
    got = shifted(send, "c", 1)
    chip = (keep.astype(F32) + got.astype(F32)).astype(BF16).reshape(8, 256, 256)
    pieces = exchanged(chip, ("yl", "x"))
    total = jnp.sum(pieces.astype(F32), axis=0)
    return (middle.astype(F32) + total).astype(BF16)


def solution(mesh):
    finer = Mesh(mesh.devices.reshape(4, 4, 2, 2, 4, 2), SP + TP)
    return jax.shard_map(
        layer,
        mesh=finer,
        in_specs=(
            P(SP, TP),
            P(SP, TP),
            P(TP, SP, None),
            P(TP, SP),
            P(None, TP),
            P(),
            P(SP, TP),
            P(SP, TP),
            P(None, None, TP),
            P(TP, SP),
        ),
        out_specs=P(SP, TP),
        check_vma=False,
    )
```

profile of v0, /device:TPU:384, one launch (start us, length us, event | category | flops | bytes accessed | tf_op | source)
XLA Modules:
  0.0 196.9 jit_solution(11894669161425677975)
XLA Ops:
  9.1 11.5 %all_to_all.30 = bf16[4,3,32,352]{3,2,1,0:T(8,128)(2,1)} all-to-all(bf16[4,3,32,352]{3,2,1,0:T(8,128)(2,1)S(1)} %shard_map.101), channel_id=1, replica_groups=mesh['zh'=4,'zl'=4,'yh'=2,'yl'=2,'x'=4,'c'=2] {'yh','yl'}, dimensions={0} | all-to-all | bytes 540672 | tf_op jit(solution)/shard_map/all_to_all | solution.py:29
  22.9 10.2 %all-to-all-start.1 = ((bf16[4,144,256]{2,1,0:T(8,128)(2,1)}), bf16[4,144,256]{2,1,0:T(8,128)(2,1)S(1)}, u32[]{:S(2)}, u32[]{:S(2)}) async-start(bf16[4,144,256]{2,1,0:T(8,128)(2,1)} %shard_map.100), calls=%async_computation.1 | async-start | bytes 589824 | tf_op jit(solution)/shard_map/all_to_all | solution.py:29
  33.1 3.4 %collective-permute-start.6 = (bf16[1024,256]{1,0:T(8,128)(2,1)S(1)}, bf16[1024,256]{1,0:T(8,128)(2,1)S(1)}, u32[]{:S(2)}, u32[]{:S(2)}) collective-permute-start(bf16[1024,256]{1,0:T(8,128)(2,1)S(1)} %copy-done.10), channel_id=1, source_target_pairs={{0,2},{2,4},{4,6},{6,0},{1,3},{3,5},{5,7},{7,1},{8,10},{10,12},{12... | collective-permute-start | bytes 1572872 | tf_op jit(solution)/shard_map/ppermute | solution.py:25
  36.5 4.6 %collective-permute-start.8 = (bf16[1024,256]{1,0:T(8,128)(2,1)S(1)}, bf16[1024,256]{1,0:T(8,128)(2,1)S(1)}, u32[]{:S(2)}, u32[]{:S(2)}) collective-permute-start(bf16[1024,256]{1,0:T(8,128)(2,1)S(1)} %copy-done.10), channel_id=1, source_target_pairs={{0,4},{2,6},{4,0},{6,2},{1,5},{3,7},{5,1},{7,3},{8,12},{10,14},{12... | collective-permute-start | bytes 1572872 | tf_op jit(solution)/shard_map/ppermute | solution.py:25
  41.2 3.3 %collective-permute-start.7 = (bf16[1024,256]{1,0:T(8,128)(2,1)S(1)}, bf16[1024,256]{1,0:T(8,128)(2,1)S(1)}, u32[]{:S(2)}, u32[]{:S(2)}) collective-permute-start(bf16[1024,256]{1,0:T(8,128)(2,1)S(1)} %copy-done.10), channel_id=1, source_target_pairs={{0,6},{2,0},{4,2},{6,4},{1,7},{3,1},{5,3},{7,5},{8,14},{10,8},{12,... | collective-permute-start | bytes 1572872 | tf_op jit(solution)/shard_map/ppermute | solution.py:25
  44.6 2.5 %collective-permute-start = (bf16[16,384]{1,0:T(8,128)(2,1)S(1)}, bf16[16,384]{1,0:T(8,128)(2,1)S(1)}, u32[]{:S(2)}, u32[]{:S(2)}) collective-permute-start(bf16[16,384]{1,0:T(8,128)(2,1)S(1)} %pad_maximum_fusion.3), channel_id=1, source_target_pairs={{0,8},{8,16},{16,24},{24,32},{32,40},{40,48},{48,56},{56,64},{64,7... | collective-permute-start | bytes 36872 | tf_op jit(solution)/shard_map/ppermute | solution.py:25
  47.0 6.8 %collective-permute-done = bf16[16,384]{1,0:T(8,128)(2,1)S(1)} collective-permute-done((bf16[16,384]{1,0:T(8,128)(2,1)S(1)}, bf16[16,384]{1,0:T(8,128)(2,1)S(1)}, u32[]{:S(2)}, u32[]{:S(2)}) %collective-permute-start) | collective-permute-done | bytes 12320 | tf_op jit(solution)/shard_map/ppermute | solution.py:25
  55.9 4.9 %collective-permute-done.10 = bf16[272,256]{1,0:T(8,128)(2,1)S(1)} collective-permute-done((bf16[272,256]{1,0:T(8,128)(2,1)S(1)}, bf16[272,256]{1,0:T(8,128)(2,1)S(1)}, u32[]{:S(2)}, u32[]{:S(2)}) %collective-permute-start.10) | collective-permute-done | bytes 139296 | tf_op jit(solution)/shard_map/ppermute | solution.py:25
  67.1 3.4 %all-to-all-start = ((bf16[4,272,128]{2,1,0:T(8,128)(2,1)}), bf16[4,272,128]{2,1,0:T(8,128)(2,1)S(1)}, u32[]{:S(2)}, u32[]{:S(2)}) async-start(bf16[4,272,128]{2,1,0:T(8,128)(2,1)} %broadcast_in_dim.4), calls=%async_computation | async-start | bytes 557056 | tf_op jit(solution)/shard_map/all_to_all | solution.py:29
  70.5 2.6 %collective-permute-start.4 = (bf16[4,144,256]{2,1,0:T(8,128)(2,1)S(1)}, bf16[4,144,256]{2,1,0:T(8,128)(2,1)S(1)}, u32[]{:S(2)}, u32[]{:S(2)}) collective-permute-start(bf16[4,144,256]{2,1,0:T(8,128)(2,1)S(1)} %all-to-all-done.1.own_ref), channel_id=1, source_target_pairs={{0,32},{32,64},{64,96},{96,128},{128,160},{160,192},{192,224},{224... | collective-permute-start | bytes 884744 | tf_op jit(solution)/shard_map/ppermute | solution.py:25
  73.2 4.9 %collective-permute-start.1 = (bf16[4,144,256]{2,1,0:T(8,128)(2,1)S(1)}, bf16[4,144,256]{2,1,0:T(8,128)(2,1)S(1)}, u32[]{:S(2)}, u32[]{:S(2)}) collective-permute-start(bf16[4,144,256]{2,1,0:T(8,128)(2,1)S(1)} %all-to-all-done.1.own_ref), channel_id=1, source_target_pairs={{0,480},{32,0},{64,32},{96,64},{128,96},{160,128},{192,160},{224,1... | collective-permute-start | bytes 884744 | tf_op jit(solution)/shard_map/ppermute | solution.py:25
  80.8 6.0 %collective-permute-start.2 = (bf16[2,144,256]{2,1,0:T(8,128)(2,1)}, bf16[2,144,256]{2,1,0:T(8,128)(2,1)}, u32[]{:S(2)}, u32[]{:S(2)}) collective-permute-start(bf16[2,144,256]{2,1,0:T(8,128)(2,1)} %get-tuple-element.12), channel_id=1, source_target_pairs={{0,448},{32,480},{64,0},{96,32},{128,64},{160,96},{192,128},{224,1... | collective-permute-start | bytes 442376 | tf_op jit(solution)/shard_map/ppermute | solution.py:25
  88.6 2.1 %broadcast_in_dim.5 = bf16[4,528,256]{2,1,0:T(8,128)(2,1)} broadcast(bf16[528,256]{1,0:T(8,128)(2,1)} %maximum_select_fusion), dimensions={1,2} | broadcast | bytes 1351680 | tf_op jit(solution)/shard_map/broadcast_in_dim | solution.py:34
  90.7 4.3 %all-to-all-start.3 = ((bf16[4,528,256]{2,1,0:T(8,128)(2,1)}), bf16[4,528,256]{2,1,0:T(8,128)(2,1)}, u32[]{:S(2)}, u32[]{:S(2)}) async-start(bf16[4,528,256]{2,1,0:T(8,128)(2,1)} %broadcast_in_dim.5), calls=%async_computation.3 | async-start | bytes 2162688 | tf_op jit(solution)/shard_map/all_to_all | solution.py:29
  95.1 5.3 %collective-permute-done.3.far_b_ref = bf16[2,144,256]{2,1,0:T(8,128)(2,1)S(1)} collective-permute-done((bf16[2,144,256]{2,1,0:T(8,128)(2,1)}, bf16[2,144,256]{2,1,0:T(8,128)(2,1)S(1)}, u32[]{:S(2)}, u32[]{:S(2)}) %collective-permute-start.3) | collective-permute-done | bytes 147488 | tf_op jit(solution)/shard_map/ppermute | solution.py:25
  100.6 19.9 %attend.1 = bf16[4,576,128]{2,1,0:T(8,128)(2,1)} custom-call(s32[7]{0:T(128)S(1)} %stack.50.at_ref, f32[2]{0:T(128)S(1)} %slice_reduce_fusion.gate_ref, bf16[4,272,128]{2,1,0:T(8,128)(2,1)S(1)} %all-to-all-done.q_ref, bf16[4,144,256]{2,1,0:T(8,128)(2,1)S(1)} %all-to-all-done.1.own_ref, bf16[4,144,256]{2,1,0:T(8,128)(2,1)S(1)} %collective-permute-done.1.next_ref, ...), custom_call_target="tpu_custom_call" | custom-call | flops 8000000000 | bytes 4194304 | tf_op jit(solution)/shard_map/attend/pallas_call | solution.py:148
  120.6 4.9 %all-to-all-start.2 = ((bf16[4,576,128]{2,1,0:T(8,128)(2,1)}), bf16[4,576,128]{2,1,0:T(8,128)(2,1)S(1)}, u32[]{:S(2)}, u32[]{:S(2)}) async-start(bf16[4,576,128]{2,1,0:T(8,128)(2,1)} %attend.1), calls=%async_computation.2 | async-start | bytes 1179648 | tf_op jit(solution)/shard_map/all_to_all | solution.py:29
  127.4 7.6 %all-to-all-done.2.in_ref = bf16[4,576,128]{2,1,0:T(8,128)(2,1)S(1)} async-done(((bf16[4,576,128]{2,1,0:T(8,128)(2,1)}), bf16[4,576,128]{2,1,0:T(8,128)(2,1)S(1)}, u32[]{:S(2)}, u32[]{:S(2)}) %all-to-all-start.2) | async-done | bytes 589856 | tf_op jit(solution)/shard_map/all_to_all | solution.py:29
  135.7 13.1 %all-gather = bf16[2112,128]{1,0:T(8,128)(2,1)S(1)} all-gather(bf16[528,128]{1,0:T(8,128)(2,1)S(1)} %merge.1), channel_id=2, replica_groups=mesh['zh'=4,'zl'=4,'yh'=2,'yl'=2,'x'=4,'c'=2] {'x'}, dimensions={0}, use_global_device_ids=true | all-gather | bytes 675840 | tf_op jit(solution)/shard_map/all_gather | solution.py:352
  148.7 2.1 %collective-permute-start.5 = (bf16[4,528,128]{2,1,0:T(8,128)(2,1)S(1)}, bf16[4,528,128]{2,1,0:T(8,128)(2,1)S(1)}, u32[]{:S(2)}, u32[]{:S(2)}) collective-permute-start(bf16[4,528,128]{2,1,0:T(8,128)(2,1)S(1)} %bitcast.16), channel_id=1, source_target_pairs={{0,1},{1,0},{2,3},{3,2},{4,5},{5,4},{6,7},{7,6},{8,9},{9,8},{10,11... | collective-permute-start | bytes 1622024 | tf_op jit(solution)/shard_map/ppermute | solution.py:25
  152.6 2.3 %copy-done.6 = bf16[64,3,32,352]{3,2,1,0:T(8,128)(2,1)S(1)} copy-done((bf16[64,3,32,352]{3,2,1,0:T(8,128)(2,1)S(1)}, bf16[64,3,32,352]{3,2,1,0:T(8,128)(2,1)}, u32[]{:S(2)}) %copy-start.6) | copy-done | bytes 4325400
  154.9 10.3 %feed.1 = (bf16[2,4,256,256]{3,2,1,0:T(8,128)(2,1)S(1)}, bf16[2,4,256,256]{3,2,1,0:T(8,128)(2,1)S(1)}, bf16[256,256]{1,0:T(8,128)(2,1)S(1)}) custom-call(s32[7]{0:T(128)S(1)} %stack.50.at_ref, bf16[4,528,128]{2,1,0:T(8,128)(2,1)S(1)} %bitcast.17, bf16[4,528,128]{2,1,0:T(8,128)(2,1)S(1)} %collective-permute-done.5.attn_other, ...), custom_call_target="tpu_custom_call" | custom-call | flops 5000000000 | bytes 16777216 | tf_op jit(solution)/shard_map/feed/pallas_call | solution.py:266
  167.3 2.5 %collective-permute-done.12 = bf16[2,4,256,256]{3,2,1,0:T(8,128)(2,1)S(1)} collective-permute-done((bf16[2,4,256,256]{3,2,1,0:T(8,128)(2,1)S(1)}, bf16[2,4,256,256]{3,2,1,0:T(8,128)(2,1)S(1)}, u32[]{:S(2)}, u32[]{:S(2)}) %collective-permute-start.12) | collective-permute-done | bytes 1048608 | tf_op jit(solution)/shard_map/ppermute | solution.py:25
  170.0 19.2 %all_to_all.31 = bf16[8,256,256]{2,1,0:T(8,128)(2,1)S(1)} all-to-all(bf16[8,256,256]{2,1,0:T(8,128)(2,1)S(1)} %bitcast.21), channel_id=1, replica_groups=mesh['zh'=4,'zl'=4,'yh'=2,'yl'=2,'x'=4,'c'=2] {'yl','x'}, dimensions={0} | all-to-all | bytes 2097152 | tf_op jit(solution)/shard_map/all_to_all | solution.py:29
  (75 shorter events, 25.2 us)
Async XLA Ops:
  6.5 146.0 %all-gather.4.cloned.1.call-start = ((), (), s32[]{:S(2)}) async-start(), calls=%async_computation.6 | async-start | bytes 5013504 | tf_op jit(solution)/shard_map/all_gather | solution.py:329
  8.9 35.6 %slice-start = ((bf16[256,256]{1,0:T(8,128)(2,1)}), bf16[16,256]{1,0:T(8,128)(2,1)S(1)}, s32[]{:S(2)}) async-start(bf16[256,256]{1,0:T(8,128)(2,1)} %param.10), calls=%async_computation.7 | async-start | bytes 16384 | tf_op jit(solution)/shard_map/slice | solution.py:330
  8.9 35.6 %slice-start.1 = ((bf16[256,128]{1,0:T(8,128)(2,1)}), bf16[16,128]{1,0:T(8,128)(2,1)S(1)}, s32[]{:S(2)}) async-start(bf16[256,128]{1,0:T(8,128)(2,1)} %param.11), calls=%async_computation.8 | async-start | bytes 8192 | tf_op jit(solution)/shard_map/slice | solution.py:330
  8.9 44.9 %copy-start.8 = (bf16[256,256]{1,0:T(8,128)(2,1)S(1)}, bf16[256,256]{1,0:T(8,128)(2,1)}, u32[]{:S(2)}) copy-start(bf16[256,256]{1,0:T(8,128)(2,1)} %param.10) | copy-start | bytes 393220
  8.9 47.0 %copy-start.14 = (bf16[256,128]{1,0:T(8,128)(2,1)S(1)}, bf16[256,128]{1,0:T(8,128)(2,1)}, u32[]{:S(2)}) copy-start(bf16[256,128]{1,0:T(8,128)(2,1)} %param.11) | copy-start | bytes 196612
  22.9 43.4 %all-to-all-start.1 = ((bf16[4,144,256]{2,1,0:T(8,128)(2,1)}), bf16[4,144,256]{2,1,0:T(8,128)(2,1)S(1)}, u32[]{:S(2)}, u32[]{:S(2)}) async-start(bf16[4,144,256]{2,1,0:T(8,128)(2,1)} %shard_map.100), calls=%async_computation.1 | async-start | bytes 589824 | tf_op jit(solution)/shard_map/all_to_all | solution.py:29
  33.1 28.4 %collective-permute-start.6 = (bf16[1024,256]{1,0:T(8,128)(2,1)S(1)}, bf16[1024,256]{1,0:T(8,128)(2,1)S(1)}, u32[]{:S(2)}, u32[]{:S(2)}) collective-permute-start(bf16[1024,256]{1,0:T(8,128)(2,1)S(1)} %copy-done.10), channel_id=1, source_target_pairs={{0,2},{2,4},{4,6},{6,0},{1,3},{3,5},{5,7},{7,1},{8,10},{10,12},{12... | collective-permute-start | bytes 1572872 | tf_op jit(solution)/shard_map/ppermute | solution.py:25
  36.5 25.0 %collective-permute-start.8 = (bf16[1024,256]{1,0:T(8,128)(2,1)S(1)}, bf16[1024,256]{1,0:T(8,128)(2,1)S(1)}, u32[]{:S(2)}, u32[]{:S(2)}) collective-permute-start(bf16[1024,256]{1,0:T(8,128)(2,1)S(1)} %copy-done.10), channel_id=1, source_target_pairs={{0,4},{2,6},{4,0},{6,2},{1,5},{3,7},{5,1},{7,3},{8,12},{10,14},{12... | collective-permute-start | bytes 1572872 | tf_op jit(solution)/shard_map/ppermute | solution.py:25
  41.2 20.5 %collective-permute-start.7 = (bf16[1024,256]{1,0:T(8,128)(2,1)S(1)}, bf16[1024,256]{1,0:T(8,128)(2,1)S(1)}, u32[]{:S(2)}, u32[]{:S(2)}) collective-permute-start(bf16[1024,256]{1,0:T(8,128)(2,1)S(1)} %copy-done.10), channel_id=1, source_target_pairs={{0,6},{2,0},{4,2},{6,4},{1,7},{3,1},{5,3},{7,5},{8,14},{10,8},{12,... | collective-permute-start | bytes 1572872 | tf_op jit(solution)/shard_map/ppermute | solution.py:25
  44.6 9.3 %collective-permute-start = (bf16[16,384]{1,0:T(8,128)(2,1)S(1)}, bf16[16,384]{1,0:T(8,128)(2,1)S(1)}, u32[]{:S(2)}, u32[]{:S(2)}) collective-permute-start(bf16[16,384]{1,0:T(8,128)(2,1)S(1)} %pad_maximum_fusion.3), channel_id=1, source_target_pairs={{0,8},{8,16},{16,24},{24,32},{32,40},{40,48},{48,56},{56,64},{64,7... | collective-permute-start | bytes 36872 | tf_op jit(solution)/shard_map/ppermute | solution.py:25
  53.9 6.9 %collective-permute-start.10 = (bf16[272,256]{1,0:T(8,128)(2,1)S(1)}, bf16[272,256]{1,0:T(8,128)(2,1)S(1)}, u32[]{:S(2)}, u32[]{:S(2)}) collective-permute-start(bf16[272,256]{1,0:T(8,128)(2,1)S(1)} %pad_maximum_fusion.1), channel_id=1, source_target_pairs={{0,8},{8,0},{1,9},{9,1},{2,10},{10,2},{3,11},{11,3},{4,12},{12,4},... | collective-permute-start | bytes 417800 | tf_op jit(solution)/shard_map/ppermute | solution.py:25
  64.4 88.2 %collective-permute-start.9 = (bf16[4,1024,256]{2,1,0:T(8,128)(2,1)S(1)}, bf16[4,1024,256]{2,1,0:T(8,128)(2,1)}, u32[]{:S(2)}, u32[]{:S(2)}) collective-permute-start(bf16[4,1024,256]{2,1,0:T(8,128)(2,1)S(1)} %pad_maximum_fusion.out_own), channel_id=1, source_target_pairs={{0,1},{1,0},{2,3},{3,2},{4,5},{5,4},{6,7},{7,6},{8,9},{9,8},{10,11... | collective-permute-start | bytes 6291464 | tf_op jit(solution)/shard_map/ppermute | solution.py:25
  67.1 21.5 %all-to-all-start = ((bf16[4,272,128]{2,1,0:T(8,128)(2,1)}), bf16[4,272,128]{2,1,0:T(8,128)(2,1)S(1)}, u32[]{:S(2)}, u32[]{:S(2)}) async-start(bf16[4,272,128]{2,1,0:T(8,128)(2,1)} %broadcast_in_dim.4), calls=%async_computation | async-start | bytes 557056 | tf_op jit(solution)/shard_map/all_to_all | solution.py:29
  70.5 30.1 %collective-permute-start.4 = (bf16[4,144,256]{2,1,0:T(8,128)(2,1)S(1)}, bf16[4,144,256]{2,1,0:T(8,128)(2,1)S(1)}, u32[]{:S(2)}, u32[]{:S(2)}) collective-permute-start(bf16[4,144,256]{2,1,0:T(8,128)(2,1)S(1)} %all-to-all-done.1.own_ref), channel_id=1, source_target_pairs={{0,32},{32,64},{64,96},{96,128},{128,160},{160,192},{192,224},{224... | collective-permute-start | bytes 884744 | tf_op jit(solution)/shard_map/ppermute | solution.py:25
  73.2 27.5 %collective-permute-start.1 = (bf16[4,144,256]{2,1,0:T(8,128)(2,1)S(1)}, bf16[4,144,256]{2,1,0:T(8,128)(2,1)S(1)}, u32[]{:S(2)}, u32[]{:S(2)}) collective-permute-start(bf16[4,144,256]{2,1,0:T(8,128)(2,1)S(1)} %all-to-all-done.1.own_ref), channel_id=1, source_target_pairs={{0,480},{32,0},{64,32},{96,64},{128,96},{160,128},{192,160},{224,1... | collective-permute-start | bytes 884744 | tf_op jit(solution)/shard_map/ppermute | solution.py:25
  78.8 21.6 %collective-permute-start.3 = (bf16[2,144,256]{2,1,0:T(8,128)(2,1)}, bf16[2,144,256]{2,1,0:T(8,128)(2,1)S(1)}, u32[]{:S(2)}, u32[]{:S(2)}) collective-permute-start(bf16[2,144,256]{2,1,0:T(8,128)(2,1)} %get-tuple-element.11), channel_id=1, source_target_pairs={{0,64},{32,96},{64,128},{96,160},{128,192},{160,224},{192,256},{22... | collective-permute-start | bytes 442376 | tf_op jit(solution)/shard_map/ppermute | solution.py:25
  80.8 19.9 %collective-permute-start.2 = (bf16[2,144,256]{2,1,0:T(8,128)(2,1)}, bf16[2,144,256]{2,1,0:T(8,128)(2,1)}, u32[]{:S(2)}, u32[]{:S(2)}) collective-permute-start(bf16[2,144,256]{2,1,0:T(8,128)(2,1)} %get-tuple-element.12), channel_id=1, source_target_pairs={{0,448},{32,480},{64,0},{96,32},{128,64},{160,96},{192,128},{224,1... | collective-permute-start | bytes 442376 | tf_op jit(solution)/shard_map/ppermute | solution.py:25
  90.7 29.9 %all-to-all-start.3 = ((bf16[4,528,256]{2,1,0:T(8,128)(2,1)}), bf16[4,528,256]{2,1,0:T(8,128)(2,1)}, u32[]{:S(2)}, u32[]{:S(2)}) async-start(bf16[4,528,256]{2,1,0:T(8,128)(2,1)} %broadcast_in_dim.5), calls=%async_computation.3 | async-start | bytes 2162688 | tf_op jit(solution)/shard_map/all_to_all | solution.py:29
  120.6 30.3 %copy-start.15 = (f32[3,2,704]{2,1,0:T(2,128)S(1)}, f32[3,2,704]{2,1,0:T(2,128)}, u32[]{:S(2)}) copy-start(f32[3,2,704]{2,1,0:T(2,128)} %param.18) | copy-start | bytes 50692
  120.6 32.0 %copy-start.7 = (f32[2048]{0:T(1024)S(1)}, f32[2048]{0:T(1024)}, u32[]{:S(2)}) copy-start(f32[2048]{0:T(1024)} %param.15) | copy-start | bytes 24580
  120.6 14.4 %all-to-all-start.2 = ((bf16[4,576,128]{2,1,0:T(8,128)(2,1)}), bf16[4,576,128]{2,1,0:T(8,128)(2,1)S(1)}, u32[]{:S(2)}, u32[]{:S(2)}) async-start(bf16[4,576,128]{2,1,0:T(8,128)(2,1)} %attend.1), calls=%async_computation.2 | async-start | bytes 1179648 | tf_op jit(solution)/shard_map/all_to_all | solution.py:29
  125.5 25.5 %collective-permute-start.11 = (bf16[4,528,256]{2,1,0:T(8,128)(2,1)}, bf16[4,528,256]{2,1,0:T(8,128)(2,1)}, u32[]{:S(2)}, u32[]{:S(2)}) collective-permute-start(bf16[4,528,256]{2,1,0:T(8,128)(2,1)} %all-to-all-done.3.resid_own), channel_id=1, source_target_pairs={{0,1},{1,0},{2,3},{3,2},{4,5},{5,4},{6,7},{7,6},{8,9},{9,8},{10,11... | collective-permute-start | bytes 3244040 | tf_op jit(solution)/shard_map/ppermute | solution.py:25
  148.7 3.8 %collective-permute-start.5 = (bf16[4,528,128]{2,1,0:T(8,128)(2,1)S(1)}, bf16[4,528,128]{2,1,0:T(8,128)(2,1)S(1)}, u32[]{:S(2)}, u32[]{:S(2)}) collective-permute-start(bf16[4,528,128]{2,1,0:T(8,128)(2,1)S(1)} %bitcast.16), channel_id=1, source_target_pairs={{0,1},{1,0},{2,3},{3,2},{4,5},{5,4},{6,7},{7,6},{8,9},{9,8},{10,11... | collective-permute-start | bytes 1622024 | tf_op jit(solution)/shard_map/ppermute | solution.py:25
  165.2 4.6 %collective-permute-start.12 = (bf16[2,4,256,256]{3,2,1,0:T(8,128)(2,1)S(1)}, bf16[2,4,256,256]{3,2,1,0:T(8,128)(2,1)S(1)}, u32[]{:S(2)}, u32[]{:S(2)}) collective-permute-start(bf16[2,4,256,256]{3,2,1,0:T(8,128)(2,1)S(1)} %get-tuple-element.10), channel_id=1, source_target_pairs={{0,1},{1,0},{2,3},{3,2},{4,5},{5,4},{6,7},{7,6},{8,9},{9,8},{10,11... | collective-permute-start | bytes 3145736 | tf_op jit(solution)/shard_map/ppermute | solution.py:25
  (12 other events, 48.4 us)
Sparse Core Ops, SparseCore 0:
  20.7 93.3 all-gather.3
where the time goes:
time: 198 us; the launch traced here: 197 us
  starting transfers between devices  62 us (31%)
  blocking collectives  43.8 us (22%)
  Pallas kernels  31.8 us (16%)
  waiting for transfers between devices  29.2 us (15%)
  between operations  13.7 us (7%)
  local copies, waits for them, and re-layouts  11.9 us (6%)
  other arithmetic  4.5 us (2%)
    ppermute x13, starting transfers between devices, shifted(): lax.ppermute(value, axis, [(i, (i + by) % size) for i in range(size)])  39.2 us
    all_to_all x2, blocking collectives, exchanged(): return lax.all_to_all(value, axis, 0, 0, tiled=True)  30.7 us
    all_to_all x4, starting transfers between devices, exchanged(): return lax.all_to_all(value, axis, 0, 0, tiled=True)  22.8 us
    ppermute x13, waiting for transfers between devices, shifted(): lax.ppermute(value, axis, [(i, (i + by) % size) for i in range(size)])  21.5 us
    pallas_call x1, Pallas kernels, attend(): pl.pallas_call(functools.partial(attend_kernel, rows=rows, block=416), ou...  19.9 us
    all_gather x1, blocking collectives, layer(): attn = lax.all_gather(attn, 'x', axis=0, tiled=False)  13.1 us
    pallas_call x1, Pallas kernels, feed(): pl.pallas_call(feed_kernel, out_shape=(half, half, jax.ShapeDtypeStruct((...  10.3 us
    all_to_all x4, waiting for transfers between devices, exchanged(): return lax.all_to_all(value, axis, 0, 0, tiled=True)  7.62 us
  transfers between devices with their start and end apart: 18, of which 8 were waited for; matrix products, arithmetic and copies ran while one was open for 4% of the time, Pallas kernels for 11%

commit v1 on v0

--- a/solution.py
+++ b/solution.py
@@ -202,7 +202,7 @@
     )(pieces)
 
 
-def feed_kernel(at_ref, attn_own, attn_other, out_own, out_other, resid_own, resid_other, gain_ref, conv_ref, w_ref,
+def feed_kernel(at_ref, attn_own, attn_other, wide_own, wide_other, gain_ref, conv_ref, w_ref,
                 keep_ref, send_ref, mid_out_ref, af, mid, normed, wg, wu, wd, sems):
     copies = []
     for k, dst in enumerate((wg, wu, wd)):
@@ -213,17 +213,17 @@
     block = at_ref[5]
     rows = HALO + 512
     at_x = block // 2
-    sides = ((core, attn_own, out_own, resid_own, keep_ref), (1 - core, attn_other, out_other, resid_other, send_ref))
-    for c, attn, _, _, _ in sides:
+    sides = ((core, attn_own, wide_own, keep_ref), (1 - core, attn_other, wide_other, send_ref))
+    for c, attn, _, _ in sides:
         for x in range(4):
             af[:, pl.ds(pl.multiple_of(128 * (2 * x + c), 128), 128)] = attn[x]
     a = af[...]
     square = jnp.zeros((rows, 1), F32)
-    for c, _, out, resid, _ in sides:
+    for c, _, wide, _ in sides:
         for i, back in enumerate((0, 1, 3, 2)):
             x = jnp.where(at_x >= back, at_x - back, at_x - back + 4)
-            branch = jnp.dot(a, out[i], preferred_element_type=F32)
-            m = (branch + resid[x].astype(F32)).astype(BF16)
+            branch = jnp.dot(a, wide[i, 0:1024, :], preferred_element_type=F32)
+            m = (branch + wide[i, 1024:1024 + rows, :].astype(F32)).astype(BF16)
             mid[:, pl.ds(pl.multiple_of(256 * (2 * x + c), 256), 256)] = m
             m = m.astype(F32)
             square = square + jnp.sum(m * m, axis=1, keepdims=True)
@@ -250,7 +250,7 @@
     up = mixed(wu, 1)
     hidden = (gate / (1.0 + jnp.exp(-gate)) * up).astype(BF16)
     copies[2].wait()
-    for c, _, _, _, part_ref in sides:
+    for c, _, _, part_ref in sides:
         for x in range(4):
             down = wd[pl.ds(2 * (2 * x + c), 2)].reshape(256, 352)
             part = lax.dot_general(hidden, down, (((1,), (1,)), ((), ())), preferred_element_type=F32).astype(BF16)
@@ -258,7 +258,7 @@
                 part_ref[p, x] = part[256 * p:256 * (p + 1)]
 
 
-def feed(at, attn, other_attn, out, other_out, resid, other_resid, gain, conv, weights):
+def feed(at, attn, other_attn, wide, other_wide, gain, conv, weights):
     smem = pl.BlockSpec(memory_space=pltpu.SMEM)
     vmem = pl.BlockSpec(memory_space=pltpu.VMEM)
     rows = HALO + 512
@@ -266,7 +266,7 @@
     return pl.pallas_call(
         feed_kernel,
         out_shape=(half, half, jax.ShapeDtypeStruct((256, 256), BF16)),
-        in_specs=[smem] + [vmem] * 8 + [pl.BlockSpec(memory_space=pltpu.HBM)],
+        in_specs=[smem] + [vmem] * 6 + [pl.BlockSpec(memory_space=pltpu.HBM)],
         out_specs=(vmem, vmem, vmem),
         scratch_shapes=[
             pltpu.VMEM((rows, 1024), BF16),
@@ -277,44 +277,47 @@
             pltpu.VMEM((16, 4, 32, 352), BF16),
             pltpu.SemaphoreType.DMA((3,)),
         ],
-        compiler_params=pltpu.CompilerParams(vmem_limit_bytes=40 * 2**20),
+        compiler_params=pltpu.CompilerParams(vmem_limit_bytes=50 * 2**20),
         cost_estimate=pl.CostEstimate(flops=5 * 10**9, bytes_accessed=2**24, transcendentals=2 * 10**5),
         name="feed",
-    )(at, attn, other_attn, out, other_out, resid, other_resid, gain, conv, weights)
-
-
-def keys_kernel(kv_ref, gate_ref, out_ref):
+    )(at, attn, other_attn, wide, other_wide, gain, conv, weights)
+
+
+def prepare_kernel(kv_ref, decay_ref, gate_ref, up_ref, down_ref, q_ref, resid_ref, keys_ref, halves_ref, tail_ref):
     turned = kv_ref[0].astype(F32).T.astype(BF16)
     row = lax.broadcasted_iota(jnp.int32, (16, 256), 0)
-    value = jnp.where(row < 3, gate_ref[0:1, :], gate_ref[1:2, :])
+    value = jnp.where(row < 3, decay_ref[0:1, :], decay_ref[1:2, :])
     which = jnp.where(row < 3, row, row - 3)
     high, middle, low = split3(value)
     pick = jnp.where(which == 0, high.astype(F32), jnp.where(which == 1, middle.astype(F32), low.astype(F32)))
     gates = jnp.where(row < 6, pick, 0.0).astype(BF16)
     for i in range(4):
-        out_ref[i, 0:64, :] = turned[0:64]
-        out_ref[i, 64:80, :] = gates
-        out_ref[i, 80:144, :] = turned[64:128]
-
-
-def halves_kernel(gate_ref, up_ref, down_ref, out_ref):
+        keys_ref[i, 0:64, :] = turned[0:64]
+        keys_ref[i, 64:80, :] = gates
+        keys_ref[i, 80:144, :] = turned[64:128]
     for k, ref in enumerate((gate_ref, up_ref, down_ref)):
         value = ref[...].astype(F32)
         for p in range(2):
             piece = value[:, 352 * p:352 * (p + 1)].astype(BF16)
             for i in range(2):
-                out_ref[2 * i + p, k] = piece
-
-
-def small_call(kernel, shape, *operands):
+                halves_ref[2 * i + p, k] = piece
+    tail_ref[:, 0:128] = q_ref[256 - HALO:256, :]
+    tail_ref[:, 128:384] = resid_ref[256 - HALO:256, :]
+
+
+def prepare(*operands):
     vmem = pl.BlockSpec(memory_space=pltpu.VMEM)
     return pl.pallas_call(
-        kernel,
-        out_shape=jax.ShapeDtypeStruct(shape, BF16),
+        prepare_kernel,
+        out_shape=(
+            jax.ShapeDtypeStruct((4, 144, 256), BF16),
+            jax.ShapeDtypeStruct((4, 3, 32, 352), BF16),
+            jax.ShapeDtypeStruct((HALO, 384), BF16),
+        ),
         in_specs=[vmem] * len(operands),
-        out_specs=vmem,
-        compiler_params=pltpu.CompilerParams(vmem_limit_bytes=8 * 2**20),
+        out_specs=(vmem, vmem, vmem),
         cost_estimate=pl.CostEstimate(flops=10**7, bytes_accessed=2**20, transcendentals=0),
+        name="prepare",
     )(*operands)
 
 
@@ -324,36 +327,35 @@
     is_first = (lax.axis_index(SP) < 2).astype(jnp.int32)
     at = jnp.stack([zh, zl, y, is_first, half, lax.axis_index(TP), lax.axis_index("c")]).astype(jnp.int32)
 
-    own = exchanged(small_call(keys_kernel, (4, 144, 256), keys_values, cum_gate), "zh")
-    rows_y = exchanged(small_call(halves_kernel, (4, 3, 32, 352), gate_weight, up_weight, down_weight.T), Y)
+    keys, halves, tail = prepare(
+        keys_values, cum_gate, gate_weight, up_weight, down_weight.T, queries, resid
+    )
+    before = shifted(tail, SP, 1)
+    rows_y = exchanged(halves, Y)
     weights = lax.all_gather(rows_y, Z, axis=0, tiled=False)
-    tail = jnp.concatenate([queries[-HALO:], resid[-HALO:]], axis=1)
-    before = shifted(tail, SP, 1)
-    out = jnp.stack([out_weight] + [shifted(out_weight, "x", by) for by in (1, 3, 2)])
-    other_out = shifted(out, "c", 1)
-    group_q = spread(jnp.concatenate([before[:, :128], queries], axis=0), Y)
+    mine = jnp.concatenate([before[:, 128:], resid], axis=0)
+    theirs = shifted(mine, "yl", 1)
+    own = exchanged(keys, "zh")
+    low = jnp.concatenate([out_weight, mine, theirs[HALO:]], axis=0)
+    high = jnp.concatenate([out_weight, theirs, mine[HALO:]], axis=0)
+    wide = jnp.where(half == 0, low, high)
+    wides = [wide] + [shifted(wide, "x", by) for by in (1, 3, 2)]
     last = shifted(own, Z, 1)
     nxt = shifted(own, Z, -1)
     far_a = shifted(own[:2], Z, -2)
     far_b = shifted(own[2:], Z, 2)
-    mine = jnp.concatenate([before[:, 128:], resid], axis=0)
-    theirs = shifted(mine, "yl", 1)
-    pair = jnp.where(
-        half == 0,
-        jnp.concatenate([mine, theirs[HALO:]], axis=0),
-        jnp.concatenate([theirs, mine[HALO:]], axis=0),
-    )
-    pair = spread(pair, "x")
-    other_pair = shifted(pair, "c", 1)
+    group_q = spread(jnp.concatenate([before[:, :128], queries], axis=0), Y)
 
     partial = attend(at, cum_gate[:, 0], group_q, own, nxt, far_a, far_b, last)
     partial = exchanged(partial, Y)
+    wide = jnp.stack(wides)
+    other_wide = shifted(wide, "c", 1)
     attn = merge(partial)
     attn = lax.all_gather(attn, "x", axis=0, tiled=False)
     other_attn = shifted(attn, "c", 1)
     conv = lax.dynamic_slice_in_dim(conv_kernel.reshape(6, 704), half * 352, 352, 1)
     keep, send, middle = feed(
-        at, attn, other_attn, out, other_out, pair, other_pair, norm_gain.reshape(1, 2048), conv, weights
+        at, attn, other_attn, wide, other_wide, norm_gain.reshape(1, 2048), conv, weights
     )
     got = shifted(send, "c", 1)
     chip = (keep.astype(F32) + got.astype(F32)).astype(BF16).reshape(8, 256, 256)

time: 198 us -> 207 us (1.045)
  the two profiles are of different devices: /device:TPU:384 before, /device:TPU:416 now
where the time goes in v1:
time: 207 us; the launch traced here: 206 us
  blocking collectives  58.3 us (28%)
  starting transfers between devices  48.8 us (24%)
  waiting for transfers between devices  44.3 us (21%)
  Pallas kernels  33.3 us (16%)
  between operations  13.6 us (7%)
  other arithmetic  5.89 us (3%)
    all_to_all x3, blocking collectives, exchanged(): return lax.all_to_all(value, axis, 0, 0, tiled=True)  44.5 us
    ppermute x12, waiting for transfers between devices, shifted(): lax.ppermute(value, axis, [(i, (i + by) % size) for i in range(size)])  44.2 us
    ppermute x12, starting transfers between devices, shifted(): lax.ppermute(value, axis, [(i, (i + by) % size) for i in range(size)])  35.1 us
    pallas_call x1, Pallas kernels, attend(): pl.pallas_call(functools.partial(attend_kernel, rows=rows, block=416), ou...  18.5 us
    all_gather x1, blocking collectives, layer(): attn = lax.all_gather(attn, 'x', axis=0, tiled=False)  13.8 us
    all_to_all x2, starting transfers between devices, exchanged(): return lax.all_to_all(value, axis, 0, 0, tiled=True)  13.6 us
    pallas_call x1, Pallas kernels, feed(): pl.pallas_call(feed_kernel, out_shape=(half, half, jax.ShapeDtypeStruct((...  12.1 us
  transfers between devices with their start and end apart: 15, of which 7 were waited for; matrix products, arithmetic and copies ran while one was open for 3% of the time, Pallas kernels for 9%

profile of v1, /device:TPU:416, one launch (start us, length us, event | category | flops | bytes accessed | tf_op | source)
XLA Modules:
  0.0 205.8 jit_solution(13692135930922755488)
XLA Ops:
  6.5 2.1 %prepare.1 = (bf16[4,144,256]{2,1,0:T(8,128)(2,1)}, bf16[4,3,32,352]{3,2,1,0:T(8,128)(2,1)}, bf16[16,384]{1,0:T(8,128)(2,1)}) custom-call(bf16[1,256,128]{2,1,0:T(8,128)(2,1)} %kv_ref.1, f32[2,256]{1,0:T(2,128)} %decay_ref.1, bf16[32,704]{1,0:T(8,128)(2,1)} %gate_ref.1, bf16[32,704]{1,0:T(8,128)(2,1)} %up_ref.1, bf16[32,704]{1,0:T(8,128)(2,1)} %bitcast.32, ...), custom_call_target="tpu_custom_call" | custom-call | flops 10000000 | bytes 1048576 | tf_op jit(solution)/shard_map/prepare/pallas_call | solution.py:310
  8.6 11.6 %all_to_all.25 = bf16[4,3,32,352]{3,2,1,0:T(8,128)(2,1)} all-to-all(bf16[4,3,32,352]{3,2,1,0:T(8,128)(2,1)} %get-tuple-element.13), channel_id=1, replica_groups=mesh['zh'=4,'zl'=4,'yh'=2,'yl'=2,'x'=4,'c'=2] {'yh','yl'}, dimensions={0} | all-to-all | bytes 540672 | tf_op jit(solution)/shard_map/all_to_all | solution.py:29
  20.2 2.5 %collective-permute-start = (bf16[16,384]{1,0:T(8,128)(2,1)}, bf16[16,384]{1,0:T(8,128)(2,1)S(1)}, u32[]{:S(2)}, u32[]{:S(2)}) collective-permute-start(bf16[16,384]{1,0:T(8,128)(2,1)} %get-tuple-element.11), channel_id=1, source_target_pairs={{0,8},{8,16},{16,24},{24,32},{32,40},{40,48},{48,56},{56,64},{64,7... | collective-permute-start | bytes 36872 | tf_op jit(solution)/shard_map/ppermute | solution.py:25
  22.7 5.4 %collective-permute-done = bf16[16,384]{1,0:T(8,128)(2,1)S(1)} collective-permute-done((bf16[16,384]{1,0:T(8,128)(2,1)}, bf16[16,384]{1,0:T(8,128)(2,1)S(1)}, u32[]{:S(2)}, u32[]{:S(2)}) %collective-permute-start) | collective-permute-done | bytes 12320 | tf_op jit(solution)/shard_map/ppermute | solution.py:25
  31.0 5.0 %collective-permute-done.6 = bf16[272,256]{1,0:T(8,128)(2,1)S(1)} collective-permute-done((bf16[272,256]{1,0:T(8,128)(2,1)S(1)}, bf16[272,256]{1,0:T(8,128)(2,1)S(1)}, u32[]{:S(2)}, u32[]{:S(2)}) %collective-permute-start.6) | collective-permute-done | bytes 139296 | tf_op jit(solution)/shard_map/ppermute | solution.py:25
  37.7 4.9 %collective-permute-start.9 = (bf16[1552,256]{1,0:T(8,128)(2,1)}, bf16[1552,256]{1,0:T(8,128)(2,1)S(1)}, u32[]{:S(2)}, u32[]{:S(2)}) collective-permute-start(bf16[1552,256]{1,0:T(8,128)(2,1)} %fusion.2), channel_id=1, source_target_pairs={{0,4},{2,6},{4,0},{6,2},{1,5},{3,7},{5,1},{7,3},{8,12},{10,14},{12... | collective-permute-start | bytes 2383880 | tf_op jit(solution)/shard_map/ppermute | solution.py:25
  42.6 3.0 %collective-permute-start.8 = (bf16[1552,256]{1,0:T(8,128)(2,1)}, bf16[1552,256]{1,0:T(8,128)(2,1)S(1)}, u32[]{:S(2)}, u32[]{:S(2)}) collective-permute-start(bf16[1552,256]{1,0:T(8,128)(2,1)} %fusion.2), channel_id=1, source_target_pairs={{0,6},{2,0},{4,2},{6,4},{1,7},{3,1},{5,3},{7,5},{8,14},{10,8},{12,... | collective-permute-start | bytes 2383880 | tf_op jit(solution)/shard_map/ppermute | solution.py:25
  45.7 2.8 %collective-permute-start.7 = (bf16[1552,256]{1,0:T(8,128)(2,1)}, bf16[1552,256]{1,0:T(8,128)(2,1)S(1)}, u32[]{:S(2)}, u32[]{:S(2)}) collective-permute-start(bf16[1552,256]{1,0:T(8,128)(2,1)} %fusion.2), channel_id=1, source_target_pairs={{0,2},{2,4},{4,6},{6,0},{1,3},{3,5},{5,7},{7,1},{8,10},{10,12},{12... | collective-permute-start | bytes 2383880 | tf_op jit(solution)/shard_map/ppermute | solution.py:25
  48.5 10.2 %all-to-all-start.1 = ((bf16[4,144,256]{2,1,0:T(8,128)(2,1)}), bf16[4,144,256]{2,1,0:T(8,128)(2,1)S(1)}, u32[]{:S(2)}, u32[]{:S(2)}) async-start(bf16[4,144,256]{2,1,0:T(8,128)(2,1)} %get-tuple-element.12), calls=%async_computation.1 | async-start | bytes 589824 | tf_op jit(solution)/shard_map/all_to_all | solution.py:29
  59.7 2.2 %collective-permute-done.9 = bf16[1552,256]{1,0:T(8,128)(2,1)S(1)} collective-permute-done((bf16[1552,256]{1,0:T(8,128)(2,1)}, bf16[1552,256]{1,0:T(8,128)(2,1)S(1)}, u32[]{:S(2)}, u32[]{:S(2)}) %collective-permute-start.9) | collective-permute-done | bytes 794656 | tf_op jit(solution)/shard_map/ppermute | solution.py:25
  61.9 12.3 %collective-permute-done.8 = bf16[1552,256]{1,0:T(8,128)(2,1)S(1)} collective-permute-done((bf16[1552,256]{1,0:T(8,128)(2,1)}, bf16[1552,256]{1,0:T(8,128)(2,1)S(1)}, u32[]{:S(2)}, u32[]{:S(2)}) %collective-permute-start.8) | collective-permute-done | bytes 794656 | tf_op jit(solution)/shard_map/ppermute | solution.py:25
  76.1 2.0 collective-permute-start.10
  78.9 3.4 %all-to-all-start = ((bf16[4,272,128]{2,1,0:T(8,128)(2,1)}), bf16[4,272,128]{2,1,0:T(8,128)(2,1)S(1)}, u32[]{:S(2)}, u32[]{:S(2)}) async-start(bf16[4,272,128]{2,1,0:T(8,128)(2,1)} %broadcast_in_dim.2), calls=%async_computation | async-start | bytes 557056 | tf_op jit(solution)/shard_map/all_to_all | solution.py:29
  82.3 2.9 %collective-permute-start.4 = (bf16[4,144,256]{2,1,0:T(8,128)(2,1)S(1)}, bf16[4,144,256]{2,1,0:T(8,128)(2,1)S(1)}, u32[]{:S(2)}, u32[]{:S(2)}) collective-permute-start(bf16[4,144,256]{2,1,0:T(8,128)(2,1)S(1)} %all-to-all-done.1.own_ref), channel_id=1, source_target_pairs={{0,32},{32,64},{64,96},{96,128},{128,160},{160,192},{192,224},{224... | collective-permute-start | bytes 884744 | tf_op jit(solution)/shard_map/ppermute | solution.py:25
  85.3 3.1 %collective-permute-start.1 = (bf16[4,144,256]{2,1,0:T(8,128)(2,1)S(1)}, bf16[4,144,256]{2,1,0:T(8,128)(2,1)S(1)}, u32[]{:S(2)}, u32[]{:S(2)}) collective-permute-start(bf16[4,144,256]{2,1,0:T(8,128)(2,1)S(1)} %all-to-all-done.1.own_ref), channel_id=1, source_target_pairs={{0,480},{32,0},{64,32},{96,64},{128,96},{160,128},{192,160},{224,1... | collective-permute-start | bytes 884744 | tf_op jit(solution)/shard_map/ppermute | solution.py:25
  88.4 4.5 %collective-permute-start.3 = (bf16[2,144,256]{2,1,0:T(8,128)(2,1)S(1)}, bf16[2,144,256]{2,1,0:T(8,128)(2,1)S(1)}, u32[]{:S(2)}, u32[]{:S(2)}) collective-permute-start(bf16[2,144,256]{2,1,0:T(8,128)(2,1)S(1)} %get-tuple-element.17), channel_id=1, source_target_pairs={{0,64},{32,96},{64,128},{96,160},{128,192},{160,224},{192,256},{22... | collective-permute-start | bytes 442376 | tf_op jit(solution)/shard_map/ppermute | solution.py:25
  92.9 3.5 %collective-permute-start.2 = (bf16[2,144,256]{2,1,0:T(8,128)(2,1)S(1)}, bf16[2,144,256]{2,1,0:T(8,128)(2,1)S(1)}, u32[]{:S(2)}, u32[]{:S(2)}) collective-permute-start(bf16[2,144,256]{2,1,0:T(8,128)(2,1)S(1)} %get-tuple-element.18), channel_id=1, source_target_pairs={{0,448},{32,480},{64,0},{96,32},{128,64},{160,96},{192,128},{224,1... | collective-permute-start | bytes 442376 | tf_op jit(solution)/shard_map/ppermute | solution.py:25
  96.6 15.0 %collective-permute-done.3.far_b_ref = bf16[2,144,256]{2,1,0:T(8,128)(2,1)S(1)} collective-permute-done((bf16[2,144,256]{2,1,0:T(8,128)(2,1)S(1)}, bf16[2,144,256]{2,1,0:T(8,128)(2,1)S(1)}, u32[]{:S(2)}, u32[]{:S(2)}) %collective-permute-start.3) | collective-permute-done | bytes 147488 | tf_op jit(solution)/shard_map/ppermute | solution.py:25
  111.6 18.5 %attend.1 = bf16[4,576,128]{2,1,0:T(8,128)(2,1)S(1)} custom-call(s32[7]{0:T(128)S(1)} %stack.48.at_ref, f32[2]{0:T(128)S(1)} %slice_reduce_fusion.gate_ref, bf16[4,272,128]{2,1,0:T(8,128)(2,1)S(1)} %all-to-all-done.q_ref, bf16[4,144,256]{2,1,0:T(8,128)(2,1)S(1)} %all-to-all-done.1.own_ref, bf16[4,144,256]{2,1,0:T(8,128)(2,1)S(1)} %collective-permute-done.1.next_ref, ...), custom_call_target="tpu_custom_call" | custom-call | flops 8000000000 | bytes 4194304 | tf_op jit(solution)/shard_map/attend/pallas_call | solution.py:148
  130.1 14.1 %all_to_all.26.in_ref = bf16[4,576,128]{2,1,0:T(8,128)(2,1)S(1)} all-to-all(bf16[4,576,128]{2,1,0:T(8,128)(2,1)S(1)} %attend.1), channel_id=1, replica_groups=mesh['zh'=4,'zl'=4,'yh'=2,'yl'=2,'x'=4,'c'=2] {'yh','yl'}, dimensions={0} | all-to-all | bytes 1179648 | tf_op jit(solution)/shard_map/all_to_all | solution.py:29
  144.8 13.8 %all-gather = bf16[2112,128]{1,0:T(8,128)(2,1)S(1)} all-gather(bf16[528,128]{1,0:T(8,128)(2,1)S(1)} %merge.1), channel_id=2, replica_groups=mesh['zh'=4,'zl'=4,'yh'=2,'yl'=2,'x'=4,'c'=2] {'x'}, dimensions={0}, use_global_device_ids=true | all-gather | bytes 675840 | tf_op jit(solution)/shard_map/all_gather | solution.py:354
  162.4 12.1 %feed.1 = (bf16[2,4,256,256]{3,2,1,0:T(8,128)(2,1)S(1)}, bf16[2,4,256,256]{3,2,1,0:T(8,128)(2,1)S(1)}, bf16[256,256]{1,0:T(8,128)(2,1)S(1)}) custom-call(s32[7]{0:T(128)S(1)} %stack.48.at_ref, bf16[4,528,128]{2,1,0:T(8,128)(2,1)S(1)} %bitcast.23, bf16[4,528,128]{2,1,0:T(8,128)(2,1)S(1)} %collective-permute-done.5.attn_other, ...), custom_call_target="tpu_custom_call" | custom-call | flops 5000000000 | bytes 16777216 | tf_op jit(solution)/shard_map/feed/pallas_call | solution.py:266
  176.6 2.5 %collective-permute-done.11 = bf16[2,4,256,256]{3,2,1,0:T(8,128)(2,1)S(1)} collective-permute-done((bf16[2,4,256,256]{3,2,1,0:T(8,128)(2,1)S(1)}, bf16[2,4,256,256]{3,2,1,0:T(8,128)(2,1)S(1)}, u32[]{:S(2)}, u32[]{:S(2)}) %collective-permute-start.11) | collective-permute-done | bytes 1048608 | tf_op jit(solution)/shard_map/ppermute | solution.py:25
  179.3 18.8 %all_to_all.27 = bf16[8,256,256]{2,1,0:T(8,128)(2,1)S(1)} all-to-all(bf16[8,256,256]{2,1,0:T(8,128)(2,1)S(1)} %bitcast.25), channel_id=1, replica_groups=mesh['zh'=4,'zl'=4,'yh'=2,'yl'=2,'x'=4,'c'=2] {'yl','x'}, dimensions={0} | all-to-all | bytes 2097152 | tf_op jit(solution)/shard_map/all_to_all | solution.py:29
  (44 shorter events, 16.0 us)
Async XLA Ops:
  6.5 30.1 %copy-start.1 = (bf16[256,256]{1,0:T(8,128)(2,1)S(1)}, bf16[256,256]{1,0:T(8,128)(2,1)}, u32[]{:S(2)}) copy-start(bf16[256,256]{1,0:T(8,128)(2,1)} %resid_ref.1) | copy-start | bytes 393220
  6.5 30.1 %copy-start.2 = (bf16[1024,256]{1,0:T(8,128)(2,1)S(1)}, bf16[1024,256]{1,0:T(8,128)(2,1)}, u32[]{:S(2)}) copy-start(bf16[1024,256]{1,0:T(8,128)(2,1)} %param.14) | copy-start | bytes 1572868
  6.5 155.9 %all-gather.4.cloned.1.call-start = ((), (), s32[]{:S(2)}) async-start(), calls=%async_computation.5 | async-start | bytes 5013504 | tf_op jit(solution)/shard_map/all_gather | solution.py:335
  20.2 7.9 %collective-permute-start = (bf16[16,384]{1,0:T(8,128)(2,1)}, bf16[16,384]{1,0:T(8,128)(2,1)S(1)}, u32[]{:S(2)}, u32[]{:S(2)}) collective-permute-start(bf16[16,384]{1,0:T(8,128)(2,1)} %get-tuple-element.11), channel_id=1, source_target_pairs={{0,8},{8,16},{16,24},{24,32},{32,40},{40,48},{48,56},{56,64},{64,7... | collective-permute-start | bytes 36872 | tf_op jit(solution)/shard_map/ppermute | solution.py:25
  29.0 6.9 %collective-permute-start.6 = (bf16[272,256]{1,0:T(8,128)(2,1)S(1)}, bf16[272,256]{1,0:T(8,128)(2,1)S(1)}, u32[]{:S(2)}, u32[]{:S(2)}) collective-permute-start(bf16[272,256]{1,0:T(8,128)(2,1)S(1)} %pad_maximum_fusion.5), channel_id=1, source_target_pairs={{0,8},{8,0},{1,9},{9,1},{2,10},{10,2},{3,11},{11,3},{4,12},{12,4},... | collective-permute-start | bytes 417800 | tf_op jit(solution)/shard_map/ppermute | solution.py:25
  37.7 24.2 %collective-permute-start.9 = (bf16[1552,256]{1,0:T(8,128)(2,1)}, bf16[1552,256]{1,0:T(8,128)(2,1)S(1)}, u32[]{:S(2)}, u32[]{:S(2)}) collective-permute-start(bf16[1552,256]{1,0:T(8,128)(2,1)} %fusion.2), channel_id=1, source_target_pairs={{0,4},{2,6},{4,0},{6,2},{1,5},{3,7},{5,1},{7,3},{8,12},{10,14},{12... | collective-permute-start | bytes 2383880 | tf_op jit(solution)/shard_map/ppermute | solution.py:25
  42.6 31.6 %collective-permute-start.8 = (bf16[1552,256]{1,0:T(8,128)(2,1)}, bf16[1552,256]{1,0:T(8,128)(2,1)S(1)}, u32[]{:S(2)}, u32[]{:S(2)}) collective-permute-start(bf16[1552,256]{1,0:T(8,128)(2,1)} %fusion.2), channel_id=1, source_target_pairs={{0,6},{2,0},{4,2},{6,4},{1,7},{3,1},{5,3},{7,5},{8,14},{10,8},{12,... | collective-permute-start | bytes 2383880 | tf_op jit(solution)/shard_map/ppermute | solution.py:25
  45.7 28.5 %collective-permute-start.7 = (bf16[1552,256]{1,0:T(8,128)(2,1)}, bf16[1552,256]{1,0:T(8,128)(2,1)S(1)}, u32[]{:S(2)}, u32[]{:S(2)}) collective-permute-start(bf16[1552,256]{1,0:T(8,128)(2,1)} %fusion.2), channel_id=1, source_target_pairs={{0,2},{2,4},{4,6},{6,0},{1,3},{3,5},{5,7},{7,1},{8,10},{10,12},{12... | collective-permute-start | bytes 2383880 | tf_op jit(solution)/shard_map/ppermute | solution.py:25
  48.5 29.7 %all-to-all-start.1 = ((bf16[4,144,256]{2,1,0:T(8,128)(2,1)}), bf16[4,144,256]{2,1,0:T(8,128)(2,1)S(1)}, u32[]{:S(2)}, u32[]{:S(2)}) async-start(bf16[4,144,256]{2,1,0:T(8,128)(2,1)} %get-tuple-element.12), calls=%async_computation.1 | async-start | bytes 589824 | tf_op jit(solution)/shard_map/all_to_all | solution.py:29
  74.2 4.0 %copy-start.3 = (bf16[256,128]{1,0:T(8,128)(2,1)S(1)}, bf16[256,128]{1,0:T(8,128)(2,1)}, u32[]{:S(2)}) copy-start(bf16[256,128]{1,0:T(8,128)(2,1)} %q_ref.1) | copy-start | bytes 196612
  76.1 20.4 %copy-start.5 = (f32[2,256]{1,0:T(2,128)S(1)}, f32[2,256]{1,0:T(2,128)}, u32[]{:S(2)}) copy-start(f32[2,256]{1,0:T(2,128)} %decay_ref.1) | copy-start | bytes 6148
  76.1 86.4 %collective-permute-start.10 = (bf16[4,1552,256]{2,1,0:T(8,128)(2,1)}, bf16[4,1552,256]{2,1,0:T(8,128)(2,1)}, u32[]{:S(2)}, u32[]{:S(2)}) collective-permute-start(bf16[4,1552,256]{2,1,0:T(8,128)(2,1)} %pad_maximum_fusion.wide_own), channel_id=1, source_target_pairs={{0,1},{1,0},{2,3},{3,2},{4,5},{5,4},{6,7},{7,6},{8,9},{9,8},{10,11... | collective-permute-start | bytes 9535496 | tf_op jit(solution)/shard_map/ppermute | solution.py:25
  78.9 17.7 %all-to-all-start = ((bf16[4,272,128]{2,1,0:T(8,128)(2,1)}), bf16[4,272,128]{2,1,0:T(8,128)(2,1)S(1)}, u32[]{:S(2)}, u32[]{:S(2)}) async-start(bf16[4,272,128]{2,1,0:T(8,128)(2,1)} %broadcast_in_dim.2), calls=%async_computation | async-start | bytes 557056 | tf_op jit(solution)/shard_map/all_to_all | solution.py:29
  82.3 29.3 %collective-permute-start.4 = (bf16[4,144,256]{2,1,0:T(8,128)(2,1)S(1)}, bf16[4,144,256]{2,1,0:T(8,128)(2,1)S(1)}, u32[]{:S(2)}, u32[]{:S(2)}) collective-permute-start(bf16[4,144,256]{2,1,0:T(8,128)(2,1)S(1)} %all-to-all-done.1.own_ref), channel_id=1, source_target_pairs={{0,32},{32,64},{64,96},{96,128},{128,160},{160,192},{192,224},{224... | collective-permute-start | bytes 884744 | tf_op jit(solution)/shard_map/ppermute | solution.py:25
  85.3 26.3 %collective-permute-start.1 = (bf16[4,144,256]{2,1,0:T(8,128)(2,1)S(1)}, bf16[4,144,256]{2,1,0:T(8,128)(2,1)S(1)}, u32[]{:S(2)}, u32[]{:S(2)}) collective-permute-start(bf16[4,144,256]{2,1,0:T(8,128)(2,1)S(1)} %all-to-all-done.1.own_ref), channel_id=1, source_target_pairs={{0,480},{32,0},{64,32},{96,64},{128,96},{160,128},{192,160},{224,1... | collective-permute-start | bytes 884744 | tf_op jit(solution)/shard_map/ppermute | solution.py:25
  88.4 23.2 %collective-permute-start.3 = (bf16[2,144,256]{2,1,0:T(8,128)(2,1)S(1)}, bf16[2,144,256]{2,1,0:T(8,128)(2,1)S(1)}, u32[]{:S(2)}, u32[]{:S(2)}) collective-permute-start(bf16[2,144,256]{2,1,0:T(8,128)(2,1)S(1)} %get-tuple-element.17), channel_id=1, source_target_pairs={{0,64},{32,96},{64,128},{96,160},{128,192},{160,224},{192,256},{22... | collective-permute-start | bytes 442376 | tf_op jit(solution)/shard_map/ppermute | solution.py:25
  92.9 18.7 %collective-permute-start.2 = (bf16[2,144,256]{2,1,0:T(8,128)(2,1)S(1)}, bf16[2,144,256]{2,1,0:T(8,128)(2,1)S(1)}, u32[]{:S(2)}, u32[]{:S(2)}) collective-permute-start(bf16[2,144,256]{2,1,0:T(8,128)(2,1)S(1)} %get-tuple-element.18), channel_id=1, source_target_pairs={{0,448},{32,480},{64,0},{96,32},{128,64},{160,96},{192,128},{224,1... | collective-permute-start | bytes 442376 | tf_op jit(solution)/shard_map/ppermute | solution.py:25
  130.1 30.5 %copy-start.4 = (f32[3,2,704]{2,1,0:T(2,128)S(1)}, f32[3,2,704]{2,1,0:T(2,128)}, u32[]{:S(2)}) copy-start(f32[3,2,704]{2,1,0:T(2,128)} %param.18) | copy-start | bytes 50692
  130.1 32.4 %copy-start = (f32[2048]{0:T(1024)S(1)}, f32[2048]{0:T(1024)}, u32[]{:S(2)}) copy-start(f32[2048]{0:T(1024)} %param.15) | copy-start | bytes 24580
  158.6 3.8 %collective-permute-start.5 = (bf16[4,528,128]{2,1,0:T(8,128)(2,1)S(1)}, bf16[4,528,128]{2,1,0:T(8,128)(2,1)S(1)}, u32[]{:S(2)}, u32[]{:S(2)}) collective-permute-start(bf16[4,528,128]{2,1,0:T(8,128)(2,1)S(1)} %bitcast.22), channel_id=1, source_target_pairs={{0,1},{1,0},{2,3},{3,2},{4,5},{5,4},{6,7},{7,6},{8,9},{9,8},{10,11... | collective-permute-start | bytes 1622024 | tf_op jit(solution)/shard_map/ppermute | solution.py:25
  174.5 4.6 %collective-permute-start.11 = (bf16[2,4,256,256]{3,2,1,0:T(8,128)(2,1)S(1)}, bf16[2,4,256,256]{3,2,1,0:T(8,128)(2,1)S(1)}, u32[]{:S(2)}, u32[]{:S(2)}) collective-permute-start(bf16[2,4,256,256]{3,2,1,0:T(8,128)(2,1)S(1)} %get-tuple-element.16), channel_id=1, source_target_pairs={{0,1},{1,0},{2,3},{3,2},{4,5},{5,4},{6,7},{7,6},{8,9},{9,8},{10,11... | collective-permute-start | bytes 3145736 | tf_op jit(solution)/shard_map/ppermute | solution.py:25
Sparse Core Ops, SparseCore 0:
  20.3 95.1 all-gather.3

commit v2 on v1

--- a/solution.py
+++ b/solution.py
@@ -42,84 +42,131 @@
     return high, middle, low
 
 
-def attend_kernel(at_ref, gate_ref, q_ref, own_ref, next_ref, far_a_ref, far_b_ref, last_ref,
-                  out_ref, qa, ka, va, norm_out, lse_rows, lse_dense, *, rows, block):
+def put_keys(ka, va, chunk, d, piece, gate_ref):
+    cols = pl.ds(256 * d, 256)
+    row = lax.broadcasted_iota(jnp.int32, (8, 256), 0)
+    ka[chunk, 0:64, cols] = piece[0:64, :]
+    g = piece[64:72, :].astype(F32)
+    bias = []
+    for head in range(2):
+        total = g[3 * head:3 * head + 1, :] + g[3 * head + 1:3 * head + 2, :]
+        bias.append(gate_ref[head] - (total + g[3 * head + 2:3 * head + 3, :]))
+    b = jnp.where(row < 3, bias[0], bias[1])
+    which = jnp.where(row < 3, row, row - 3)
+    high, middle, low = split3(b)
+    pick = jnp.where(which == 0, high.astype(F32), jnp.where(which == 1, middle.astype(F32), low.astype(F32)))
+    ka[chunk, 64:72, cols] = jnp.where(row < 6, pick, 0.0).astype(BF16)
+    ka[chunk, 72:128, cols] = jnp.zeros((56, 256), BF16)
+    va[chunk, 0:64, cols] = piece[72:136, :]
+    va[chunk, 64:128, cols] = jnp.ones((64, 256), BF16)
+
+
+def fold_keys(queries, keys, values, state, query_pos, key_pos):
+    scores = []
+    for i, q in enumerate(queries):
+        s = lax.dot_general(q, keys, (((1,), (0,)), ((), ())), preferred_element_type=F32)
+        if key_pos is not None:
+            s = jnp.where(query_pos[i] >= key_pos, s, MASKED)
+        scores.append(s)
+    new_state = []
+    for s, (top, acc) in zip(scores, state):
+        new_top = jnp.maximum(top, jnp.max(s, axis=1, keepdims=True))
+        p = jnp.exp(s - new_top).astype(BF16)
+        more = lax.dot_general(p, values, (((1,), (1,)), ((), ())), preferred_element_type=F32)
+        new_state.append((new_top, acc * jnp.exp(top - new_top) + more))
+    return tuple(new_state)
+
+
+def row_blocks(z):
+    rows, part = HALO + 1024, 416
+    blocks = []
+    for start in range(0, 2 * rows, part):
+        row = start + lax.broadcasted_iota(jnp.int32, (part, 1), 0)
+        blocks.append((start, row >= rows, z * 1024 - HALO + jnp.where(row >= rows, row - rows, row)))
+    return part, blocks
+
+
+def attend_own_kernel(at_ref, gate_ref, q_ref, own_ref, qa, state_ref, ka, va):
     zh, zl, y = at_ref[0], at_ref[1], at_ref[2]
     z = 4 * zh + zl
+    rows = HALO + 1024
     lane = lax.broadcasted_iota(jnp.int32, (1, 128), 1)
-    group = rows - HALO
 
     def put_queries(start, piece):
         x = piece.astype(F32) * 0.125
         for head in range(2):
-            part = x if head == 0 else pltpu.roll(x, 64, 1)
+            side = x if head == 0 else pltpu.roll(x, 64, 1)
             first = 64 + 3 * head
             ones = jnp.where((lane >= first) & (lane < first + 3), 1.0, 0.0)
-            both = jnp.where(lane < 64, part, ones)
-            qa[pl.ds(head * rows + start, piece.shape[0]), :] = both.astype(BF16)
+            both = jnp.where(lane < 64, side, ones)
+            qa[head * rows + start:head * rows + start + piece.shape[0], :] = both.astype(BF16)
 
     put_queries(0, q_ref[0, 0:HALO, :])
     for i in range(4):
         put_queries(HALO + 256 * i, q_ref[i, HALO:HALO + 256, :])
-
-    part_row = lax.broadcasted_iota(jnp.int32, (16, 256), 0)
-
-    def put_keys(chunk, d, piece):
-        cols = pl.ds(256 * d, 256)
-        ka[chunk, 0:64, cols] = piece[0:64, :]
-        g = piece[64:80, :].astype(F32)
-        bias = []
-        for head in range(2):
-            total = g[3 * head:3 * head + 1, :] + g[3 * head + 1:3 * head + 2, :]
-            bias.append(gate_ref[head] - (total + g[3 * head + 2:3 * head + 3, :]))
-        b = jnp.where(part_row < 3, bias[0], bias[1])
-        which = jnp.where(part_row < 3, part_row, part_row - 3)
-        high, middle, low = split3(b)
-        pick = jnp.where(which == 0, high.astype(F32), jnp.where(which == 1, middle.astype(F32), low.astype(F32)))
-        ka[chunk, 64:80, cols] = jnp.where(part_row < 6, pick, 0.0).astype(BF16)
-        ka[chunk, 80:128, cols] = jnp.zeros((48, 256), BF16)
-        va[chunk, 0:64, cols] = piece[80:144, :]
-        va[chunk, 64:128, cols] = jnp.ones((64, 256), BF16)
-
+    for chunk in range(4):
+        put_keys(ka, va, 0, chunk, own_ref[chunk], gate_ref)
+    key_lane = lax.broadcasted_iota(jnp.int32, (1, 1024), 1)
+    key_chunk = key_lane // 256
+    key_pos = (4 * key_chunk + zl) * 1024 + y * 256 + (key_lane - 256 * key_chunk)
+    part, blocks = row_blocks(z)
+    state = tuple((jnp.full((part, 1), MASKED, F32), jnp.zeros((part, 128), F32)) for _ in blocks)
+    queries = [qa[start:start + part, :] for start, _, _ in blocks]
+    state = fold_keys(queries, ka[0], va[0], state, [pos for _, _, pos in blocks], key_pos)
+    for (start, _, _), (top, acc) in zip(blocks, state):
+        state_ref[start:start + part, :] = jnp.where(lane < 96, acc, top)
+
+
+def attend_own(at, gate, queries, own):
+    rows = HALO + 1024
+    smem = pl.BlockSpec(memory_space=pltpu.SMEM)
+    vmem = pl.BlockSpec(memory_space=pltpu.VMEM)
+    return pl.pallas_call(
+        attend_own_kernel,
+        out_shape=(jax.ShapeDtypeStruct((2 * rows, 128), BF16), jax.ShapeDtypeStruct((2 * rows, 128), F32)),
+        in_specs=[smem, smem, vmem, vmem],
+        out_specs=(vmem, vmem),
+        scratch_shapes=[pltpu.VMEM((1, 128, 1024), BF16), pltpu.VMEM((1, 128, 1024), BF16)],
+        compiler_params=pltpu.CompilerParams(vmem_limit_bytes=30 * 2**20),
+        cost_estimate=pl.CostEstimate(flops=2 * 10**9, bytes_accessed=2**20, transcendentals=2 * 10**6),
+        name="attend_own",
+    )(at, gate, queries, own)
+
+
+def attend_rest_kernel(at_ref, gate_ref, qa, state_ref, next_ref, far_a_ref, far_b_ref, last_ref,
+                       out_ref, ka, va, norm_out, lse_rows, lse_dense):
+    zh, zl, y = at_ref[0], at_ref[1], at_ref[2]
+    z = 4 * zh + zl
+    rows = HALO + 1024
+    lane = lax.broadcasted_iota(jnp.int32, (1, 128), 1)
     for chunk in range(4):
         far = far_a_ref[chunk] if chunk < 2 else far_b_ref[chunk - 2]
-        pieces = (own_ref[chunk], next_ref[chunk], far, last_ref[chunk])
-        for d in range(4):
-            put_keys(chunk, d, pieces[d])
-
-    key_lane = lax.broadcasted_iota(jnp.int32, (1, 1024), 1)
+        for d, piece in enumerate((next_ref[chunk], far, last_ref[chunk])):
+            put_keys(ka, va, chunk, d, piece, gate_ref)
+    key_lane = lax.broadcasted_iota(jnp.int32, (1, 768), 1)
     key_d = key_lane // 256
+    turn = zl + 1 + key_d
+    turn = jnp.where(turn >= 4, turn - 4, turn)
+    key_rest = turn * 1024 + y * 256 + (key_lane - 256 * key_d)
     first_masked = jnp.maximum(zh - jnp.where(zl == 0, 1, 0), 0)
-
-    def row_block(r, _):
-        start = pl.multiple_of(r * block, block)
-        q = qa[pl.ds(start, block), :]
-        row = start + lax.broadcasted_iota(jnp.int32, (block, 1), 0)
-        query_pos = z * group - HALO + jnp.where(row >= rows, row - rows, row)
-
-        def step(masked, chunk, state):
-            top, acc = state
-            s = lax.dot_general(q, ka[chunk], (((1,), (0,)), ((), ())), preferred_element_type=F32)
-            if masked:
-                turn = zl + key_d
-                key_z = 4 * chunk + jnp.where(turn >= 4, turn - 4, turn)
-                key_pos = key_z * group + y * 256 + (key_lane - 256 * key_d)
-                s = jnp.where(query_pos >= key_pos, s, MASKED)
-            new_top = jnp.maximum(top, jnp.max(s, axis=1, keepdims=True))
-            p = jnp.exp(s - new_top).astype(BF16)
-            more = lax.dot_general(p, va[chunk], (((1,), (1,)), ((), ())), preferred_element_type=F32)
-            return new_top, acc * jnp.exp(top - new_top) + more
-
-        state = (jnp.full((block, 1), MASKED, F32), jnp.zeros((block, 128), F32))
-        state = lax.fori_loop(0, first_masked, functools.partial(step, False), state)
-        top, acc = lax.fori_loop(first_masked, zh + 1, functools.partial(step, True), state)
+    part, blocks = row_blocks(z)
+
+    def step(masked, chunk, state):
+        queries = [qa[start:start + part, :] for start, _, _ in blocks]
+        key_pos = chunk * 4096 + key_rest if masked else None
+        return fold_keys(queries, ka[chunk], va[chunk], state, [pos for _, _, pos in blocks], key_pos)
+
+    state = []
+    for start, _, _ in blocks:
+        piece = state_ref[start:start + part, :]
+        state.append((piece[:, 127:128], piece))
+    state = lax.fori_loop(0, first_masked, functools.partial(step, False), tuple(state))
+    state = lax.fori_loop(first_masked, zh + 1, functools.partial(step, True), state)
+    for (start, second, _), (top, acc) in zip(blocks, state):
         total = acc[:, 64:65]
-        gate = jnp.where(row >= rows, gate_ref[1], gate_ref[0])
-        norm_out[pl.ds(start, block), :] = acc / total
-        lse_rows[pl.ds(start, block), :] = jnp.broadcast_to(top + jnp.log(total) - gate, (block, 128))
-        return 0
-
-    lax.fori_loop(0, 2 * rows // block, row_block, 0)
+        gate = jnp.where(second, gate_ref[1], gate_ref[0])
+        norm_out[start:start + part, :] = acc * (1.0 / total)
+        lse_rows[start:start + part, :] = jnp.broadcast_to(top + jnp.log(total) - gate, (part, 128))
     tail = lse_rows.shape[0] - 2 * rows
     lse_rows[pl.ds(2 * rows, tail), :] = jnp.zeros((tail, 128), F32)
     lse_dense[...] = jnp.zeros(lse_dense.shape, F32)
@@ -140,28 +187,27 @@
                 out_ref[2 * pair + i, pair_rows + 16 * k:pair_rows + 16 * (k + 1), :] = parts[k]
 
 
-def attend(at, gate, queries, own, nxt, far_a, far_b, last):
+def attend_rest(at, gate, queries, state, nxt, far_a, far_b, last):
     rows = HALO + 1024
     pair_rows = HALO + 512
     smem = pl.BlockSpec(memory_space=pltpu.SMEM)
     vmem = pl.BlockSpec(memory_space=pltpu.VMEM)
     return pl.pallas_call(
-        functools.partial(attend_kernel, rows=rows, block=416),
+        attend_rest_kernel,
         out_shape=jax.ShapeDtypeStruct((4, pair_rows + 48, 128), BF16),
         in_specs=[smem, smem] + [vmem] * 6,
         out_specs=vmem,
         scratch_shapes=[
-            pltpu.VMEM((2 * rows, 128), BF16),
-            pltpu.VMEM((4, 128, 1024), BF16),
-            pltpu.VMEM((4, 128, 1024), BF16),
+            pltpu.VMEM((4, 128, 768), BF16),
+            pltpu.VMEM((4, 128, 768), BF16),
             pltpu.VMEM((2 * rows, 128), F32),
             pltpu.VMEM((2 * rows + 112, 128), F32),
             pltpu.VMEM((16, 128), F32),
         ],
-        compiler_params=pltpu.CompilerParams(vmem_limit_bytes=24 * 2**20),
-        cost_estimate=pl.CostEstimate(flops=8 * 10**9, bytes_accessed=4 * 2**20, transcendentals=8 * 10**6),
-        name="attend",
-    )(at, gate, queries, own, nxt, far_a, far_b, last)
+        compiler_params=pltpu.CompilerParams(vmem_limit_bytes=36 * 2**20),
+        cost_estimate=pl.CostEstimate(flops=6 * 10**9, bytes_accessed=4 * 2**20, transcendentals=6 * 10**6),
+        name="attend_rest",
+    )(at, gate, queries, state, nxt, far_a, far_b, last)
 
 
 def merge_kernel(in_ref, out_ref):
@@ -203,7 +249,13 @@
 
 
 def feed_kernel(at_ref, attn_own, attn_other, wide_own, wide_other, gain_ref, conv_ref, w_ref,
-                keep_ref, send_ref, mid_out_ref, af, mid, normed, wg, wu, wd, sems):
+                keep_ref, send_ref, mid_out_ref, af, mid, scaled, wide_in, wg, wu, wd, sems):
+    fetches = []
+    for side, wide in enumerate((wide_own, wide_other)):
+        for i in range(4):
+            fetch = pltpu.make_async_copy(wide.at[i], wide_in.at[side, i], sems.at[3 + 4 * side + i])
+            fetch.start()
+            fetches.append(fetch)
     copies = []
     for k, dst in enumerate((wg, wu, wd)):
         copy = pltpu.make_async_copy(w_ref.at[:, :, k], dst, sems.at[k])
@@ -213,33 +265,35 @@
     block = at_ref[5]
     rows = HALO + 512
     at_x = block // 2
-    sides = ((core, attn_own, wide_own, keep_ref), (1 - core, attn_other, wide_other, send_ref))
-    for c, attn, _, _ in sides:
+    sides = ((core, attn_own, keep_ref), (1 - core, attn_other, send_ref))
+    for c, attn, _ in sides:
         for x in range(4):
             af[:, pl.ds(pl.multiple_of(128 * (2 * x + c), 128), 128)] = attn[x]
     a = af[...]
     square = jnp.zeros((rows, 1), F32)
-    for c, _, wide, _ in sides:
+    for side, (c, _, _) in enumerate(sides):
         for i, back in enumerate((0, 1, 3, 2)):
+            fetches[4 * side + i].wait()
             x = jnp.where(at_x >= back, at_x - back, at_x - back + 4)
-            branch = jnp.dot(a, wide[i, 0:1024, :], preferred_element_type=F32)
-            m = (branch + wide[i, 1024:1024 + rows, :].astype(F32)).astype(BF16)
-            mid[:, pl.ds(pl.multiple_of(256 * (2 * x + c), 256), 256)] = m
+            cols = pl.ds(pl.multiple_of(256 * (2 * x + c), 256), 256)
+            branch = jnp.dot(a, wide_in[side, i, 0:1024, :], preferred_element_type=F32)
+            m = (branch + wide_in[side, i, 1024:1024 + rows, :].astype(F32)).astype(BF16)
+            if side == 0 and i == 0:
+                mid[...] = m
             m = m.astype(F32)
             square = square + jnp.sum(m * m, axis=1, keepdims=True)
+            scaled[:, cols] = (m * gain_ref[:, cols]).astype(BF16)
     inverse = lax.rsqrt(square * (1.0 / 2048) + NORM_EPS)
-    for j in range(8):
-        cols = slice(256 * j, 256 * (j + 1))
-        normed[:, cols] = (mid[:, cols].astype(F32) * inverse * gain_ref[:, cols]).astype(BF16)
-    mid_out_ref[...] = mid[pl.ds(pl.multiple_of(HALO + 256 * half, 16), 256), pl.ds(pl.multiple_of(256 * block, 256), 256)]
-    n = normed[...]
+    mid_out_ref[...] = mid[pl.ds(pl.multiple_of(HALO + 256 * half, 16), 256), :]
+    n = scaled[...]
     copies[0].wait()
     copies[1].wait()
     row = lax.broadcasted_iota(jnp.int32, (rows, 1), 0)
     keep = jnp.logical_not((row < HALO) & (is_first == 1))
 
     def mixed(weight, index):
-        pre = jnp.dot(n, weight[...].reshape(2048, 352), preferred_element_type=F32).astype(BF16).astype(F32)
+        pre = jnp.dot(n, weight[...].reshape(2048, 352), preferred_element_type=F32)
+        pre = (pre * inverse).astype(BF16).astype(F32)
         pre = jnp.where(keep, pre, 0.0)
         total = jnp.zeros((512, 352), F32)
         for k in range(3):
@@ -250,7 +304,7 @@
     up = mixed(wu, 1)
     hidden = (gate / (1.0 + jnp.exp(-gate)) * up).astype(BF16)
     copies[2].wait()
-    for c, _, _, part_ref in sides:
+    for c, _, part_ref in sides:
         for x in range(4):
             down = wd[pl.ds(2 * (2 * x + c), 2)].reshape(256, 352)
             part = lax.dot_general(hidden, down, (((1,), (1,)), ((), ())), preferred_element_type=F32).astype(BF16)
@@ -263,19 +317,21 @@
     vmem = pl.BlockSpec(memory_space=pltpu.VMEM)
     rows = HALO + 512
     half = jax.ShapeDtypeStruct((2, 4, 256, 256), BF16)
+    hbm = pl.BlockSpec(memory_space=pltpu.HBM)
     return pl.pallas_call(
         feed_kernel,
         out_shape=(half, half, jax.ShapeDtypeStruct((256, 256), BF16)),
-        in_specs=[smem] + [vmem] * 6 + [pl.BlockSpec(memory_space=pltpu.HBM)],
+        in_specs=[smem, vmem, vmem, hbm, hbm, vmem, vmem, hbm],
         out_specs=(vmem, vmem, vmem),
         scratch_shapes=[
             pltpu.VMEM((rows, 1024), BF16),
+            pltpu.VMEM((rows, 256), BF16),
             pltpu.VMEM((rows, 2048), BF16),
-            pltpu.VMEM((rows, 2048), BF16),
+            pltpu.VMEM((2, 4, 1024 + rows, 256), BF16),
             pltpu.VMEM((16, 4, 32, 352), BF16),
             pltpu.VMEM((16, 4, 32, 352), BF16),
             pltpu.VMEM((16, 4, 32, 352), BF16),
-            pltpu.SemaphoreType.DMA((3,)),
+            pltpu.SemaphoreType.DMA((11,)),
         ],
         compiler_params=pltpu.CompilerParams(vmem_limit_bytes=50 * 2**20),
         cost_estimate=pl.CostEstimate(flops=5 * 10**9, bytes_accessed=2**24, transcendentals=2 * 10**5),
@@ -285,7 +341,7 @@
 
 def prepare_kernel(kv_ref, decay_ref, gate_ref, up_ref, down_ref, q_ref, resid_ref, keys_ref, halves_ref, tail_ref):
     turned = kv_ref[0].astype(F32).T.astype(BF16)
-    row = lax.broadcasted_iota(jnp.int32, (16, 256), 0)
+    row = lax.broadcasted_iota(jnp.int32, (8, 256), 0)
     value = jnp.where(row < 3, decay_ref[0:1, :], decay_ref[1:2, :])
     which = jnp.where(row < 3, row, row - 3)
     high, middle, low = split3(value)
@@ -293,8 +349,8 @@
     gates = jnp.where(row < 6, pick, 0.0).astype(BF16)
     for i in range(4):
         keys_ref[i, 0:64, :] = turned[0:64]
-        keys_ref[i, 64:80, :] = gates
-        keys_ref[i, 80:144, :] = turned[64:128]
+        keys_ref[i, 64:72, :] = gates
+        keys_ref[i, 72:136, :] = turned[64:128]
     for k, ref in enumerate((gate_ref, up_ref, down_ref)):
         value = ref[...].astype(F32)
         for p in range(2):
@@ -310,7 +366,7 @@
     return pl.pallas_call(
         prepare_kernel,
         out_shape=(
-            jax.ShapeDtypeStruct((4, 144, 256), BF16),
+            jax.ShapeDtypeStruct((4, 136, 256), BF16),
             jax.ShapeDtypeStruct((4, 3, 32, 352), BF16),
             jax.ShapeDtypeStruct((HALO, 384), BF16),
         ),
@@ -346,7 +402,8 @@
     far_b = shifted(own[2:], Z, 2)
     group_q = spread(jnp.concatenate([before[:, :128], queries], axis=0), Y)
 
-    partial = attend(at, cum_gate[:, 0], group_q, own, nxt, far_a, far_b, last)
+    queries, state = attend_own(at, cum_gate[:, 0], group_q, own)
+    partial = attend_rest(at, cum_gate[:, 0], queries, state, nxt, far_a, far_b, last)
     partial = exchanged(partial, Y)
     wide = jnp.stack(wides)
     other_wide = shifted(wide, "c", 1)

time: 207 us -> 228 us (1.10)
  the two profiles are of different devices: /device:TPU:416 before, /device:TPU:448 now
where the time goes in v2:
time: 228 us; the launch traced here: 227 us
  waiting for transfers between devices  65.3 us (29%)
  blocking collectives  57.5 us (25%)
  starting transfers between devices  48.8 us (21%)
  Pallas kernels  36.3 us (16%)
  between operations  13.7 us (6%)
  other arithmetic  4.14 us (2%)
    ppermute x12, waiting for transfers between devices, shifted(): lax.ppermute(value, axis, [(i, (i + by) % size) for i in range(size)])  45.7 us
    all_to_all x3, blocking collectives, exchanged(): return lax.all_to_all(value, axis, 0, 0, tiled=True)  44.2 us
    ppermute x12, starting transfers between devices, shifted(): lax.ppermute(value, axis, [(i, (i + by) % size) for i in range(size)])  35.2 us
    all_to_all x2, waiting for transfers between devices, exchanged(): return lax.all_to_all(value, axis, 0, 0, tiled=True)  19.5 us
    pallas_call x1, Pallas kernels, attend_rest(): pl.pallas_call(attend_rest_kernel, out_shape=jax.ShapeDtypeStruct((4, pai...  17.8 us
    all_to_all x2, starting transfers between devices, exchanged(): return lax.all_to_all(value, axis, 0, 0, tiled=True)  13.7 us
    all_gather x1, blocking collectives, layer(): attn = lax.all_gather(attn, 'x', axis=0, tiled=False)  13.3 us
    pallas_call x1, Pallas kernels, feed(): pl.pallas_call(feed_kernel, out_shape=(half, half, jax.ShapeDtypeStruct((...  12.3 us
  transfers between devices with their start and end apart: 15, of which 8 were waited for; matrix products, arithmetic and copies ran while one was open for 2% of the time, Pallas kernels for 10%

profile of v2, /device:TPU:448, one launch (start us, length us, event | category | flops | bytes accessed | tf_op | source)
XLA Modules:
  0.0 226.8 jit_solution(4137006505985915661)
XLA Ops:
  6.5 2.0 prepare.1
  8.6 11.6 %all_to_all.25 = bf16[4,3,32,352]{3,2,1,0:T(8,128)(2,1)} all-to-all(bf16[4,3,32,352]{3,2,1,0:T(8,128)(2,1)} %get-tuple-element.17), channel_id=1, replica_groups=mesh['zh'=4,'zl'=4,'yh'=2,'yl'=2,'x'=4,'c'=2] {'yh','yl'}, dimensions={0} | all-to-all | bytes 540672 | tf_op jit(solution)/shard_map/all_to_all | solution.py:29
  20.2 2.5 %collective-permute-start = (bf16[16,384]{1,0:T(8,128)(2,1)}, bf16[16,384]{1,0:T(8,128)(2,1)S(1)}, u32[]{:S(2)}, u32[]{:S(2)}) collective-permute-start(bf16[16,384]{1,0:T(8,128)(2,1)} %get-tuple-element.13), channel_id=1, source_target_pairs={{0,8},{8,16},{16,24},{24,32},{32,40},{40,48},{48,56},{56,64},{64,7... | collective-permute-start | bytes 36872 | tf_op jit(solution)/shard_map/ppermute | solution.py:25
  22.7 5.4 %collective-permute-done = bf16[16,384]{1,0:T(8,128)(2,1)S(1)} collective-permute-done((bf16[16,384]{1,0:T(8,128)(2,1)}, bf16[16,384]{1,0:T(8,128)(2,1)S(1)}, u32[]{:S(2)}, u32[]{:S(2)}) %collective-permute-start) | collective-permute-done | bytes 12320 | tf_op jit(solution)/shard_map/ppermute | solution.py:25
  31.0 5.0 %collective-permute-done.6 = bf16[272,256]{1,0:T(8,128)(2,1)S(1)} collective-permute-done((bf16[272,256]{1,0:T(8,128)(2,1)S(1)}, bf16[272,256]{1,0:T(8,128)(2,1)S(1)}, u32[]{:S(2)}, u32[]{:S(2)}) %collective-permute-start.6) | collective-permute-done | bytes 139296 | tf_op jit(solution)/shard_map/ppermute | solution.py:25
  36.1 4.9 %collective-permute-start.9 = (bf16[1552,256]{1,0:T(8,128)(2,1)S(1)}, bf16[1552,256]{1,0:T(8,128)(2,1)S(1)}, u32[]{:S(2)}, u32[]{:S(2)}) collective-permute-start(bf16[1552,256]{1,0:T(8,128)(2,1)S(1)} %fusion.2), channel_id=1, source_target_pairs={{0,4},{2,6},{4,0},{6,2},{1,5},{3,7},{5,1},{7,3},{8,12},{10,14},{12... | collective-permute-start | bytes 2383880 | tf_op jit(solution)/shard_map/ppermute | solution.py:25
  41.1 3.0 %collective-permute-start.8 = (bf16[1552,256]{1,0:T(8,128)(2,1)S(1)}, bf16[1552,256]{1,0:T(8,128)(2,1)S(1)}, u32[]{:S(2)}, u32[]{:S(2)}) collective-permute-start(bf16[1552,256]{1,0:T(8,128)(2,1)S(1)} %fusion.2), channel_id=1, source_target_pairs={{0,6},{2,0},{4,2},{6,4},{1,7},{3,1},{5,3},{7,5},{8,14},{10,8},{12,... | collective-permute-start | bytes 2383880 | tf_op jit(solution)/shard_map/ppermute | solution.py:25
  44.1 2.8 %collective-permute-start.7 = (bf16[1552,256]{1,0:T(8,128)(2,1)S(1)}, bf16[1552,256]{1,0:T(8,128)(2,1)S(1)}, u32[]{:S(2)}, u32[]{:S(2)}) collective-permute-start(bf16[1552,256]{1,0:T(8,128)(2,1)S(1)} %fusion.2), channel_id=1, source_target_pairs={{0,2},{2,4},{4,6},{6,0},{1,3},{3,5},{5,7},{7,1},{8,10},{10,12},{12... | collective-permute-start | bytes 2383880 | tf_op jit(solution)/shard_map/ppermute | solution.py:25
  47.0 13.1 %collective-permute-done.9 = bf16[1552,256]{1,0:T(8,128)(2,1)S(1)} collective-permute-done((bf16[1552,256]{1,0:T(8,128)(2,1)S(1)}, bf16[1552,256]{1,0:T(8,128)(2,1)S(1)}, u32[]{:S(2)}, u32[]{:S(2)}) %collective-permute-start.9) | collective-permute-done | bytes 794656 | tf_op jit(solution)/shard_map/ppermute | solution.py:25
  60.1 12.3 %collective-permute-done.8 = bf16[1552,256]{1,0:T(8,128)(2,1)S(1)} collective-permute-done((bf16[1552,256]{1,0:T(8,128)(2,1)S(1)}, bf16[1552,256]{1,0:T(8,128)(2,1)S(1)}, u32[]{:S(2)}, u32[]{:S(2)}) %collective-permute-start.8) | collective-permute-done | bytes 794656 | tf_op jit(solution)/shard_map/ppermute | solution.py:25
  76.2 10.2 %all-to-all-start.1 = ((bf16[4,136,256]{2,1,0:T(8,128)(2,1)}), bf16[4,136,256]{2,1,0:T(8,128)(2,1)S(1)}, u32[]{:S(2)}, u32[]{:S(2)}) async-start(bf16[4,136,256]{2,1,0:T(8,128)(2,1)} %get-tuple-element.14), calls=%async_computation.1 | async-start | bytes 557056 | tf_op jit(solution)/shard_map/all_to_all | solution.py:29
  86.7 19.5 %all-to-all-done.1.own_ref = bf16[4,136,256]{2,1,0:T(8,128)(2,1)S(1)} async-done(((bf16[4,136,256]{2,1,0:T(8,128)(2,1)}), bf16[4,136,256]{2,1,0:T(8,128)(2,1)S(1)}, u32[]{:S(2)}, u32[]{:S(2)}) %all-to-all-start.1) | async-done | bytes 278560 | tf_op jit(solution)/shard_map/all_to_all | solution.py:29
  106.9 3.4 %all-to-all-start = ((bf16[4,272,128]{2,1,0:T(8,128)(2,1)}), bf16[4,272,128]{2,1,0:T(8,128)(2,1)S(1)}, u32[]{:S(2)}, u32[]{:S(2)}) async-start(bf16[4,272,128]{2,1,0:T(8,128)(2,1)} %broadcast_in_dim.2), calls=%async_computation | async-start | bytes 557056 | tf_op jit(solution)/shard_map/all_to_all | solution.py:29
  112.3 3.9 %collective-permute-start.1 = (bf16[4,136,256]{2,1,0:T(8,128)(2,1)S(1)}, bf16[4,136,256]{2,1,0:T(8,128)(2,1)S(1)}, u32[]{:S(2)}, u32[]{:S(2)}) collective-permute-start(bf16[4,136,256]{2,1,0:T(8,128)(2,1)S(1)} %all-to-all-done.1.own_ref), channel_id=1, source_target_pairs={{0,480},{32,0},{64,32},{96,64},{128,96},{160,128},{192,160},{224,1... | collective-permute-start | bytes 835592 | tf_op jit(solution)/shard_map/ppermute | solution.py:25
  116.3 6.2 %collective-permute-start.3 = (bf16[2,136,256]{2,1,0:T(8,128)(2,1)S(1)}, bf16[2,136,256]{2,1,0:T(8,128)(2,1)S(1)}, u32[]{:S(2)}, u32[]{:S(2)}) collective-permute-start(bf16[2,136,256]{2,1,0:T(8,128)(2,1)S(1)} %get-tuple-element.21), channel_id=1, source_target_pairs={{0,64},{32,96},{64,128},{96,160},{128,192},{160,224},{192,256},{22... | collective-permute-start | bytes 417800 | tf_op jit(solution)/shard_map/ppermute | solution.py:25
  124.4 3.5 %attend_own.1 = (bf16[2080,128]{1,0:T(8,128)(2,1)S(1)}, f32[2080,128]{1,0:T(8,128)S(1)}) custom-call(s32[7]{0:T(128)S(1)} %stack.48.at_ref, f32[2]{0:T(128)S(1)} %slice_reduce_fusion.gate_ref, bf16[4,272,128]{2,1,0:T(8,128)(2,1)S(1)} %all-to-all-done.q_ref, bf16[4,136,256]{2,1,0:T(8,128)(2,1)S(1)} %all-to-all-done.1.own_ref), custom_call_target="tpu_custom_call" | custom-call | flops 2000000000 | bytes 1048576 | tf_op jit(solution)/shard_map/attend_own/pallas_call | solution.py:124
  127.9 5.8 %collective-permute-done.2.far_a_ref = bf16[2,136,256]{2,1,0:T(8,128)(2,1)S(1)} collective-permute-done((bf16[2,136,256]{2,1,0:T(8,128)(2,1)S(1)}, bf16[2,136,256]{2,1,0:T(8,128)(2,1)S(1)}, u32[]{:S(2)}, u32[]{:S(2)}) %collective-permute-start.2) | collective-permute-done | bytes 139296 | tf_op jit(solution)/shard_map/ppermute | solution.py:25
  133.7 17.8 %attend_rest.1 = bf16[4,576,128]{2,1,0:T(8,128)(2,1)S(1)} custom-call(s32[7]{0:T(128)S(1)} %stack.48.at_ref, f32[2]{0:T(128)S(1)} %slice_reduce_fusion.gate_ref, bf16[2080,128]{1,0:T(8,128)(2,1)S(1)} %get-tuple-element.15.qa, f32[2080,128]{1,0:T(8,128)S(1)} %get-tuple-element.16.state_ref, bf16[4,136,256]{2,1,0:T(8,128)(2,1)S(1)} %collective-permute-done.1.next_ref, ...), custom_call_target="tpu_custom_call" | custom-call | flops 6000000000 | bytes 4194304 | tf_op jit(solution)/shard_map/attend_rest/pallas_call | solution.py:195
  151.6 13.9 %all_to_all.26.in_ref = bf16[4,576,128]{2,1,0:T(8,128)(2,1)S(1)} all-to-all(bf16[4,576,128]{2,1,0:T(8,128)(2,1)S(1)} %attend_rest.1), channel_id=1, replica_groups=mesh['zh'=4,'zl'=4,'yh'=2,'yl'=2,'x'=4,'c'=2] {'yh','yl'}, dimensions={0} | all-to-all | bytes 1179648 | tf_op jit(solution)/shard_map/all_to_all | solution.py:29
  166.1 13.3 %all-gather = bf16[2112,128]{1,0:T(8,128)(2,1)S(1)} all-gather(bf16[528,128]{1,0:T(8,128)(2,1)S(1)} %merge.1), channel_id=2, replica_groups=mesh['zh'=4,'zl'=4,'yh'=2,'yl'=2,'x'=4,'c'=2] {'x'}, dimensions={0}, use_global_device_ids=true | all-gather | bytes 675840 | tf_op jit(solution)/shard_map/all_gather | solution.py:411
  179.4 2.1 collective-permute-start.5
  183.3 12.3 %feed.1 = (bf16[2,4,256,256]{3,2,1,0:T(8,128)(2,1)S(1)}, bf16[2,4,256,256]{3,2,1,0:T(8,128)(2,1)S(1)}, bf16[256,256]{1,0:T(8,128)(2,1)S(1)}) custom-call(s32[7]{0:T(128)S(1)} %stack.48.at_ref, bf16[4,528,128]{2,1,0:T(8,128)(2,1)S(1)} %bitcast.23, bf16[4,528,128]{2,1,0:T(8,128)(2,1)S(1)} %collective-permute-done.5.attn_other, ...), custom_call_target="tpu_custom_call" | custom-call | flops 5000000000 | bytes 16777216 | tf_op jit(solution)/shard_map/feed/pallas_call | solution.py:321
  197.6 2.5 %collective-permute-done.11 = bf16[2,4,256,256]{3,2,1,0:T(8,128)(2,1)S(1)} collective-permute-done((bf16[2,4,256,256]{3,2,1,0:T(8,128)(2,1)S(1)}, bf16[2,4,256,256]{3,2,1,0:T(8,128)(2,1)S(1)}, u32[]{:S(2)}, u32[]{:S(2)}) %collective-permute-start.11) | collective-permute-done | bytes 1048608 | tf_op jit(solution)/shard_map/ppermute | solution.py:25
  200.5 18.7 %all_to_all.27 = bf16[8,256,256]{2,1,0:T(8,128)(2,1)S(1)} all-to-all(bf16[8,256,256]{2,1,0:T(8,128)(2,1)S(1)} %bitcast.25), channel_id=1, replica_groups=mesh['zh'=4,'zl'=4,'yh'=2,'yl'=2,'x'=4,'c'=2] {'yl','x'}, dimensions={0} | all-to-all | bytes 2097152 | tf_op jit(solution)/shard_map/all_to_all | solution.py:29
  (45 shorter events, 17.2 us)
Async XLA Ops:
  6.5 29.5 %copy-start.1 = (bf16[256,256]{1,0:T(8,128)(2,1)S(1)}, bf16[256,256]{1,0:T(8,128)(2,1)}, u32[]{:S(2)}) copy-start(bf16[256,256]{1,0:T(8,128)(2,1)} %resid_ref.1) | copy-start | bytes 393220
  6.5 29.5 %copy-start.2 = (bf16[1024,256]{1,0:T(8,128)(2,1)S(1)}, bf16[1024,256]{1,0:T(8,128)(2,1)}, u32[]{:S(2)}) copy-start(bf16[1024,256]{1,0:T(8,128)(2,1)} %param.14) | copy-start | bytes 1572868
  6.5 176.7 %all-gather.4.cloned.1.call-start = ((), (), s32[]{:S(2)}) async-start(), calls=%async_computation.5 | async-start | bytes 5013504 | tf_op jit(solution)/shard_map/all_gather | solution.py:391
  20.2 7.9 %collective-permute-start = (bf16[16,384]{1,0:T(8,128)(2,1)}, bf16[16,384]{1,0:T(8,128)(2,1)S(1)}, u32[]{:S(2)}, u32[]{:S(2)}) collective-permute-start(bf16[16,384]{1,0:T(8,128)(2,1)} %get-tuple-element.13), channel_id=1, source_target_pairs={{0,8},{8,16},{16,24},{24,32},{32,40},{40,48},{48,56},{56,64},{64,7... | collective-permute-start | bytes 36872 | tf_op jit(solution)/shard_map/ppermute | solution.py:25
  29.0 6.9 %collective-permute-start.6 = (bf16[272,256]{1,0:T(8,128)(2,1)S(1)}, bf16[272,256]{1,0:T(8,128)(2,1)S(1)}, u32[]{:S(2)}, u32[]{:S(2)}) collective-permute-start(bf16[272,256]{1,0:T(8,128)(2,1)S(1)} %pad_maximum_fusion.5), channel_id=1, source_target_pairs={{0,8},{8,0},{1,9},{9,1},{2,10},{10,2},{3,11},{11,3},{4,12},{12,4},... | collective-permute-start | bytes 417800 | tf_op jit(solution)/shard_map/ppermute | solution.py:25
  36.1 24.0 %collective-permute-start.9 = (bf16[1552,256]{1,0:T(8,128)(2,1)S(1)}, bf16[1552,256]{1,0:T(8,128)(2,1)S(1)}, u32[]{:S(2)}, u32[]{:S(2)}) collective-permute-start(bf16[1552,256]{1,0:T(8,128)(2,1)S(1)} %fusion.2), channel_id=1, source_target_pairs={{0,4},{2,6},{4,0},{6,2},{1,5},{3,7},{5,1},{7,3},{8,12},{10,14},{12... | collective-permute-start | bytes 2383880 | tf_op jit(solution)/shard_map/ppermute | solution.py:25
  41.1 31.3 %collective-permute-start.8 = (bf16[1552,256]{1,0:T(8,128)(2,1)S(1)}, bf16[1552,256]{1,0:T(8,128)(2,1)S(1)}, u32[]{:S(2)}, u32[]{:S(2)}) collective-permute-start(bf16[1552,256]{1,0:T(8,128)(2,1)S(1)} %fusion.2), channel_id=1, source_target_pairs={{0,6},{2,0},{4,2},{6,4},{1,7},{3,1},{5,3},{7,5},{8,14},{10,8},{12,... | collective-permute-start | bytes 2383880 | tf_op jit(solution)/shard_map/ppermute | solution.py:25
  44.1 28.3 %collective-permute-start.7 = (bf16[1552,256]{1,0:T(8,128)(2,1)S(1)}, bf16[1552,256]{1,0:T(8,128)(2,1)S(1)}, u32[]{:S(2)}, u32[]{:S(2)}) collective-permute-start(bf16[1552,256]{1,0:T(8,128)(2,1)S(1)} %fusion.2), channel_id=1, source_target_pairs={{0,2},{2,4},{4,6},{6,0},{1,3},{3,5},{5,7},{7,1},{8,10},{10,12},{12... | collective-permute-start | bytes 2383880 | tf_op jit(solution)/shard_map/ppermute | solution.py:25
  72.4 14.1 %copy-start.5 = (f32[2,256]{1,0:T(2,128)S(1)}, f32[2,256]{1,0:T(2,128)}, u32[]{:S(2)}) copy-start(f32[2,256]{1,0:T(2,128)} %decay_ref.1) | copy-start | bytes 6148
  72.4 14.2 %copy-start.3 = (bf16[256,128]{1,0:T(8,128)(2,1)S(1)}, bf16[256,128]{1,0:T(8,128)(2,1)}, u32[]{:S(2)}) copy-start(bf16[256,128]{1,0:T(8,128)(2,1)} %q_ref.1) | copy-start | bytes 196612
  74.3 108.9 %collective-permute-start.10 = (bf16[4,1552,256]{2,1,0:T(8,128)(2,1)}, bf16[4,1552,256]{2,1,0:T(8,128)(2,1)}, u32[]{:S(2)}, u32[]{:S(2)}) collective-permute-start(bf16[4,1552,256]{2,1,0:T(8,128)(2,1)} %pad_maximum_fusion.wide_own), channel_id=1, source_target_pairs={{0,1},{1,0},{2,3},{3,2},{4,5},{5,4},{6,7},{7,6},{8,9},{9,8},{10,11... | collective-permute-start | bytes 9535496 | tf_op jit(solution)/shard_map/ppermute | solution.py:25
  76.2 30.0 %all-to-all-start.1 = ((bf16[4,136,256]{2,1,0:T(8,128)(2,1)}), bf16[4,136,256]{2,1,0:T(8,128)(2,1)S(1)}, u32[]{:S(2)}, u32[]{:S(2)}) async-start(bf16[4,136,256]{2,1,0:T(8,128)(2,1)} %get-tuple-element.14), calls=%async_computation.1 | async-start | bytes 557056 | tf_op jit(solution)/shard_map/all_to_all | solution.py:29
  106.9 17.5 %all-to-all-start = ((bf16[4,272,128]{2,1,0:T(8,128)(2,1)}), bf16[4,272,128]{2,1,0:T(8,128)(2,1)S(1)}, u32[]{:S(2)}, u32[]{:S(2)}) async-start(bf16[4,272,128]{2,1,0:T(8,128)(2,1)} %broadcast_in_dim.2), calls=%async_computation | async-start | bytes 557056 | tf_op jit(solution)/shard_map/all_to_all | solution.py:29
  110.4 23.3 %collective-permute-start.4 = (bf16[4,136,256]{2,1,0:T(8,128)(2,1)S(1)}, bf16[4,136,256]{2,1,0:T(8,128)(2,1)S(1)}, u32[]{:S(2)}, u32[]{:S(2)}) collective-permute-start(bf16[4,136,256]{2,1,0:T(8,128)(2,1)S(1)} %all-to-all-done.1.own_ref), channel_id=1, source_target_pairs={{0,32},{32,64},{64,96},{96,128},{128,160},{160,192},{192,224},{224... | collective-permute-start | bytes 835592 | tf_op jit(solution)/shard_map/ppermute | solution.py:25
  112.3 21.4 %collective-permute-start.1 = (bf16[4,136,256]{2,1,0:T(8,128)(2,1)S(1)}, bf16[4,136,256]{2,1,0:T(8,128)(2,1)S(1)}, u32[]{:S(2)}, u32[]{:S(2)}) collective-permute-start(bf16[4,136,256]{2,1,0:T(8,128)(2,1)S(1)} %all-to-all-done.1.own_ref), channel_id=1, source_target_pairs={{0,480},{32,0},{64,32},{96,64},{128,96},{160,128},{192,160},{224,1... | collective-permute-start | bytes 835592 | tf_op jit(solution)/shard_map/ppermute | solution.py:25
  116.3 11.6 %collective-permute-start.3 = (bf16[2,136,256]{2,1,0:T(8,128)(2,1)S(1)}, bf16[2,136,256]{2,1,0:T(8,128)(2,1)S(1)}, u32[]{:S(2)}, u32[]{:S(2)}) collective-permute-start(bf16[2,136,256]{2,1,0:T(8,128)(2,1)S(1)} %get-tuple-element.21), channel_id=1, source_target_pairs={{0,64},{32,96},{64,128},{96,160},{128,192},{160,224},{192,256},{22... | collective-permute-start | bytes 417800 | tf_op jit(solution)/shard_map/ppermute | solution.py:25
  122.5 11.2 %collective-permute-start.2 = (bf16[2,136,256]{2,1,0:T(8,128)(2,1)S(1)}, bf16[2,136,256]{2,1,0:T(8,128)(2,1)S(1)}, u32[]{:S(2)}, u32[]{:S(2)}) collective-permute-start(bf16[2,136,256]{2,1,0:T(8,128)(2,1)S(1)} %get-tuple-element.22), channel_id=1, source_target_pairs={{0,448},{32,480},{64,0},{96,32},{128,64},{160,96},{192,128},{224,1... | collective-permute-start | bytes 417800 | tf_op jit(solution)/shard_map/ppermute | solution.py:25
  151.5 30.0 %copy-start.4 = (f32[3,2,704]{2,1,0:T(2,128)S(1)}, f32[3,2,704]{2,1,0:T(2,128)}, u32[]{:S(2)}) copy-start(f32[3,2,704]{2,1,0:T(2,128)} %param.18) | copy-start | bytes 50692
  151.5 31.7 %copy-start = (f32[2048]{0:T(1024)S(1)}, f32[2048]{0:T(1024)}, u32[]{:S(2)}) copy-start(f32[2048]{0:T(1024)} %param.15) | copy-start | bytes 24580
  179.4 3.8 %collective-permute-start.5 = (bf16[4,528,128]{2,1,0:T(8,128)(2,1)S(1)}, bf16[4,528,128]{2,1,0:T(8,128)(2,1)S(1)}, u32[]{:S(2)}, u32[]{:S(2)}) collective-permute-start(bf16[4,528,128]{2,1,0:T(8,128)(2,1)S(1)} %bitcast.22), channel_id=1, source_target_pairs={{0,1},{1,0},{2,3},{3,2},{4,5},{5,4},{6,7},{7,6},{8,9},{9,8},{10,11... | collective-permute-start | bytes 1622024 | tf_op jit(solution)/shard_map/ppermute | solution.py:25
  195.6 4.6 %collective-permute-start.11 = (bf16[2,4,256,256]{3,2,1,0:T(8,128)(2,1)S(1)}, bf16[2,4,256,256]{3,2,1,0:T(8,128)(2,1)S(1)}, u32[]{:S(2)}, u32[]{:S(2)}) collective-permute-start(bf16[2,4,256,256]{3,2,1,0:T(8,128)(2,1)S(1)} %get-tuple-element.20), channel_id=1, source_target_pairs={{0,1},{1,0},{2,3},{3,2},{4,5},{5,4},{6,7},{7,6},{8,9},{9,8},{10,11... | collective-permute-start | bytes 3145736 | tf_op jit(solution)/shard_map/ppermute | solution.py:25
Sparse Core Ops, SparseCore 0:
  20.3 82.9 all-gather.3

commit v3 on v2

--- a/solution.py
+++ b/solution.py
@@ -27,11 +27,6 @@
 
 def exchanged(value, axis):
     return lax.all_to_all(value, axis, 0, 0, tiled=True)
-
-
-def spread(value, axis):
-    size = lax.axis_size(axis)
-    return exchanged(jnp.broadcast_to(value[None], (size, *value.shape)), axis)
 
 
 def split3(value):
@@ -86,7 +81,8 @@
     return part, blocks
 
 
-def attend_own_kernel(at_ref, gate_ref, q_ref, own_ref, qa, state_ref, ka, va):
+def attend_own_kernel(at_ref, gate_ref, q0_ref, q1_ref, q2_ref, q3_ref, own_ref, qa, state_ref, ka, va):
+    q_refs = (q0_ref, q1_ref, q2_ref, q3_ref)
     zh, zl, y = at_ref[0], at_ref[1], at_ref[2]
     z = 4 * zh + zl
     rows = HALO + 1024
@@ -99,11 +95,17 @@
             first = 64 + 3 * head
             ones = jnp.where((lane >= first) & (lane < first + 3), 1.0, 0.0)
             both = jnp.where(lane < 64, side, ones)
-            qa[head * rows + start:head * rows + start + piece.shape[0], :] = both.astype(BF16)
-
-    put_queries(0, q_ref[0, 0:HALO, :])
-    for i in range(4):
-        put_queries(HALO + 256 * i, q_ref[i, HALO:HALO + 256, :])
+            first_row = pl.multiple_of(head * rows + start, HALO)
+            qa[pl.ds(first_row, piece.shape[0]), :] = both.astype(BF16)
+
+    for back, q_ref in zip((0, 1, 3, 2), q_refs):
+        from_y = jnp.where(y >= back, y - back, y - back + 4)
+        put_queries(HALO + 256 * from_y, q_ref[HALO:HALO + 256, :])
+
+        @pl.when(from_y == 0)
+        def _(q_ref=q_ref):
+            put_queries(0, q_ref[0:HALO, :])
+
     for chunk in range(4):
         put_keys(ka, va, 0, chunk, own_ref[chunk], gate_ref)
     key_lane = lax.broadcasted_iota(jnp.int32, (1, 1024), 1)
@@ -124,17 +126,17 @@
     return pl.pallas_call(
         attend_own_kernel,
         out_shape=(jax.ShapeDtypeStruct((2 * rows, 128), BF16), jax.ShapeDtypeStruct((2 * rows, 128), F32)),
-        in_specs=[smem, smem, vmem, vmem],
+        in_specs=[smem, smem] + [vmem] * 5,
         out_specs=(vmem, vmem),
         scratch_shapes=[pltpu.VMEM((1, 128, 1024), BF16), pltpu.VMEM((1, 128, 1024), BF16)],
         compiler_params=pltpu.CompilerParams(vmem_limit_bytes=30 * 2**20),
         cost_estimate=pl.CostEstimate(flops=2 * 10**9, bytes_accessed=2**20, transcendentals=2 * 10**6),
         name="attend_own",
-    )(at, gate, queries, own)
+    )(at, gate, *queries, own)
 
 
 def attend_rest_kernel(at_ref, gate_ref, qa, state_ref, next_ref, far_a_ref, far_b_ref, last_ref,
-                       out_ref, ka, va, norm_out, lse_rows, lse_dense):
+                       out_ref, ka, va, states, norm_out, lse_rows, lse_dense):
     zh, zl, y = at_ref[0], at_ref[1], at_ref[2]
     z = 4 * zh + zl
     rows = HALO + 1024
@@ -151,18 +153,29 @@
     first_masked = jnp.maximum(zh - jnp.where(zl == 0, 1, 0), 0)
     part, blocks = row_blocks(z)
 
-    def step(masked, chunk, state):
+    for chunk in range(1, 4):
+        @pl.when(chunk > zh)
+        def _(chunk=chunk):
+            states[chunk] = jnp.where(lane < 96, jnp.zeros((2 * rows, 128), F32), MASKED)
+
+    def step(masked, chunk, _):
+        fresh = tuple((jnp.full((part, 1), MASKED, F32), jnp.zeros((part, 128), F32)) for _ in blocks)
         queries = [qa[start:start + part, :] for start, _, _ in blocks]
         key_pos = chunk * 4096 + key_rest if masked else None
-        return fold_keys(queries, ka[chunk], va[chunk], state, [pos for _, _, pos in blocks], key_pos)
-
-    state = []
-    for start, _, _ in blocks:
-        piece = state_ref[start:start + part, :]
-        state.append((piece[:, 127:128], piece))
-    state = lax.fori_loop(0, first_masked, functools.partial(step, False), tuple(state))
-    state = lax.fori_loop(first_masked, zh + 1, functools.partial(step, True), state)
-    for (start, second, _), (top, acc) in zip(blocks, state):
+        state = fold_keys(queries, ka[chunk], va[chunk], fresh, [pos for _, _, pos in blocks], key_pos)
+        for (start, _, _), (top, acc) in zip(blocks, state):
+            states[chunk, start:start + part, :] = jnp.where(lane < 96, acc, top)
+        return 0
+
+    lax.fori_loop(0, first_masked, functools.partial(step, False), 0)
+    lax.fori_loop(first_masked, zh + 1, functools.partial(step, True), 0)
+    for start, second, _ in blocks:
+        pieces = [state_ref[start:start + part, :]] + [states[chunk, start:start + part, :] for chunk in range(4)]
+        tops = [piece[:, 127:128] for piece in pieces]
+        top = functools.reduce(jnp.maximum, tops)
+        acc = jnp.zeros((part, 128), F32)
+        for piece, own_top in zip(pieces, tops):
+            acc = acc + piece * jnp.exp(own_top - top)
         total = acc[:, 64:65]
         gate = jnp.where(second, gate_ref[1], gate_ref[0])
         norm_out[start:start + part, :] = acc * (1.0 / total)
@@ -200,6 +213,7 @@
         scratch_shapes=[
             pltpu.VMEM((4, 128, 768), BF16),
             pltpu.VMEM((4, 128, 768), BF16),
+            pltpu.VMEM((4, 2 * rows, 128), F32),
             pltpu.VMEM((2 * rows, 128), F32),
             pltpu.VMEM((2 * rows + 112, 128), F32),
             pltpu.VMEM((16, 128), F32),
@@ -250,17 +264,14 @@
 
 def feed_kernel(at_ref, attn_own, attn_other, wide_own, wide_other, gain_ref, conv_ref, w_ref,
                 keep_ref, send_ref, mid_out_ref, af, mid, scaled, wide_in, wg, wu, wd, sems):
-    fetches = []
-    for side, wide in enumerate((wide_own, wide_other)):
-        for i in range(4):
-            fetch = pltpu.make_async_copy(wide.at[i], wide_in.at[side, i], sems.at[3 + 4 * side + i])
-            fetch.start()
-            fetches.append(fetch)
-    copies = []
-    for k, dst in enumerate((wg, wu, wd)):
-        copy = pltpu.make_async_copy(w_ref.at[:, :, k], dst, sems.at[k])
-        copy.start()
-        copies.append(copy)
+    fetches = [
+        pltpu.make_async_copy(wide.at[i], wide_in.at[side, i], sems.at[3 + 4 * side + i])
+        for side, wide in enumerate((wide_own, wide_other))
+        for i in range(4)
+    ]
+    copies = [pltpu.make_async_copy(w_ref.at[:, :, k], dst, sems.at[k]) for k, dst in enumerate((wg, wu, wd))]
+    for fetch in fetches + copies:
+        fetch.start()
     is_first, half, core = at_ref[3], at_ref[4], at_ref[6]
     block = at_ref[5]
     rows = HALO + 512
@@ -270,7 +281,7 @@
         for x in range(4):
             af[:, pl.ds(pl.multiple_of(128 * (2 * x + c), 128), 128)] = attn[x]
     a = af[...]
-    square = jnp.zeros((rows, 1), F32)
+    square = jnp.zeros((rows, 128), F32)
     for side, (c, _, _) in enumerate(sides):
         for i, back in enumerate((0, 1, 3, 2)):
             fetches[4 * side + i].wait()
@@ -281,9 +292,10 @@
             if side == 0 and i == 0:
                 mid[...] = m
             m = m.astype(F32)
-            square = square + jnp.sum(m * m, axis=1, keepdims=True)
+            squared = m * m
+            square = square + squared[:, :128] + squared[:, 128:]
             scaled[:, cols] = (m * gain_ref[:, cols]).astype(BF16)
-    inverse = lax.rsqrt(square * (1.0 / 2048) + NORM_EPS)
+    inverse = lax.rsqrt(jnp.sum(square, axis=1, keepdims=True) * (1.0 / 2048) + NORM_EPS)
     mid_out_ref[...] = mid[pl.ds(pl.multiple_of(HALO + 256 * half, 16), 256), :]
     n = scaled[...]
     copies[0].wait()
@@ -291,25 +303,28 @@
     row = lax.broadcasted_iota(jnp.int32, (rows, 1), 0)
     keep = jnp.logical_not((row < HALO) & (is_first == 1))
 
-    def mixed(weight, index):
+    def projected(weight):
         pre = jnp.dot(n, weight[...].reshape(2048, 352), preferred_element_type=F32)
-        pre = (pre * inverse).astype(BF16).astype(F32)
-        pre = jnp.where(keep, pre, 0.0)
-        total = jnp.zeros((512, 352), F32)
+        return jnp.where(keep, (pre * inverse).astype(BF16).astype(F32), 0.0)
+
+    def mixed(pre, index, start):
+        total = jnp.zeros((256, 352), F32)
         for k in range(3):
-            total = total + conv_ref[2 * k + index:2 * k + index + 1, :] * pre[HALO - 2 + k:HALO - 2 + k + 512]
+            first = HALO - 2 + k + start
+            total = total + conv_ref[2 * k + index:2 * k + index + 1, :] * pre[first:first + 256]
         return total
 
-    gate = mixed(wg, 0)
-    up = mixed(wu, 1)
-    hidden = (gate / (1.0 + jnp.exp(-gate)) * up).astype(BF16)
+    pre_gate = projected(wg)
+    pre_up = projected(wu)
     copies[2].wait()
-    for c, _, part_ref in sides:
-        for x in range(4):
-            down = wd[pl.ds(2 * (2 * x + c), 2)].reshape(256, 352)
-            part = lax.dot_general(hidden, down, (((1,), (1,)), ((), ())), preferred_element_type=F32).astype(BF16)
-            for p in range(2):
-                part_ref[p, x] = part[256 * p:256 * (p + 1)]
+    for p in range(2):
+        gate = mixed(pre_gate, 0, 256 * p)
+        hidden = (gate / (1.0 + jnp.exp(-gate)) * mixed(pre_up, 1, 256 * p)).astype(BF16)
+        for c, _, part_ref in sides:
+            for x in range(4):
+                down = wd[pl.ds(2 * (2 * x + c), 2)].reshape(256, 352)
+                part = lax.dot_general(hidden, down, (((1,), (1,)), ((), ())), preferred_element_type=F32)
+                part_ref[p, x] = part.astype(BF16)
 
 
 def feed(at, attn, other_attn, wide, other_wide, gain, conv, weights):
@@ -400,7 +415,8 @@
     nxt = shifted(own, Z, -1)
     far_a = shifted(own[:2], Z, -2)
     far_b = shifted(own[2:], Z, 2)
-    group_q = spread(jnp.concatenate([before[:, :128], queries], axis=0), Y)
+    queries = jnp.concatenate([before[:, :128], queries], axis=0)
+    group_q = [queries] + [shifted(queries, Y, by) for by in (1, 3, 2)]
 
     queries, state = attend_own(at, cum_gate[:, 0], group_q, own)
     partial = attend_rest(at, cum_gate[:, 0], queries, state, nxt, far_a, far_b, last)

time: 228 us -> 216 us (0.947)
  the two profiles are of different devices: /device:TPU:448 before, /device:TPU:24 now
where the time goes in v3:
time: 216 us; the launch traced here: 213 us
  blocking collectives  60.7 us (28%)
  starting transfers between devices  60.5 us (28%)
  waiting for transfers between devices  49.1 us (23%)
  Pallas kernels  24.6 us (11%)
  between operations  13.7 us (6%)
  other arithmetic  4.14 us (2%)
    all_to_all x3, blocking collectives, exchanged(): return lax.all_to_all(value, axis, 0, 0, tiled=True)  47 us
    ppermute x15, starting transfers between devices, shifted(): lax.ppermute(value, axis, [(i, (i + by) % size) for i in range(size)])  46.3 us
    ppermute x15, waiting for transfers between devices, shifted(): lax.ppermute(value, axis, [(i, (i + by) % size) for i in range(size)])  38.6 us
    all_to_all x1, starting transfers between devices, exchanged(): return lax.all_to_all(value, axis, 0, 0, tiled=True)  14.2 us
    all_gather x1, blocking collectives, layer(): attn = lax.all_gather(attn, 'x', axis=0, tiled=False)  13.7 us
    pallas_call x1, Pallas kernels, feed(): pl.pallas_call(feed_kernel, out_shape=(half, half, jax.ShapeDtypeStruct((...  11.7 us
    all_to_all x1, waiting for transfers between devices, exchanged(): return lax.all_to_all(value, axis, 0, 0, tiled=True)  10.5 us
    pallas_call x1, Pallas kernels, attend_rest(): pl.pallas_call(attend_rest_kernel, out_shape=jax.ShapeDtypeStruct((4, pai...  6.26 us
  transfers between devices with their start and end apart: 17, of which 8 were waited for; matrix products, arithmetic and copies ran while one was open for 2% of the time, Pallas kernels for 5%

profile of v3, /device:TPU:24, one launch (start us, length us, event | category | flops | bytes accessed | tf_op | source)
XLA Modules:
  0.0 213.1 jit_solution(11552302871626779239)
XLA Ops:
  8.6 14.5 %all_to_all.20 = bf16[4,3,32,352]{3,2,1,0:T(8,128)(2,1)} all-to-all(bf16[4,3,32,352]{3,2,1,0:T(8,128)(2,1)} %get-tuple-element.17), channel_id=1, replica_groups=mesh['zh'=4,'zl'=4,'yh'=2,'yl'=2,'x'=4,'c'=2] {'yh','yl'}, dimensions={0} | all-to-all | bytes 540672 | tf_op jit(solution)/shard_map/all_to_all | solution.py:29
  25.0 4.0 %collective-permute-done = bf16[16,384]{1,0:T(8,128)(2,1)S(1)} collective-permute-done((bf16[16,384]{1,0:T(8,128)(2,1)}, bf16[16,384]{1,0:T(8,128)(2,1)S(1)}, u32[]{:S(2)}, u32[]{:S(2)}) %collective-permute-start) | collective-permute-done | bytes 12320 | tf_op jit(solution)/shard_map/ppermute | solution.py:25
  30.0 2.3 %collective-permute-start.9 = (bf16[272,256]{1,0:T(8,128)(2,1)S(1)}, bf16[272,256]{1,0:T(8,128)(2,1)S(1)}, u32[]{:S(2)}, u32[]{:S(2)}) collective-permute-start(bf16[272,256]{1,0:T(8,128)(2,1)S(1)} %pad_maximum_fusion.5), channel_id=1, source_target_pairs={{0,8},{8,0},{1,9},{9,1},{2,10},{10,2},{3,11},{11,3},{4,12},{12,4},... | collective-permute-start | bytes 417800 | tf_op jit(solution)/shard_map/ppermute | solution.py:25
  32.2 4.7 %collective-permute-done.9 = bf16[272,256]{1,0:T(8,128)(2,1)S(1)} collective-permute-done((bf16[272,256]{1,0:T(8,128)(2,1)S(1)}, bf16[272,256]{1,0:T(8,128)(2,1)S(1)}, u32[]{:S(2)}, u32[]{:S(2)}) %collective-permute-start.9) | collective-permute-done | bytes 139296 | tf_op jit(solution)/shard_map/ppermute | solution.py:25
  39.0 2.3 %collective-permute-start.11 = (bf16[1552,256]{1,0:T(8,128)(2,1)S(1)}, bf16[1552,256]{1,0:T(8,128)(2,1)S(1)}, u32[]{:S(2)}, u32[]{:S(2)}) collective-permute-start(bf16[1552,256]{1,0:T(8,128)(2,1)S(1)} %fusion.2), channel_id=1, source_target_pairs={{0,6},{2,0},{4,2},{6,4},{1,7},{3,1},{5,3},{7,5},{8,14},{10,8},{12,... | collective-permute-start | bytes 2383880 | tf_op jit(solution)/shard_map/ppermute | solution.py:25
  41.3 3.5 %collective-permute-start.10 = (bf16[1552,256]{1,0:T(8,128)(2,1)S(1)}, bf16[1552,256]{1,0:T(8,128)(2,1)S(1)}, u32[]{:S(2)}, u32[]{:S(2)}) collective-permute-start(bf16[1552,256]{1,0:T(8,128)(2,1)S(1)} %fusion.2), channel_id=1, source_target_pairs={{0,2},{2,4},{4,6},{6,0},{1,3},{3,5},{5,7},{7,1},{8,10},{10,12},{12... | collective-permute-start | bytes 2383880 | tf_op jit(solution)/shard_map/ppermute | solution.py:25
  44.9 16.1 %collective-permute-done.12 = bf16[1552,256]{1,0:T(8,128)(2,1)S(1)} collective-permute-done((bf16[1552,256]{1,0:T(8,128)(2,1)S(1)}, bf16[1552,256]{1,0:T(8,128)(2,1)S(1)}, u32[]{:S(2)}, u32[]{:S(2)}) %collective-permute-start.12) | collective-permute-done | bytes 794656 | tf_op jit(solution)/shard_map/ppermute | solution.py:25
  61.1 8.8 %collective-permute-done.11 = bf16[1552,256]{1,0:T(8,128)(2,1)S(1)} collective-permute-done((bf16[1552,256]{1,0:T(8,128)(2,1)S(1)}, bf16[1552,256]{1,0:T(8,128)(2,1)S(1)}, u32[]{:S(2)}, u32[]{:S(2)}) %collective-permute-start.11) | collective-permute-done | bytes 794656 | tf_op jit(solution)/shard_map/ppermute | solution.py:25
  73.7 14.2 %all-to-all-start = ((bf16[4,136,256]{2,1,0:T(8,128)(2,1)}), bf16[4,136,256]{2,1,0:T(8,128)(2,1)S(1)}, u32[]{:S(2)}, u32[]{:S(2)}) async-start(bf16[4,136,256]{2,1,0:T(8,128)(2,1)} %get-tuple-element.14), calls=%async_computation | async-start | bytes 557056 | tf_op jit(solution)/shard_map/all_to_all | solution.py:29
  88.0 6.5 %collective-permute-start.3 = (bf16[272,128]{1,0:T(8,128)(2,1)S(1)}, bf16[272,128]{1,0:T(8,128)(2,1)S(1)}, u32[]{:S(2)}, u32[]{:S(2)}) collective-permute-start(bf16[272,128]{1,0:T(8,128)(2,1)S(1)} %pad_maximum_fusion.6.q0_ref), channel_id=1, source_target_pairs={{0,16},{8,24},{16,0},{24,8},{1,17},{9,25},{17,1},{25,9},{2,18},{10... | collective-permute-start | bytes 208904 | tf_op jit(solution)/shard_map/ppermute | solution.py:25
  94.6 3.0 %collective-permute-start.2 = (bf16[272,128]{1,0:T(8,128)(2,1)S(1)}, bf16[272,128]{1,0:T(8,128)(2,1)S(1)}, u32[]{:S(2)}, u32[]{:S(2)}) collective-permute-start(bf16[272,128]{1,0:T(8,128)(2,1)S(1)} %pad_maximum_fusion.6.q0_ref), channel_id=1, source_target_pairs={{0,24},{8,0},{16,8},{24,16},{1,25},{9,1},{17,9},{25,17},{2,26},{10... | collective-permute-start | bytes 208904 | tf_op jit(solution)/shard_map/ppermute | solution.py:25
  97.7 4.0 %collective-permute-start.1 = (bf16[272,128]{1,0:T(8,128)(2,1)S(1)}, bf16[272,128]{1,0:T(8,128)(2,1)S(1)}, u32[]{:S(2)}, u32[]{:S(2)}) collective-permute-start(bf16[272,128]{1,0:T(8,128)(2,1)S(1)} %pad_maximum_fusion.6.q0_ref), channel_id=1, source_target_pairs={{0,8},{8,16},{16,24},{24,0},{1,9},{9,17},{17,25},{25,1},{2,10},{10... | collective-permute-start | bytes 208904 | tf_op jit(solution)/shard_map/ppermute | solution.py:25
  101.7 10.5 %all-to-all-done.own_ref = bf16[4,136,256]{2,1,0:T(8,128)(2,1)S(1)} async-done(((bf16[4,136,256]{2,1,0:T(8,128)(2,1)}), bf16[4,136,256]{2,1,0:T(8,128)(2,1)S(1)}, u32[]{:S(2)}, u32[]{:S(2)}) %all-to-all-start) | async-done | bytes 278560 | tf_op jit(solution)/shard_map/all_to_all | solution.py:29
  112.2 3.8 %collective-permute-start.7 = (bf16[4,136,256]{2,1,0:T(8,128)(2,1)S(1)}, bf16[4,136,256]{2,1,0:T(8,128)(2,1)S(1)}, u32[]{:S(2)}, u32[]{:S(2)}) collective-permute-start(bf16[4,136,256]{2,1,0:T(8,128)(2,1)S(1)} %all-to-all-done.own_ref), channel_id=1, source_target_pairs={{0,32},{32,64},{64,96},{96,128},{128,160},{160,192},{192,224},{224... | collective-permute-start | bytes 835592 | tf_op jit(solution)/shard_map/ppermute | solution.py:25
  115.9 3.3 %collective-permute-start.4 = (bf16[4,136,256]{2,1,0:T(8,128)(2,1)S(1)}, bf16[4,136,256]{2,1,0:T(8,128)(2,1)S(1)}, u32[]{:S(2)}, u32[]{:S(2)}) collective-permute-start(bf16[4,136,256]{2,1,0:T(8,128)(2,1)S(1)} %all-to-all-done.own_ref), channel_id=1, source_target_pairs={{0,480},{32,0},{64,32},{96,64},{128,96},{160,128},{192,160},{224,1... | collective-permute-start | bytes 835592 | tf_op jit(solution)/shard_map/ppermute | solution.py:25
  119.3 2.6 %collective-permute-start.6 = (bf16[2,136,256]{2,1,0:T(8,128)(2,1)S(1)}, bf16[2,136,256]{2,1,0:T(8,128)(2,1)S(1)}, u32[]{:S(2)}, u32[]{:S(2)}) collective-permute-start(bf16[2,136,256]{2,1,0:T(8,128)(2,1)S(1)} %get-tuple-element.21), channel_id=1, source_target_pairs={{0,64},{32,96},{64,128},{96,160},{128,192},{160,224},{192,256},{22... | collective-permute-start | bytes 417800 | tf_op jit(solution)/shard_map/ppermute | solution.py:25
  121.9 5.4 %collective-permute-start.5 = (bf16[2,136,256]{2,1,0:T(8,128)(2,1)S(1)}, bf16[2,136,256]{2,1,0:T(8,128)(2,1)S(1)}, u32[]{:S(2)}, u32[]{:S(2)}) collective-permute-start(bf16[2,136,256]{2,1,0:T(8,128)(2,1)S(1)} %get-tuple-element.22), channel_id=1, source_target_pairs={{0,448},{32,480},{64,0},{96,32},{128,64},{160,96},{192,128},{224,1... | collective-permute-start | bytes 417800 | tf_op jit(solution)/shard_map/ppermute | solution.py:25
  127.2 3.9 %attend_own.1 = (bf16[2080,128]{1,0:T(8,128)(2,1)S(1)}, f32[2080,128]{1,0:T(8,128)S(1)}) custom-call(s32[7]{0:T(128)S(1)} %stack.48.at_ref, f32[2]{0:T(128)S(1)} %slice_reduce_fusion.gate_ref, bf16[272,128]{1,0:T(8,128)(2,1)S(1)} %pad_maximum_fusion.6.q0_ref, bf16[272,128]{1,0:T(8,128)(2,1)S(1)} %collective-permute-done.1.q1_ref, ...), custom_call_target="tpu_custom_call" | custom-call | flops 2000000000 | bytes 1048576 | tf_op jit(solution)/shard_map/attend_own/pallas_call | solution.py:126
  131.8 6.3 %attend_rest.1 = bf16[4,576,128]{2,1,0:T(8,128)(2,1)S(1)} custom-call(s32[7]{0:T(128)S(1)} %stack.48.at_ref, f32[2]{0:T(128)S(1)} %slice_reduce_fusion.gate_ref, bf16[2080,128]{1,0:T(8,128)(2,1)S(1)} %get-tuple-element.15.qa, f32[2080,128]{1,0:T(8,128)S(1)} %get-tuple-element.16.state_ref, bf16[4,136,256]{2,1,0:T(8,128)(2,1)S(1)} %collective-permute-done.4.next_ref, ...), custom_call_target="tpu_custom_call" | custom-call | flops 6000000000 | bytes 4194304 | tf_op jit(solution)/shard_map/attend_rest/pallas_call | solution.py:208
  138.1 13.6 %all_to_all.21.in_ref = bf16[4,576,128]{2,1,0:T(8,128)(2,1)S(1)} all-to-all(bf16[4,576,128]{2,1,0:T(8,128)(2,1)S(1)} %attend_rest.1), channel_id=1, replica_groups=mesh['zh'=4,'zl'=4,'yh'=2,'yl'=2,'x'=4,'c'=2] {'yh','yl'}, dimensions={0} | all-to-all | bytes 1179648 | tf_op jit(solution)/shard_map/all_to_all | solution.py:29
  152.4 13.7 %all-gather = bf16[2112,128]{1,0:T(8,128)(2,1)S(1)} all-gather(bf16[528,128]{1,0:T(8,128)(2,1)S(1)} %merge.1), channel_id=2, replica_groups=mesh['zh'=4,'zl'=4,'yh'=2,'yl'=2,'x'=4,'c'=2] {'x'}, dimensions={0}, use_global_device_ids=true | all-gather | bytes 675840 | tf_op jit(solution)/shard_map/all_gather | solution.py:427
  169.9 11.7 %feed.1 = (bf16[2,4,256,256]{3,2,1,0:T(8,128)(2,1)S(1)}, bf16[2,4,256,256]{3,2,1,0:T(8,128)(2,1)S(1)}, bf16[256,256]{1,0:T(8,128)(2,1)S(1)}) custom-call(s32[7]{0:T(128)S(1)} %stack.48.at_ref, bf16[4,528,128]{2,1,0:T(8,128)(2,1)S(1)} %bitcast.23, bf16[4,528,128]{2,1,0:T(8,128)(2,1)S(1)} %collective-permute-done.8.attn_other, ...), custom_call_target="tpu_custom_call" | custom-call | flops 5000000000 | bytes 16777216 | tf_op jit(solution)/shard_map/feed/pallas_call | solution.py:336
  183.7 2.5 %collective-permute-done.14 = bf16[2,4,256,256]{3,2,1,0:T(8,128)(2,1)S(1)} collective-permute-done((bf16[2,4,256,256]{3,2,1,0:T(8,128)(2,1)S(1)}, bf16[2,4,256,256]{3,2,1,0:T(8,128)(2,1)S(1)}, u32[]{:S(2)}, u32[]{:S(2)}) %collective-permute-start.14) | collective-permute-done | bytes 1048608 | tf_op jit(solution)/shard_map/ppermute | solution.py:25
  186.5 18.9 %all_to_all.22 = bf16[8,256,256]{2,1,0:T(8,128)(2,1)S(1)} all-to-all(bf16[8,256,256]{2,1,0:T(8,128)(2,1)S(1)} %bitcast.25), channel_id=1, replica_groups=mesh['zh'=4,'zl'=4,'yh'=2,'yl'=2,'x'=4,'c'=2] {'yl','x'}, dimensions={0} | all-to-all | bytes 2097152 | tf_op jit(solution)/shard_map/all_to_all | solution.py:29
  (48 shorter events, 19.4 us)
Async XLA Ops:
  6.5 30.4 %copy-start.1 = (bf16[256,256]{1,0:T(8,128)(2,1)S(1)}, bf16[256,256]{1,0:T(8,128)(2,1)}, u32[]{:S(2)}) copy-start(bf16[256,256]{1,0:T(8,128)(2,1)} %resid_ref.1) | copy-start | bytes 393220
  6.5 30.4 %copy-start.2 = (bf16[1024,256]{1,0:T(8,128)(2,1)S(1)}, bf16[1024,256]{1,0:T(8,128)(2,1)}, u32[]{:S(2)}) copy-start(bf16[1024,256]{1,0:T(8,128)(2,1)} %param.14) | copy-start | bytes 1572868
  6.5 163.3 %all-gather.4.cloned.1.call-start = ((), (), s32[]{:S(2)}) async-start(), calls=%async_computation.4 | async-start | bytes 5013504 | tf_op jit(solution)/shard_map/all_gather | solution.py:406
  23.1 5.9 %collective-permute-start = (bf16[16,384]{1,0:T(8,128)(2,1)}, bf16[16,384]{1,0:T(8,128)(2,1)S(1)}, u32[]{:S(2)}, u32[]{:S(2)}) collective-permute-start(bf16[16,384]{1,0:T(8,128)(2,1)} %get-tuple-element.13), channel_id=1, source_target_pairs={{0,8},{8,16},{16,24},{24,32},{32,40},{40,48},{48,56},{56,64},{64,7... | collective-permute-start | bytes 36872 | tf_op jit(solution)/shard_map/ppermute | solution.py:25
  30.0 6.9 %collective-permute-start.9 = (bf16[272,256]{1,0:T(8,128)(2,1)S(1)}, bf16[272,256]{1,0:T(8,128)(2,1)S(1)}, u32[]{:S(2)}, u32[]{:S(2)}) collective-permute-start(bf16[272,256]{1,0:T(8,128)(2,1)S(1)} %pad_maximum_fusion.5), channel_id=1, source_target_pairs={{0,8},{8,0},{1,9},{9,1},{2,10},{10,2},{3,11},{11,3},{4,12},{12,4},... | collective-permute-start | bytes 417800 | tf_op jit(solution)/shard_map/ppermute | solution.py:25
  37.1 24.0 %collective-permute-start.12 = (bf16[1552,256]{1,0:T(8,128)(2,1)S(1)}, bf16[1552,256]{1,0:T(8,128)(2,1)S(1)}, u32[]{:S(2)}, u32[]{:S(2)}) collective-permute-start(bf16[1552,256]{1,0:T(8,128)(2,1)S(1)} %fusion.2), channel_id=1, source_target_pairs={{0,4},{2,6},{4,0},{6,2},{1,5},{3,7},{5,1},{7,3},{8,12},{10,14},{12... | collective-permute-start | bytes 2383880 | tf_op jit(solution)/shard_map/ppermute | solution.py:25
  39.0 30.9 %collective-permute-start.11 = (bf16[1552,256]{1,0:T(8,128)(2,1)S(1)}, bf16[1552,256]{1,0:T(8,128)(2,1)S(1)}, u32[]{:S(2)}, u32[]{:S(2)}) collective-permute-start(bf16[1552,256]{1,0:T(8,128)(2,1)S(1)} %fusion.2), channel_id=1, source_target_pairs={{0,6},{2,0},{4,2},{6,4},{1,7},{3,1},{5,3},{7,5},{8,14},{10,8},{12,... | collective-permute-start | bytes 2383880 | tf_op jit(solution)/shard_map/ppermute | solution.py:25
  41.3 28.6 %collective-permute-start.10 = (bf16[1552,256]{1,0:T(8,128)(2,1)S(1)}, bf16[1552,256]{1,0:T(8,128)(2,1)S(1)}, u32[]{:S(2)}, u32[]{:S(2)}) collective-permute-start(bf16[1552,256]{1,0:T(8,128)(2,1)S(1)} %fusion.2), channel_id=1, source_target_pairs={{0,2},{2,4},{4,6},{6,0},{1,3},{3,5},{5,7},{7,1},{8,10},{10,12},{12... | collective-permute-start | bytes 2383880 | tf_op jit(solution)/shard_map/ppermute | solution.py:25
  69.9 18.1 %copy-start.3 = (bf16[256,128]{1,0:T(8,128)(2,1)S(1)}, bf16[256,128]{1,0:T(8,128)(2,1)}, u32[]{:S(2)}) copy-start(bf16[256,128]{1,0:T(8,128)(2,1)} %q_ref.1) | copy-start | bytes 196612
  69.9 24.6 %copy-start.5 = (f32[2,256]{1,0:T(2,128)S(1)}, f32[2,256]{1,0:T(2,128)}, u32[]{:S(2)}) copy-start(f32[2,256]{1,0:T(2,128)} %decay_ref.1) | copy-start | bytes 6148
  71.8 98.1 %collective-permute-start.13 = (bf16[4,1552,256]{2,1,0:T(8,128)(2,1)}, bf16[4,1552,256]{2,1,0:T(8,128)(2,1)}, u32[]{:S(2)}, u32[]{:S(2)}) collective-permute-start(bf16[4,1552,256]{2,1,0:T(8,128)(2,1)} %pad_maximum_fusion.wide_own), channel_id=1, source_target_pairs={{0,1},{1,0},{2,3},{3,2},{4,5},{5,4},{6,7},{7,6},{8,9},{9,8},{10,11... | collective-permute-start | bytes 9535496 | tf_op jit(solution)/shard_map/ppermute | solution.py:25
  73.7 38.5 %all-to-all-start = ((bf16[4,136,256]{2,1,0:T(8,128)(2,1)}), bf16[4,136,256]{2,1,0:T(8,128)(2,1)S(1)}, u32[]{:S(2)}, u32[]{:S(2)}) async-start(bf16[4,136,256]{2,1,0:T(8,128)(2,1)} %get-tuple-element.14), calls=%async_computation | async-start | bytes 557056 | tf_op jit(solution)/shard_map/all_to_all | solution.py:29
  88.0 27.9 %collective-permute-start.3 = (bf16[272,128]{1,0:T(8,128)(2,1)S(1)}, bf16[272,128]{1,0:T(8,128)(2,1)S(1)}, u32[]{:S(2)}, u32[]{:S(2)}) collective-permute-start(bf16[272,128]{1,0:T(8,128)(2,1)S(1)} %pad_maximum_fusion.6.q0_ref), channel_id=1, source_target_pairs={{0,16},{8,24},{16,0},{24,8},{1,17},{9,25},{17,1},{25,9},{2,18},{10... | collective-permute-start | bytes 208904 | tf_op jit(solution)/shard_map/ppermute | solution.py:25
  94.6 24.6 %collective-permute-start.2 = (bf16[272,128]{1,0:T(8,128)(2,1)S(1)}, bf16[272,128]{1,0:T(8,128)(2,1)S(1)}, u32[]{:S(2)}, u32[]{:S(2)}) collective-permute-start(bf16[272,128]{1,0:T(8,128)(2,1)S(1)} %pad_maximum_fusion.6.q0_ref), channel_id=1, source_target_pairs={{0,24},{8,0},{16,8},{24,16},{1,25},{9,1},{17,9},{25,17},{2,26},{10... | collective-permute-start | bytes 208904 | tf_op jit(solution)/shard_map/ppermute | solution.py:25
  97.7 24.2 %collective-permute-start.1 = (bf16[272,128]{1,0:T(8,128)(2,1)S(1)}, bf16[272,128]{1,0:T(8,128)(2,1)S(1)}, u32[]{:S(2)}, u32[]{:S(2)}) collective-permute-start(bf16[272,128]{1,0:T(8,128)(2,1)S(1)} %pad_maximum_fusion.6.q0_ref), channel_id=1, source_target_pairs={{0,8},{8,16},{16,24},{24,0},{1,9},{9,17},{17,25},{25,1},{2,10},{10... | collective-permute-start | bytes 208904 | tf_op jit(solution)/shard_map/ppermute | solution.py:25
  112.2 19.7 %collective-permute-start.7 = (bf16[4,136,256]{2,1,0:T(8,128)(2,1)S(1)}, bf16[4,136,256]{2,1,0:T(8,128)(2,1)S(1)}, u32[]{:S(2)}, u32[]{:S(2)}) collective-permute-start(bf16[4,136,256]{2,1,0:T(8,128)(2,1)S(1)} %all-to-all-done.own_ref), channel_id=1, source_target_pairs={{0,32},{32,64},{64,96},{96,128},{128,160},{160,192},{192,224},{224... | collective-permute-start | bytes 835592 | tf_op jit(solution)/shard_map/ppermute | solution.py:25
  115.9 15.9 %collective-permute-start.4 = (bf16[4,136,256]{2,1,0:T(8,128)(2,1)S(1)}, bf16[4,136,256]{2,1,0:T(8,128)(2,1)S(1)}, u32[]{:S(2)}, u32[]{:S(2)}) collective-permute-start(bf16[4,136,256]{2,1,0:T(8,128)(2,1)S(1)} %all-to-all-done.own_ref), channel_id=1, source_target_pairs={{0,480},{32,0},{64,32},{96,64},{128,96},{160,128},{192,160},{224,1... | collective-permute-start | bytes 835592 | tf_op jit(solution)/shard_map/ppermute | solution.py:25
  119.3 11.9 %collective-permute-start.6 = (bf16[2,136,256]{2,1,0:T(8,128)(2,1)S(1)}, bf16[2,136,256]{2,1,0:T(8,128)(2,1)S(1)}, u32[]{:S(2)}, u32[]{:S(2)}) collective-permute-start(bf16[2,136,256]{2,1,0:T(8,128)(2,1)S(1)} %get-tuple-element.21), channel_id=1, source_target_pairs={{0,64},{32,96},{64,128},{96,160},{128,192},{160,224},{192,256},{22... | collective-permute-start | bytes 417800 | tf_op jit(solution)/shard_map/ppermute | solution.py:25
  121.9 10.0 %collective-permute-start.5 = (bf16[2,136,256]{2,1,0:T(8,128)(2,1)S(1)}, bf16[2,136,256]{2,1,0:T(8,128)(2,1)S(1)}, u32[]{:S(2)}, u32[]{:S(2)}) collective-permute-start(bf16[2,136,256]{2,1,0:T(8,128)(2,1)S(1)} %get-tuple-element.22), channel_id=1, source_target_pairs={{0,448},{32,480},{64,0},{96,32},{128,64},{160,96},{192,128},{224,1... | collective-permute-start | bytes 417800 | tf_op jit(solution)/shard_map/ppermute | solution.py:25
  138.1 29.9 %copy-start.4 = (f32[3,2,704]{2,1,0:T(2,128)S(1)}, f32[3,2,704]{2,1,0:T(2,128)}, u32[]{:S(2)}) copy-start(f32[3,2,704]{2,1,0:T(2,128)} %param.18) | copy-start | bytes 50692
  138.1 31.8 %copy-start = (f32[2048]{0:T(1024)S(1)}, f32[2048]{0:T(1024)}, u32[]{:S(2)}) copy-start(f32[2048]{0:T(1024)} %param.15) | copy-start | bytes 24580
  166.1 3.8 %collective-permute-start.8 = (bf16[4,528,128]{2,1,0:T(8,128)(2,1)S(1)}, bf16[4,528,128]{2,1,0:T(8,128)(2,1)S(1)}, u32[]{:S(2)}, u32[]{:S(2)}) collective-permute-start(bf16[4,528,128]{2,1,0:T(8,128)(2,1)S(1)} %bitcast.22), channel_id=1, source_target_pairs={{0,1},{1,0},{2,3},{3,2},{4,5},{5,4},{6,7},{7,6},{8,9},{9,8},{10,11... | collective-permute-start | bytes 1622024 | tf_op jit(solution)/shard_map/ppermute | solution.py:25
  181.6 4.6 %collective-permute-start.14 = (bf16[2,4,256,256]{3,2,1,0:T(8,128)(2,1)S(1)}, bf16[2,4,256,256]{3,2,1,0:T(8,128)(2,1)S(1)}, u32[]{:S(2)}, u32[]{:S(2)}) collective-permute-start(bf16[2,4,256,256]{3,2,1,0:T(8,128)(2,1)S(1)} %get-tuple-element.20), channel_id=1, source_target_pairs={{0,1},{1,0},{2,3},{3,2},{4,5},{5,4},{6,7},{7,6},{8,9},{9,8},{10,11... | collective-permute-start | bytes 3145736 | tf_op jit(solution)/shard_map/ppermute | solution.py:25
Sparse Core Ops, SparseCore 0:
  23.2 87.6 all-gather.3

commit v4 on v3

--- a/solution.py
+++ b/solution.py
@@ -27,6 +27,11 @@
 
 def exchanged(value, axis):
     return lax.all_to_all(value, axis, 0, 0, tiled=True)
+
+
+def spread(value, axis):
+    size = lax.axis_size(axis)
+    return exchanged(jnp.broadcast_to(value[None], (size, *value.shape)), axis)
 
 
 def split3(value):
@@ -81,8 +86,7 @@
     return part, blocks
 
 
-def attend_own_kernel(at_ref, gate_ref, q0_ref, q1_ref, q2_ref, q3_ref, own_ref, qa, state_ref, ka, va):
-    q_refs = (q0_ref, q1_ref, q2_ref, q3_ref)
+def attend_own_kernel(at_ref, gate_ref, q_ref, own_ref, qa, state_ref, ka, va):
     zh, zl, y = at_ref[0], at_ref[1], at_ref[2]
     z = 4 * zh + zl
     rows = HALO + 1024
@@ -95,17 +99,11 @@
             first = 64 + 3 * head
             ones = jnp.where((lane >= first) & (lane < first + 3), 1.0, 0.0)
             both = jnp.where(lane < 64, side, ones)
-            first_row = pl.multiple_of(head * rows + start, HALO)
-            qa[pl.ds(first_row, piece.shape[0]), :] = both.astype(BF16)
-
-    for back, q_ref in zip((0, 1, 3, 2), q_refs):
-        from_y = jnp.where(y >= back, y - back, y - back + 4)
-        put_queries(HALO + 256 * from_y, q_ref[HALO:HALO + 256, :])
-
-        @pl.when(from_y == 0)
-        def _(q_ref=q_ref):
-            put_queries(0, q_ref[0:HALO, :])
-
+            qa[head * rows + start:head * rows + start + piece.shape[0], :] = both.astype(BF16)
+
+    put_queries(0, q_ref[0, 0:HALO, :])
+    for i in range(4):
+        put_queries(HALO + 256 * i, q_ref[i, HALO:HALO + 256, :])
     for chunk in range(4):
         put_keys(ka, va, 0, chunk, own_ref[chunk], gate_ref)
     key_lane = lax.broadcasted_iota(jnp.int32, (1, 1024), 1)
@@ -126,13 +124,13 @@
     return pl.pallas_call(
         attend_own_kernel,
         out_shape=(jax.ShapeDtypeStruct((2 * rows, 128), BF16), jax.ShapeDtypeStruct((2 * rows, 128), F32)),
-        in_specs=[smem, smem] + [vmem] * 5,
+        in_specs=[smem, smem, vmem, vmem],
         out_specs=(vmem, vmem),
         scratch_shapes=[pltpu.VMEM((1, 128, 1024), BF16), pltpu.VMEM((1, 128, 1024), BF16)],
         compiler_params=pltpu.CompilerParams(vmem_limit_bytes=30 * 2**20),
         cost_estimate=pl.CostEstimate(flops=2 * 10**9, bytes_accessed=2**20, transcendentals=2 * 10**6),
         name="attend_own",
-    )(at, gate, *queries, own)
+    )(at, gate, queries, own)
 
 
 def attend_rest_kernel(at_ref, gate_ref, qa, state_ref, next_ref, far_a_ref, far_b_ref, last_ref,
@@ -410,13 +408,13 @@
     low = jnp.concatenate([out_weight, mine, theirs[HALO:]], axis=0)
     high = jnp.concatenate([out_weight, theirs, mine[HALO:]], axis=0)
     wide = jnp.where(half == 0, low, high)
-    wides = [wide] + [shifted(wide, "x", by) for by in (1, 3, 2)]
+    wides = [wide, shifted(wide, "x", 1), shifted(wide, "x", 3)]
+    wides.append(shifted(wide, "x", 2))
     last = shifted(own, Z, 1)
     nxt = shifted(own, Z, -1)
     far_a = shifted(own[:2], Z, -2)
     far_b = shifted(own[2:], Z, 2)
-    queries = jnp.concatenate([before[:, :128], queries], axis=0)
-    group_q = [queries] + [shifted(queries, Y, by) for by in (1, 3, 2)]
+    group_q = spread(jnp.concatenate([before[:, :128], queries], axis=0), Y)
 
     queries, state = attend_own(at, cum_gate[:, 0], group_q, own)
     partial = attend_rest(at, cum_gate[:, 0], queries, state, nxt, far_a, far_b, last)

time: 216 us -> 222 us (1.028)
  waiting for transfers between devices: 49.1 us -> 62.9 us
  starting transfers between devices: 60.5 us -> 53.5 us
    all_to_all x1 -> x2, waiting for transfers between devices: 10.5 us -> 24 us  [exchanged(): return lax.all_to_all(value, axis, 0, 0, tiled=True)]
    ppermute x15 -> x12, starting transfers between devices: 46.3 us -> 32.8 us  [shifted(): lax.ppermute(value, axis, [(i, (i + by) % size) for i in range(size)])]
    all_to_all x1 -> x2, starting transfers between devices: 14.2 us -> 20.7 us  [exchanged(): return lax.all_to_all(value, axis, 0, 0, tiled=True)]
    ppermute x15 -> x12, waiting for transfers between devices: 38.6 us -> 38.9 us  [shifted(): lax.ppermute(value, axis, [(i, (i + by) % size) for i in range(size)])]
  transfers between devices with their start and end apart: 17 -> 15, of which waited for: 8 -> 8; matrix products, arithmetic and copies ran while one was open for 2% -> 2% of each run, Pallas kernels for 5% -> 5%
where the time goes in v4:
time: 222 us; the launch traced here: 219 us
  waiting for transfers between devices  62.9 us (28%)
  blocking collectives  59.3 us (27%)
  starting transfers between devices  53.5 us (24%)
  Pallas kernels  24.2 us (11%)
  between operations  13.7 us (6%)
  other arithmetic  4.15 us (2%)
    all_to_all x3, blocking collectives, exchanged(): return lax.all_to_all(value, axis, 0, 0, tiled=True)  46.1 us
    ppermute x12, waiting for transfers between devices, shifted(): lax.ppermute(value, axis, [(i, (i + by) % size) for i in range(size)])  38.9 us
    ppermute x12, starting transfers between devices, shifted(): lax.ppermute(value, axis, [(i, (i + by) % size) for i in range(size)])  32.8 us
    all_to_all x2, waiting for transfers between devices, exchanged(): return lax.all_to_all(value, axis, 0, 0, tiled=True)  24 us
    all_to_all x2, starting transfers between devices, exchanged(): return lax.all_to_all(value, axis, 0, 0, tiled=True)  20.7 us
    all_gather x1, blocking collectives, layer(): attn = lax.all_gather(attn, 'x', axis=0, tiled=False)  13.1 us
    pallas_call x1, Pallas kernels, feed(): pl.pallas_call(feed_kernel, out_shape=(half, half, jax.ShapeDtypeStruct((...  11.7 us
    pallas_call x1, Pallas kernels, attend_rest(): pl.pallas_call(attend_rest_kernel, out_shape=jax.ShapeDtypeStruct((4, pai...  6.26 us
  transfers between devices with their start and end apart: 15, of which 8 were waited for; matrix products, arithmetic and copies ran while one was open for 2% of the time, Pallas kernels for 5%

profile of v4, /device:TPU:24, one launch (start us, length us, event | category | flops | bytes accessed | tf_op | source)
XLA Modules:
  0.0 218.8 jit_solution(11969961924402245640)
XLA Ops:
  6.5 2.0 prepare.1
  8.6 14.5 %all_to_all.25 = bf16[4,3,32,352]{3,2,1,0:T(8,128)(2,1)} all-to-all(bf16[4,3,32,352]{3,2,1,0:T(8,128)(2,1)} %get-tuple-element.17), channel_id=1, replica_groups=mesh['zh'=4,'zl'=4,'yh'=2,'yl'=2,'x'=4,'c'=2] {'yh','yl'}, dimensions={0} | all-to-all | bytes 540672 | tf_op jit(solution)/shard_map/all_to_all | solution.py:29
  25.0 4.0 %collective-permute-done = bf16[16,384]{1,0:T(8,128)(2,1)S(1)} collective-permute-done((bf16[16,384]{1,0:T(8,128)(2,1)}, bf16[16,384]{1,0:T(8,128)(2,1)S(1)}, u32[]{:S(2)}, u32[]{:S(2)}) %collective-permute-start) | collective-permute-done | bytes 12320 | tf_op jit(solution)/shard_map/ppermute | solution.py:25
  30.0 2.3 %collective-permute-start.6 = (bf16[272,256]{1,0:T(8,128)(2,1)S(1)}, bf16[272,256]{1,0:T(8,128)(2,1)S(1)}, u32[]{:S(2)}, u32[]{:S(2)}) collective-permute-start(bf16[272,256]{1,0:T(8,128)(2,1)S(1)} %pad_maximum_fusion.5), channel_id=1, source_target_pairs={{0,8},{8,0},{1,9},{9,1},{2,10},{10,2},{3,11},{11,3},{4,12},{12,4},... | collective-permute-start | bytes 417800 | tf_op jit(solution)/shard_map/ppermute | solution.py:25
  32.2 4.7 %collective-permute-done.6 = bf16[272,256]{1,0:T(8,128)(2,1)S(1)} collective-permute-done((bf16[272,256]{1,0:T(8,128)(2,1)S(1)}, bf16[272,256]{1,0:T(8,128)(2,1)S(1)}, u32[]{:S(2)}, u32[]{:S(2)}) %collective-permute-start.6) | collective-permute-done | bytes 139296 | tf_op jit(solution)/shard_map/ppermute | solution.py:25
  37.1 1.9 collective-permute-start.9
  39.0 2.3 %collective-permute-start.8 = (bf16[1552,256]{1,0:T(8,128)(2,1)S(1)}, bf16[1552,256]{1,0:T(8,128)(2,1)S(1)}, u32[]{:S(2)}, u32[]{:S(2)}) collective-permute-start(bf16[1552,256]{1,0:T(8,128)(2,1)S(1)} %fusion.2), channel_id=1, source_target_pairs={{0,6},{2,0},{4,2},{6,4},{1,7},{3,1},{5,3},{7,5},{8,14},{10,8},{12,... | collective-permute-start | bytes 2383880 | tf_op jit(solution)/shard_map/ppermute | solution.py:25
  41.3 3.5 %collective-permute-start.7 = (bf16[1552,256]{1,0:T(8,128)(2,1)S(1)}, bf16[1552,256]{1,0:T(8,128)(2,1)S(1)}, u32[]{:S(2)}, u32[]{:S(2)}) collective-permute-start(bf16[1552,256]{1,0:T(8,128)(2,1)S(1)} %fusion.2), channel_id=1, source_target_pairs={{0,2},{2,4},{4,6},{6,0},{1,3},{3,5},{5,7},{7,1},{8,10},{10,12},{12... | collective-permute-start | bytes 2383880 | tf_op jit(solution)/shard_map/ppermute | solution.py:25
  44.9 16.1 %collective-permute-done.9 = bf16[1552,256]{1,0:T(8,128)(2,1)S(1)} collective-permute-done((bf16[1552,256]{1,0:T(8,128)(2,1)S(1)}, bf16[1552,256]{1,0:T(8,128)(2,1)S(1)}, u32[]{:S(2)}, u32[]{:S(2)}) %collective-permute-start.9) | collective-permute-done | bytes 794656 | tf_op jit(solution)/shard_map/ppermute | solution.py:25
  61.1 8.8 %collective-permute-done.8 = bf16[1552,256]{1,0:T(8,128)(2,1)S(1)} collective-permute-done((bf16[1552,256]{1,0:T(8,128)(2,1)S(1)}, bf16[1552,256]{1,0:T(8,128)(2,1)S(1)}, u32[]{:S(2)}, u32[]{:S(2)}) %collective-permute-start.8) | collective-permute-done | bytes 794656 | tf_op jit(solution)/shard_map/ppermute | solution.py:25
  73.7 14.2 %all-to-all-start.1 = ((bf16[4,136,256]{2,1,0:T(8,128)(2,1)}), bf16[4,136,256]{2,1,0:T(8,128)(2,1)S(1)}, u32[]{:S(2)}, u32[]{:S(2)}) async-start(bf16[4,136,256]{2,1,0:T(8,128)(2,1)} %get-tuple-element.14), calls=%async_computation.1 | async-start | bytes 557056 | tf_op jit(solution)/shard_map/all_to_all | solution.py:29
  88.1 24.0 %all-to-all-done.1.own_ref = bf16[4,136,256]{2,1,0:T(8,128)(2,1)S(1)} async-done(((bf16[4,136,256]{2,1,0:T(8,128)(2,1)}), bf16[4,136,256]{2,1,0:T(8,128)(2,1)S(1)}, u32[]{:S(2)}, u32[]{:S(2)}) %all-to-all-start.1) | async-done | bytes 278560 | tf_op jit(solution)/shard_map/all_to_all | solution.py:29
  112.9 6.5 %all-to-all-start = ((bf16[4,272,128]{2,1,0:T(8,128)(2,1)}), bf16[4,272,128]{2,1,0:T(8,128)(2,1)S(1)}, u32[]{:S(2)}, u32[]{:S(2)}) async-start(bf16[4,272,128]{2,1,0:T(8,128)(2,1)} %broadcast_in_dim.2), calls=%async_computation | async-start | bytes 557056 | tf_op jit(solution)/shard_map/all_to_all | solution.py:29
  121.4 5.1 %collective-permute-start.1 = (bf16[4,136,256]{2,1,0:T(8,128)(2,1)S(1)}, bf16[4,136,256]{2,1,0:T(8,128)(2,1)S(1)}, u32[]{:S(2)}, u32[]{:S(2)}) collective-permute-start(bf16[4,136,256]{2,1,0:T(8,128)(2,1)S(1)} %all-to-all-done.1.own_ref), channel_id=1, source_target_pairs={{0,480},{32,0},{64,32},{96,64},{128,96},{160,128},{192,160},{224,1... | collective-permute-start | bytes 835592 | tf_op jit(solution)/shard_map/ppermute | solution.py:25
  126.5 1.9 collective-permute-start.3
  128.5 6.0 %collective-permute-start.2 = (bf16[2,136,256]{2,1,0:T(8,128)(2,1)S(1)}, bf16[2,136,256]{2,1,0:T(8,128)(2,1)S(1)}, u32[]{:S(2)}, u32[]{:S(2)}) collective-permute-start(bf16[2,136,256]{2,1,0:T(8,128)(2,1)S(1)} %get-tuple-element.22), channel_id=1, source_target_pairs={{0,448},{32,480},{64,0},{96,32},{128,64},{160,96},{192,128},{224,1... | collective-permute-start | bytes 417800 | tf_op jit(solution)/shard_map/ppermute | solution.py:25
  134.5 3.5 %attend_own.1 = (bf16[2080,128]{1,0:T(8,128)(2,1)S(1)}, f32[2080,128]{1,0:T(8,128)S(1)}) custom-call(s32[7]{0:T(128)S(1)} %stack.48.at_ref, f32[2]{0:T(128)S(1)} %slice_reduce_fusion.gate_ref, bf16[4,272,128]{2,1,0:T(8,128)(2,1)S(1)} %all-to-all-done.q_ref, bf16[4,136,256]{2,1,0:T(8,128)(2,1)S(1)} %all-to-all-done.1.own_ref), custom_call_target="tpu_custom_call" | custom-call | flops 2000000000 | bytes 1048576 | tf_op jit(solution)/shard_map/attend_own/pallas_call | solution.py:124
  139.0 6.3 %attend_rest.1 = bf16[4,576,128]{2,1,0:T(8,128)(2,1)S(1)} custom-call(s32[7]{0:T(128)S(1)} %stack.48.at_ref, f32[2]{0:T(128)S(1)} %slice_reduce_fusion.gate_ref, bf16[2080,128]{1,0:T(8,128)(2,1)S(1)} %get-tuple-element.15.qa, f32[2080,128]{1,0:T(8,128)S(1)} %get-tuple-element.16.state_ref, bf16[4,136,256]{2,1,0:T(8,128)(2,1)S(1)} %collective-permute-done.1.next_ref, ...), custom_call_target="tpu_custom_call" | custom-call | flops 6000000000 | bytes 4194304 | tf_op jit(solution)/shard_map/attend_rest/pallas_call | solution.py:206
  145.3 11.6 %all_to_all.26.in_ref = bf16[4,576,128]{2,1,0:T(8,128)(2,1)S(1)} all-to-all(bf16[4,576,128]{2,1,0:T(8,128)(2,1)S(1)} %attend_rest.1), channel_id=1, replica_groups=mesh['zh'=4,'zl'=4,'yh'=2,'yl'=2,'x'=4,'c'=2] {'yh','yl'}, dimensions={0} | all-to-all | bytes 1179648 | tf_op jit(solution)/shard_map/all_to_all | solution.py:29
  157.5 13.1 %all-gather = bf16[2112,128]{1,0:T(8,128)(2,1)S(1)} all-gather(bf16[528,128]{1,0:T(8,128)(2,1)S(1)} %merge.1), channel_id=2, replica_groups=mesh['zh'=4,'zl'=4,'yh'=2,'yl'=2,'x'=4,'c'=2] {'x'}, dimensions={0}, use_global_device_ids=true | all-gather | bytes 675840 | tf_op jit(solution)/shard_map/all_gather | solution.py:425
  174.4 11.7 %feed.1 = (bf16[2,4,256,256]{3,2,1,0:T(8,128)(2,1)S(1)}, bf16[2,4,256,256]{3,2,1,0:T(8,128)(2,1)S(1)}, bf16[256,256]{1,0:T(8,128)(2,1)S(1)}) custom-call(s32[7]{0:T(128)S(1)} %stack.48.at_ref, bf16[4,528,128]{2,1,0:T(8,128)(2,1)S(1)} %bitcast.23, bf16[4,528,128]{2,1,0:T(8,128)(2,1)S(1)} %collective-permute-done.5.attn_other, ...), custom_call_target="tpu_custom_call" | custom-call | flops 5000000000 | bytes 16777216 | tf_op jit(solution)/shard_map/feed/pallas_call | solution.py:334
  186.2 2.0 collective-permute-start.11
  188.2 2.5 %collective-permute-done.11 = bf16[2,4,256,256]{3,2,1,0:T(8,128)(2,1)S(1)} collective-permute-done((bf16[2,4,256,256]{3,2,1,0:T(8,128)(2,1)S(1)}, bf16[2,4,256,256]{3,2,1,0:T(8,128)(2,1)S(1)}, u32[]{:S(2)}, u32[]{:S(2)}) %collective-permute-start.11) | collective-permute-done | bytes 1048608 | tf_op jit(solution)/shard_map/ppermute | solution.py:25
  191.1 20.1 %all_to_all.27 = bf16[8,256,256]{2,1,0:T(8,128)(2,1)S(1)} all-to-all(bf16[8,256,256]{2,1,0:T(8,128)(2,1)S(1)} %bitcast.25), channel_id=1, replica_groups=mesh['zh'=4,'zl'=4,'yh'=2,'yl'=2,'x'=4,'c'=2] {'yl','x'}, dimensions={0} | all-to-all | bytes 2097152 | tf_op jit(solution)/shard_map/all_to_all | solution.py:29
  (45 shorter events, 16.4 us)
Async XLA Ops:
  6.5 30.4 %copy-start.1 = (bf16[256,256]{1,0:T(8,128)(2,1)S(1)}, bf16[256,256]{1,0:T(8,128)(2,1)}, u32[]{:S(2)}) copy-start(bf16[256,256]{1,0:T(8,128)(2,1)} %resid_ref.1) | copy-start | bytes 393220
  6.5 30.4 %copy-start.2 = (bf16[1024,256]{1,0:T(8,128)(2,1)S(1)}, bf16[1024,256]{1,0:T(8,128)(2,1)}, u32[]{:S(2)}) copy-start(bf16[1024,256]{1,0:T(8,128)(2,1)} %param.14) | copy-start | bytes 1572868
  6.5 167.9 %all-gather.4.cloned.1.call-start = ((), (), s32[]{:S(2)}) async-start(), calls=%async_computation.5 | async-start | bytes 5013504 | tf_op jit(solution)/shard_map/all_gather | solution.py:404
  23.1 5.9 %collective-permute-start = (bf16[16,384]{1,0:T(8,128)(2,1)}, bf16[16,384]{1,0:T(8,128)(2,1)S(1)}, u32[]{:S(2)}, u32[]{:S(2)}) collective-permute-start(bf16[16,384]{1,0:T(8,128)(2,1)} %get-tuple-element.13), channel_id=1, source_target_pairs={{0,8},{8,16},{16,24},{24,32},{32,40},{40,48},{48,56},{56,64},{64,7... | collective-permute-start | bytes 36872 | tf_op jit(solution)/shard_map/ppermute | solution.py:25
  30.0 6.9 %collective-permute-start.6 = (bf16[272,256]{1,0:T(8,128)(2,1)S(1)}, bf16[272,256]{1,0:T(8,128)(2,1)S(1)}, u32[]{:S(2)}, u32[]{:S(2)}) collective-permute-start(bf16[272,256]{1,0:T(8,128)(2,1)S(1)} %pad_maximum_fusion.5), channel_id=1, source_target_pairs={{0,8},{8,0},{1,9},{9,1},{2,10},{10,2},{3,11},{11,3},{4,12},{12,4},... | collective-permute-start | bytes 417800 | tf_op jit(solution)/shard_map/ppermute | solution.py:25
  37.1 24.0 %collective-permute-start.9 = (bf16[1552,256]{1,0:T(8,128)(2,1)S(1)}, bf16[1552,256]{1,0:T(8,128)(2,1)S(1)}, u32[]{:S(2)}, u32[]{:S(2)}) collective-permute-start(bf16[1552,256]{1,0:T(8,128)(2,1)S(1)} %fusion.2), channel_id=1, source_target_pairs={{0,4},{2,6},{4,0},{6,2},{1,5},{3,7},{5,1},{7,3},{8,12},{10,14},{12... | collective-permute-start | bytes 2383880 | tf_op jit(solution)/shard_map/ppermute | solution.py:25
  39.0 30.9 %collective-permute-start.8 = (bf16[1552,256]{1,0:T(8,128)(2,1)S(1)}, bf16[1552,256]{1,0:T(8,128)(2,1)S(1)}, u32[]{:S(2)}, u32[]{:S(2)}) collective-permute-start(bf16[1552,256]{1,0:T(8,128)(2,1)S(1)} %fusion.2), channel_id=1, source_target_pairs={{0,6},{2,0},{4,2},{6,4},{1,7},{3,1},{5,3},{7,5},{8,14},{10,8},{12,... | collective-permute-start | bytes 2383880 | tf_op jit(solution)/shard_map/ppermute | solution.py:25
  41.3 28.6 %collective-permute-start.7 = (bf16[1552,256]{1,0:T(8,128)(2,1)S(1)}, bf16[1552,256]{1,0:T(8,128)(2,1)S(1)}, u32[]{:S(2)}, u32[]{:S(2)}) collective-permute-start(bf16[1552,256]{1,0:T(8,128)(2,1)S(1)} %fusion.2), channel_id=1, source_target_pairs={{0,2},{2,4},{4,6},{6,0},{1,3},{3,5},{5,7},{7,1},{8,10},{10,12},{12... | collective-permute-start | bytes 2383880 | tf_op jit(solution)/shard_map/ppermute | solution.py:25
  69.9 18.1 %copy-start.5 = (f32[2,256]{1,0:T(2,128)S(1)}, f32[2,256]{1,0:T(2,128)}, u32[]{:S(2)}) copy-start(f32[2,256]{1,0:T(2,128)} %decay_ref.1) | copy-start | bytes 6148
  69.9 18.2 %copy-start.3 = (bf16[256,128]{1,0:T(8,128)(2,1)S(1)}, bf16[256,128]{1,0:T(8,128)(2,1)}, u32[]{:S(2)}) copy-start(bf16[256,128]{1,0:T(8,128)(2,1)} %q_ref.1) | copy-start | bytes 196612
  71.8 102.6 %collective-permute-start.10 = (bf16[4,1552,256]{2,1,0:T(8,128)(2,1)}, bf16[4,1552,256]{2,1,0:T(8,128)(2,1)}, u32[]{:S(2)}, u32[]{:S(2)}) collective-permute-start(bf16[4,1552,256]{2,1,0:T(8,128)(2,1)} %pad_maximum_fusion.wide_own), channel_id=1, source_target_pairs={{0,1},{1,0},{2,3},{3,2},{4,5},{5,4},{6,7},{7,6},{8,9},{9,8},{10,11... | collective-permute-start | bytes 9535496 | tf_op jit(solution)/shard_map/ppermute | solution.py:25
  73.7 38.4 %all-to-all-start.1 = ((bf16[4,136,256]{2,1,0:T(8,128)(2,1)}), bf16[4,136,256]{2,1,0:T(8,128)(2,1)S(1)}, u32[]{:S(2)}, u32[]{:S(2)}) async-start(bf16[4,136,256]{2,1,0:T(8,128)(2,1)} %get-tuple-element.14), calls=%async_computation.1 | async-start | bytes 557056 | tf_op jit(solution)/shard_map/all_to_all | solution.py:29
  112.9 21.6 %all-to-all-start = ((bf16[4,272,128]{2,1,0:T(8,128)(2,1)}), bf16[4,272,128]{2,1,0:T(8,128)(2,1)S(1)}, u32[]{:S(2)}, u32[]{:S(2)}) async-start(bf16[4,272,128]{2,1,0:T(8,128)(2,1)} %broadcast_in_dim.2), calls=%async_computation | async-start | bytes 557056 | tf_op jit(solution)/shard_map/all_to_all | solution.py:29
  119.4 19.5 %collective-permute-start.4 = (bf16[4,136,256]{2,1,0:T(8,128)(2,1)S(1)}, bf16[4,136,256]{2,1,0:T(8,128)(2,1)S(1)}, u32[]{:S(2)}, u32[]{:S(2)}) collective-permute-start(bf16[4,136,256]{2,1,0:T(8,128)(2,1)S(1)} %all-to-all-done.1.own_ref), channel_id=1, source_target_pairs={{0,32},{32,64},{64,96},{96,128},{128,160},{160,192},{192,224},{224... | collective-permute-start | bytes 835592 | tf_op jit(solution)/shard_map/ppermute | solution.py:25
  121.4 17.6 %collective-permute-start.1 = (bf16[4,136,256]{2,1,0:T(8,128)(2,1)S(1)}, bf16[4,136,256]{2,1,0:T(8,128)(2,1)S(1)}, u32[]{:S(2)}, u32[]{:S(2)}) collective-permute-start(bf16[4,136,256]{2,1,0:T(8,128)(2,1)S(1)} %all-to-all-done.1.own_ref), channel_id=1, source_target_pairs={{0,480},{32,0},{64,32},{96,64},{128,96},{160,128},{192,160},{224,1... | collective-permute-start | bytes 835592 | tf_op jit(solution)/shard_map/ppermute | solution.py:25
  126.5 11.4 %collective-permute-start.3 = (bf16[2,136,256]{2,1,0:T(8,128)(2,1)S(1)}, bf16[2,136,256]{2,1,0:T(8,128)(2,1)S(1)}, u32[]{:S(2)}, u32[]{:S(2)}) collective-permute-start(bf16[2,136,256]{2,1,0:T(8,128)(2,1)S(1)} %get-tuple-element.21), channel_id=1, source_target_pairs={{0,64},{32,96},{64,128},{96,160},{128,192},{160,224},{192,256},{22... | collective-permute-start | bytes 417800 | tf_op jit(solution)/shard_map/ppermute | solution.py:25
  128.5 10.5 %collective-permute-start.2 = (bf16[2,136,256]{2,1,0:T(8,128)(2,1)S(1)}, bf16[2,136,256]{2,1,0:T(8,128)(2,1)S(1)}, u32[]{:S(2)}, u32[]{:S(2)}) collective-permute-start(bf16[2,136,256]{2,1,0:T(8,128)(2,1)S(1)} %get-tuple-element.22), channel_id=1, source_target_pairs={{0,448},{32,480},{64,0},{96,32},{128,64},{160,96},{192,128},{224,1... | collective-permute-start | bytes 417800 | tf_op jit(solution)/shard_map/ppermute | solution.py:25
  145.2 27.3 %copy-start.4 = (f32[3,2,704]{2,1,0:T(2,128)S(1)}, f32[3,2,704]{2,1,0:T(2,128)}, u32[]{:S(2)}) copy-start(f32[3,2,704]{2,1,0:T(2,128)} %param.18) | copy-start | bytes 50692
  145.2 29.2 %copy-start = (f32[2048]{0:T(1024)S(1)}, f32[2048]{0:T(1024)}, u32[]{:S(2)}) copy-start(f32[2048]{0:T(1024)} %param.15) | copy-start | bytes 24580
  170.6 3.8 %collective-permute-start.5 = (bf16[4,528,128]{2,1,0:T(8,128)(2,1)S(1)}, bf16[4,528,128]{2,1,0:T(8,128)(2,1)S(1)}, u32[]{:S(2)}, u32[]{:S(2)}) collective-permute-start(bf16[4,528,128]{2,1,0:T(8,128)(2,1)S(1)} %bitcast.22), channel_id=1, source_target_pairs={{0,1},{1,0},{2,3},{3,2},{4,5},{5,4},{6,7},{7,6},{8,9},{9,8},{10,11... | collective-permute-start | bytes 1622024 | tf_op jit(solution)/shard_map/ppermute | solution.py:25
  186.2 4.6 %collective-permute-start.11 = (bf16[2,4,256,256]{3,2,1,0:T(8,128)(2,1)S(1)}, bf16[2,4,256,256]{3,2,1,0:T(8,128)(2,1)S(1)}, u32[]{:S(2)}, u32[]{:S(2)}) collective-permute-start(bf16[2,4,256,256]{3,2,1,0:T(8,128)(2,1)S(1)} %get-tuple-element.20), channel_id=1, source_target_pairs={{0,1},{1,0},{2,3},{3,2},{4,5},{5,4},{6,7},{7,6},{8,9},{9,8},{10,11... | collective-permute-start | bytes 3145736 | tf_op jit(solution)/shard_map/ppermute | solution.py:25
Sparse Core Ops, SparseCore 0:
  23.2 87.6 all-gather.3
